TPU v7x, 128 devices: a whole 4x4x4 slice. The times are simulated.
128 devices in a mesh: sp: 16 (over z, y), tp: 4 (over x), dp: 2 (over core).
Axes of the slice: x: 4, y: 4, z: 4, core: 2. Of those that a mesh axis runs over, the one named last changes fastest.
Arguments:
- latent: bfloat16 [32768, 2048], P(('dp', 'sp', 'tp')), parts along dimension 0, may hold values from -6 to 6
- cond: bfloat16 [4096], P('dp'), parts along dimension 0, may hold values from -6 to 6
- ctx_rows: bfloat16 [2048, 2048], P(('dp', 'sp')), parts along dimension 0, may hold values from -6 to 6
- ctx_cond: bfloat16 [2048], replicated, may hold values from -6 to 6
- mod_weight: bfloat16 [3, 2048, 2048], P(None, 'sp', 'tp'), may hold values from -0.125 to 0.125
- norm_gain: float32 [2048], replicated, may hold values from 0.1 to 1.9
- out_gain: float32 [2048], replicated, may hold values from 0.1 to 1.9
- w_query: bfloat16 [2048, 1024], replicated, may hold values from -16 to 16
- w_key: bfloat16 [2048, 256], replicated, may hold values from -1 to 1
- w_value: bfloat16 [2048, 256], replicated, may hold values from -0.125 to 0.125
- w_out: bfloat16 [1024, 2048], replicated, may hold values from -0.1875 to 0.1875
- sink: float32 [16], replicated, may hold values from 3 to 8
Outputs:
- updated: bfloat16 [32768, 2048], P(('dp', 'sp', 'tp')), parts along dimension 0
There are 2 independent parts, one for each index of `dp`. A program takes and returns all parts, laid end to end along the dimension named above; an argument that names none is the same for every part. Nothing has to cross between parts.
All inputs are finite; a program needn't handle non-finite values.
Results may differ from a plain program's by a relative error of at most 0.0053.
Values may be sent and summed in bfloat16 or wider, within the bound.
No kernel may reach another device: no remote copies, remote signals or barrier semaphores. Data moves between devices by JAX's collectives and lax.ppermute only.
A program may use at most 128 MiB of HBM per device.

v0:
```python
import jax
import jax.numpy as jnp
from jax import lax
from jax.sharding import PartitionSpec as P

HEAD_DIM = 64
WINDOW = 128
SPAN = 128
GRID_W = 64


EPSILON = 1e-06
NEG_BIG = -1e30


def sent_to_all(x, axis):
    size = lax.axis_size(axis)
    return lax.all_to_all(jnp.broadcast_to(x[None], (size, *x.shape)), axis, 0, 0, tiled=True)


def taken_together(x, axis):
    return sent_to_all(x, axis).sum(axis=0)


def in_one(arrays, axis):
    ends = [0]
    for a in arrays:
        ends.append(ends[-1] + a.size)
    so_far = taken_together(jnp.concatenate([a.ravel() for a in arrays]), axis)
    return tuple((so_far[b:e].reshape(a.shape) for a, b, e in zip(arrays, ends, ends[1:])))


def in_one_piece(arrays, axis, dim, along):
    ends, at = ([], 0)
    for a in arrays[:-1]:
        at += a.shape[along]
        ends.append(at)
    both = jnp.concatenate(arrays, axis=along)
    return tuple(jnp.split(lax.all_gather(both, axis, axis=dim, tiled=True), ends, axis=along))


def in_order(pieces, dim):
    pieces = jnp.moveaxis(pieces, 0, dim)
    lengths = pieces.shape
    return pieces.reshape(*lengths[:dim], lengths[dim] * lengths[dim + 1], *lengths[dim + 2 :])


def collect(x, axis, dim):
    return in_order(sent_to_all(x, axis), dim)


def with_halo(x, sides, width):
    edges = {}
    for axis, dim in sides:
        size, length = (lax.axis_size(axis), x.shape[dim])
        up = [(i, (i + 1) % size) for i in range(size - 1)]
        last = lax.slice_in_dim(x, length - width, length, axis=dim)
        leading = lax.slice_in_dim(x, 0, width, axis=dim)
        edges[dim] = (
            lax.ppermute(last, axis, up),
            lax.ppermute(leading, axis, [(b, a) for a, b in up]),
        )
    done = []
    for _, dim in sides:
        low, high = edges[dim]
        around = [(width, width) if d in done else (0, 0) for d in range(x.ndim)]
        x = jnp.concatenate([jnp.pad(low, around), x, jnp.pad(high, around)], axis=dim)
        done.append(dim)
    return x


def rope_angles(positions, head_width):
    freq_count = head_width // 4
    inverse = 10000.0 ** (-jnp.arange(freq_count, dtype=jnp.float32) / freq_count)
    grid_row = (positions // GRID_W).astype(jnp.float32)
    grid_col = (positions % GRID_W).astype(jnp.float32)
    angles = jnp.concatenate([grid_row[:, None] * inverse, grid_col[:, None] * inverse], axis=-1)
    return (jnp.cos(angles), jnp.sin(angles))


def rotate(values, cosine, sine_table):
    half_width = values.shape[-1] // 2
    floats = values.astype(jnp.float32)
    first = floats[..., :half_width]
    second = floats[..., half_width:]
    cos_b = cosine[:, None]
    sin_b = sine_table[:, None]
    return jnp.concatenate(
        [first * cos_b - second * sin_b, first * sin_b + second * cos_b], axis=-1
    ).astype(jnp.bfloat16)


def mod_norm(rows, gain, scale_vec, shift_vec):
    floats = rows.astype(jnp.float32)
    normed = floats * lax.rsqrt(jnp.mean(floats * floats, axis=-1, keepdims=True) + EPSILON) * gain
    return (normed * (1.0 + scale_vec) + shift_vec).astype(jnp.bfloat16)


def band_attention(
    query_rot,
    query_plain,
    key_padded,
    value_padded,
    key_ctx,
    value_ctx,
    sink_group,
    offset,
    seq_total,
):
    length_dev, groups, head_width = query_rot.shape
    blocks = length_dev // SPAN
    query_blocks = query_rot.reshape(blocks, SPAN, groups, head_width)
    plain_blocks = query_plain.reshape(blocks, SPAN, groups, head_width)
    key_split = key_padded.reshape(blocks + 2, SPAN, head_width)
    value_split = value_padded.reshape(blocks + 2, SPAN, head_width)
    key_band = jnp.concatenate([key_split[:-2], key_split[1:-1], key_split[2:]], axis=1)
    value_band = jnp.concatenate([value_split[:-2], value_split[1:-1], value_split[2:]], axis=1)
    factor = head_width ** (-0.5)
    local = (
        jnp.einsum("nigd,njd->ngij", query_blocks, key_band, preferred_element_type=jnp.float32)
        * factor
    )
    block_start = offset + jnp.arange(blocks, dtype=jnp.int32) * SPAN
    query_pos = block_start[:, None, None] + jnp.arange(SPAN, dtype=jnp.int32)[None, :, None]
    key_pos = (
        block_start[:, None, None] + jnp.arange(3 * SPAN, dtype=jnp.int32)[None, None, :] - SPAN
    )
    allowed = (jnp.abs(query_pos - key_pos) <= WINDOW) & (key_pos >= 0) & (key_pos < seq_total)
    local = jnp.where(allowed[:, None], local, NEG_BIG)
    context = (
        jnp.einsum("nigd,cd->ngic", plain_blocks, key_ctx, preferred_element_type=jnp.float32)
        * factor
    )
    sink_col = sink_group[None, :, None]
    row_max = jnp.maximum(jnp.maximum(jnp.max(local, axis=-1), jnp.max(context, axis=-1)), sink_col)
    exp_local = jnp.exp(local - row_max[..., None])
    exp_ctx = jnp.exp(context - row_max[..., None])
    exp_sink = jnp.exp(sink_col - row_max)
    denom = jnp.sum(exp_local, axis=-1) + jnp.sum(exp_ctx, axis=-1) + exp_sink
    weight_local = (exp_local / denom[..., None]).astype(jnp.bfloat16)
    weight_ctx = (exp_ctx / denom[..., None]).astype(jnp.bfloat16)
    mixed = jnp.einsum(
        "ngij,njd->nigd", weight_local, value_band, preferred_element_type=jnp.float32
    ) + jnp.einsum("ngic,cd->nigd", weight_ctx, value_ctx, preferred_element_type=jnp.float32)
    return mixed.astype(jnp.bfloat16).reshape(length_dev, groups * head_width)


def shards(
    latent,
    cond,
    ctx_rows,
    ctx_cond,
    mod_weight,
    norm_gain,
    out_gain,
    w_query,
    w_key,
    w_value,
    w_out,
    sink,
):
    sp_size = lax.axis_size("sp")
    tp_size = lax.axis_size("tp")
    sp_index = lax.axis_index("sp")
    tp_index = lax.axis_index("tp")
    row_piece = mod_weight.shape[1]
    head_width = HEAD_DIM
    kv_count = w_key.shape[1] // head_width
    group_size = w_query.shape[1] // w_key.shape[1]
    vectors = jax.nn.silu(jnp.stack([cond, ctx_cond]).astype(jnp.float32)).astype(jnp.bfloat16)
    own_rows = lax.dynamic_slice_in_dim(vectors, sp_index * row_piece, row_piece, 1)
    shift_part = jnp.dot(own_rows, mod_weight[0], preferred_element_type=jnp.float32)
    scale_part = jnp.dot(own_rows, mod_weight[1], preferred_element_type=jnp.float32)
    gate_part = jnp.dot(own_rows[:1], mod_weight[2], preferred_element_type=jnp.float32)
    summed = in_one((shift_part, scale_part, gate_part), "sp")
    shift_vec, scale_vec, gate_vec = in_one_piece((summed[0], summed[1], summed[2]), "tp", 1, 0)
    key_width = w_key.shape[1]
    ctx_hidden = mod_norm(ctx_rows, norm_gain, scale_vec[1], shift_vec[1])
    own_keys = jnp.dot(ctx_hidden, w_key, preferred_element_type=jnp.float32).astype(jnp.bfloat16)
    own_values = jnp.dot(ctx_hidden, w_value, preferred_element_type=jnp.float32).astype(
        jnp.bfloat16
    )
    collected = collect(jnp.concatenate([own_keys, own_values], axis=1), "sp", 0)
    key_ctx = collected[:, :key_width]
    value_ctx = collected[:, key_width:]
    hidden = mod_norm(latent, norm_gain, scale_vec[0], shift_vec[0])
    query = jnp.dot(hidden, w_query, preferred_element_type=jnp.float32).astype(jnp.bfloat16)
    key_rows = jnp.dot(hidden, w_key, preferred_element_type=jnp.float32).astype(jnp.bfloat16)
    value_rows = jnp.dot(hidden, w_value, preferred_element_type=jnp.float32).astype(jnp.bfloat16)
    row_count = query.shape[0]
    offset = (sp_index * tp_size + tp_index) * row_count
    seq_total = sp_size * tp_size * row_count
    cosine, sine_table = rope_angles(offset + jnp.arange(row_count, dtype=jnp.int32), head_width)
    query_heads = query.reshape(row_count, kv_count * group_size, head_width)
    query_rot = rotate(query_heads, cosine, sine_table).reshape(
        row_count, kv_count, group_size, head_width
    )
    query_grid = query_heads.reshape(row_count, kv_count, group_size, head_width)
    key_rot = rotate(key_rows.reshape(row_count, kv_count, head_width), cosine, sine_table)
    key_value = jnp.concatenate([key_rot.reshape(row_count, key_width), value_rows], axis=1)
    padded = with_halo(key_value, ((("sp", "tp"), 0),), SPAN)
    padded_rows = padded.shape[0]
    key_pad = padded[:, :key_width].reshape(padded_rows, kv_count, head_width)
    value_pad = padded[:, key_width:].reshape(padded_rows, kv_count, head_width)
    ctx_count = key_ctx.shape[0]

    def one_head(q_rot, q_plain, k_pad, v_pad, k_ctx, v_ctx, sink_group):
        return band_attention(
            q_rot, q_plain, k_pad, v_pad, k_ctx, v_ctx, sink_group, offset, seq_total
        )

    attended = jax.vmap(one_head, in_axes=(1, 1, 1, 1, 1, 1, 0), out_axes=1)(
        query_rot,
        query_grid,
        key_pad,
        value_pad,
        key_ctx.reshape(ctx_count, kv_count, head_width),
        value_ctx.reshape(ctx_count, kv_count, head_width),
        sink.reshape(kv_count, group_size),
    )
    mixed = attended.reshape(row_count, kv_count * group_size * head_width)
    projected = jnp.dot(mixed, w_out, preferred_element_type=jnp.float32)
    normed = (
        projected
        * lax.rsqrt(jnp.mean(projected * projected, axis=-1, keepdims=True) + EPSILON)
        * out_gain
    )
    return (latent.astype(jnp.float32) + gate_vec[0] * normed).astype(jnp.bfloat16)


def solution(mesh):
    placed = (
        P(("dp", "sp", "tp"), None),
        P("dp"),
        P(("dp", "sp"), None),
        P(),
        P(None, "sp", "tp"),
        P(),
        P(),
        P(),
        P(),
        P(),
        P(),
        P(),
    )
    return jax.shard_map(
        shards, mesh=mesh, in_specs=placed, out_specs=P(("dp", "sp", "tp"), None), check_vma=False
    )
```

profile of v0, /device:TPU:32, one launch (start us, length us, event | category | flops | bytes accessed | tf_op | source)
XLA Modules:
  0.0 113.0 jit_solution(10597692137023334534)
XLA Ops:
  0.0 0.8 stack.10
  1.6 1.0 fusion.38
  2.7 1.0 convolution_bitcast_fusion
  3.7 1.0 convolution_bitcast_fusion.1
  5.5 8.1 %all-to-all-start = ((f32[16,1,2560]{2,1,0:T(1,128)}), f32[16,1,2560]{2,1,0:T(1,128)S(1)}, u32[]{:S(2)}, u32[]{:S(2)}) async-start(f32[16,1,2560]{2,1,0:T(1,128)} %broadcast_in_dim.12), calls=%async_computation | async-start | bytes 327680 | tf_op jit(solution)/shard_map/all_to_all | solution.py:18
  13.8 1.1 fusion.16
  14.9 1.5 %fusion.6 = f32[256]{0:T(256)S(1)} fusion(bf16[256,2048]{1,0:T(8,128)(2,1)} %param.12), kind=kLoop, calls=%fused_computation.15 | loop fusion | flops 1572608 | bytes 1049600 | tf_op jit(solution)/shard_map/reduce_sum | solution.py:95
  17.9 2.0 %all-to-all-done = f32[16,1,2560]{2,1,0:T(1,128)S(1)} async-done(((f32[16,1,2560]{2,1,0:T(1,128)}), f32[16,1,2560]{2,1,0:T(1,128)S(1)}, u32[]{:S(2)}, u32[]{:S(2)}) %all-to-all-start) | async-done | bytes 163872 | tf_op jit(solution)/shard_map/all_to_all | solution.py:18
  20.1 12.3 %all_gather.3 = f32[5,2048]{1,0:T(8,128)S(1)} all-gather(f32[5,512]{1,0:T(8,128)S(1)} %pad_maximum_fusion.5), channel_id=1, replica_groups=mesh['sp'=16,'tp'=4,'dp'=2] {'tp'}, dimensions={1}, use_global_device_ids=true | all-gather | bytes 51200 | tf_op jit(solution)/shard_map/all_gather | solution.py:39
  32.5 1.7 %convolution_convert_fusion.3 = bf16[64,256]{1,0:T(8,128)(2,1)S(1)} fusion(bf16[2048,256]{1,0:T(8,128)(2,1)} %param.21, bf16[64,2048]{1,0:T(8,128)(2,1)} %param.14, f32[2048]{0:T(1024)S(1)} %bitcast.162, f32[2048]{0:T(1024)S(1)} %bitcast.164, f32[2048]{0:T(1024)} %param.17, f32[64]{0:T(128)S(1)} %add_rsqrt_fusion.2), kind=kOutput, calls=%fused_computation.29 | convolution fusion | flops 67911680 | bytes 1368320 | tf_op jit(solution)/shard_map/dot_general | solution.py:180
  34.5 1.4 %convolution_convert_fusion.2 = bf16[256,256]{0,1:T(8,128)(2,1)} fusion(bf16[2048,256]{1,0:T(8,128)(2,1)S(1)} %copy-done, bf16[256,2048]{1,0:T(8,128)(2,1)S(1)} %copy-done.1, f32[2048]{0:T(1024)S(1)} %bitcast.156, f32[2048]{0:T(1024)S(1)} %bitcast.159, f32[2048]{0:T(1024)S(1)} %copy-done.12, f32[256]{0:T(256)S(1)} %add_rsqrt_fusion.1), kind=kOutput, calls=%fused_computation.28 | convolution fusion | flops 271646720 | bytes 2253824 | tf_op jit(solution)/shard_map/dot_general | solution.py:188
  36.8 1.4 %convolution_convert_fusion = bf16[256,1024]{1,0:T(8,128)(2,1)S(1)} fusion(bf16[2048,1024]{1,0:T(8,128)(2,1)S(1)} %copy-done.10, bf16[256,2048]{1,0:T(8,128)(2,1)S(1)} %copy-done.1, f32[2048]{0:T(1024)S(1)} %bitcast.158, f32[2048]{0:T(1024)S(1)} %bitcast.161, f32[2048]{0:T(1024)S(1)} %copy-done.12, f32[256]{0:T(256)S(1)} %add_rsqrt_fusion.1), kind=kOutput, calls=%fused_computation.26 | convolution fusion | flops 1077149696 | bytes 5792768 | tf_op jit(solution)/shard_map/dot_general | solution.py:187
  38.9 1.0 copy.58
  39.9 1.2 %copy.55 = f32[256,1024]{0,1:T(8,128)S(1)} copy(bf16[256,1024]{1,0:T(8,128)(2,1)} %copy-done.3) | data formatting | bytes 1572864 | tf_op jit(solution)/shard_map/convert_element_type | solution.py:83
  41.2 1.1 broadcast_in_dim.15
  42.3 5.4 %all-to-all-start.1 = ((bf16[16,64,512]{2,1,0:T(8,128)(2,1)}), bf16[16,64,512]{2,1,0:T(8,128)(2,1)S(1)}, u32[]{:S(2)}, u32[]{:S(2)}) async-start(bf16[16,64,512]{2,1,0:T(8,128)(2,1)} %broadcast_in_dim.15), calls=%async_computation.1 | async-start | bytes 2097152 | tf_op jit(solution)/shard_map/all_to_all | solution.py:18
  47.7 0.9 convert.20
  48.7 6.4 %collective-permute-start.1 = (bf16[128,512]{0,1:T(8,128)(2,1)S(1)}, bf16[128,512]{0,1:T(8,128)(2,1)S(1)}, u32[]{:S(2)}, u32[]{:S(2)}) collective-permute-start(bf16[128,512]{0,1:T(8,128)(2,1)S(1)} %get-tuple-element.20), channel_id=1, source_target_pairs={{2,0},{4,2},{6,4},{8,6},{10,8},{12,10},{14,12},{16,14},{18,16},{20... | collective-permute-start | bytes 393224 | tf_op jit(solution)/shard_map/ppermute | solution.py:61
  55.1 2.1 %collective-permute-start = (bf16[128,512]{0,1:T(8,128)(2,1)S(1)}, bf16[128,512]{0,1:T(8,128)(2,1)S(1)}, u32[]{:S(2)}, u32[]{:S(2)}) collective-permute-start(bf16[128,512]{0,1:T(8,128)(2,1)S(1)} %get-tuple-element.19), channel_id=1, source_target_pairs={{0,2},{2,4},{4,6},{6,8},{8,10},{10,12},{12,14},{14,16},{16,18},{18... | collective-permute-start | bytes 393224 | tf_op jit(solution)/shard_map/ppermute | solution.py:60
  57.2 0.9 subtract_convert_fusion
  58.2 8.0 %collective-permute-done = bf16[128,512]{0,1:T(8,128)(2,1)S(1)} collective-permute-done((bf16[128,512]{0,1:T(8,128)(2,1)S(1)}, bf16[128,512]{0,1:T(8,128)(2,1)S(1)}, u32[]{:S(2)}, u32[]{:S(2)}) %collective-permute-start) | collective-permute-done | bytes 131104 | tf_op jit(solution)/shard_map/ppermute | solution.py:60
  68.6 4.7 %fusion.4 = (f32[4,2,4,128]{3,2,1,0:T(4,128)S(1)}, f32[4,2,384,128,4]{3,2,4,1,0:T(8,128)}) fusion(pred[2,128,384]{1,2,0:T(8,128)(4,1)S(1)} %fusion.36, bf16[4,2,128,64]{2,3,1,0:T(8,128)(2,1)S(1)} %copy.79, bf16[4,2,128,64]{2,3,1,0:T(8,128)(2,1)S(1)} %copy.78, bf16[4,2,128,64]{2,3,1,0:T(8,128)(2,1)S(1)} %copy.77, bf16[256,4,4,32]{0,3,2,1:T(8,128)(2,1)} %bitcast.150, ...), kind=kOutput, calls=%fused_computation.10 | convolution fusion | flops 208269312 | bytes 7323648 | tf_op jit(solution)/shard_map/vmap(nigd,njd->ngij)/dot_general | solution.py:120
  73.3 0.9 fusion.63
  74.1 1.0 copy.61
  75.1 2.2 %copy.57 = bf16[1024,256]{0,1:T(8,128)(2,1)} copy(bf16[1024,256]{1,0:T(8,128)(2,1)} %get-tuple-element.7) | data formatting | bytes 1048576 | tf_op jit(solution)/shard_map/slice | solution.py:184
  77.3 9.5 %bitcast_reduce_fusion = (f32[4,2,4,128]{3,2,1,0:T(4,128)S(1)}, f32[4,1024,2,128,4]{3,1,4,2,0:T(8,128)}) fusion(bf16[1024,4,64,1,1]{0,2,4,3,1:T(8,128)(2,1)} %bitcast.142, bf16[4,4,8,2,8,128]{5,4,3,2,1,0:T(8,128)(2,1)} %bitcast.141), kind=kOutput, calls=%fused_computation.1 | convolution fusion | flops 545255424 | bytes 17842176 | tf_op jit(solution)/shard_map/vmap(nigd,cd->ngic)/dot_general | solution.py:131
  86.9 1.4 %fusion.3 = f32[4,2,4,128]{3,2,1,0:T(4,128)S(1)} fusion(f32[4,2,384,128,4]{3,2,4,1,0:T(8,128)S(1)} %bitcast.136, f32[4,2,4,128]{3,2,1,0:T(4,128)S(1)} %maximum_maximum_fusion, pred[2,128,384]{1,2,0:T(8,128)(4,1)S(1)} %fusion.36), kind=kLoop, calls=%fused_computation.9 | loop fusion | flops 6287360 | bytes 6422528 | tf_op jit(solution)/shard_map/vmap()/reduce_sum | solution.py:139
  88.3 8.8 %fusion.1 = f32[4,2,4,128]{3,2,1,0:T(4,128)S(1)} fusion(f32[4,1024,2,128,4]{3,1,4,2,0:T(8,128)} %get-tuple-element.37, f32[4,2,4,128]{3,2,1,0:T(4,128)S(1)} %maximum_maximum_fusion), kind=kLoop, calls=%fused_computation.4 | loop fusion | flops 12578816 | bytes 16809984 | tf_op jit(solution)/shard_map/vmap()/reduce_sum | solution.py:139
  97.2 7.9 %fusion.13 = f32[4,2,128,4,64]{2,4,3,1,0:T(8,128)S(1)} fusion(bf16[1024,4,64,1,1]{0,2,4,3,1:T(8,128)(2,1)S(1)} %bitcast.147, f32[4,1024,2,128,4]{3,1,4,2,0:T(8,128)} %get-tuple-element.37, f32[4,2,4,128]{3,2,1,0:T(4,128)S(1)} %exponential_add_fusion, f32[4,2,4,128]{3,2,1,0:T(4,128)S(1)} %maximum_maximum_fusion), kind=kOutput, calls=%fused_computation.23 | convolution fusion | flops 553648128 | bytes 18382848 | tf_op jit(solution)/shard_map/vmap(ngic,cd->nigd)/dot_general | solution.py:144
  105.2 1.8 %fusion.15 = bf16[4,2,128,4,64]{2,4,3,1,0:T(8,128)(2,1)S(1)} fusion(f32[4,2,128,4,64]{2,4,3,1,0:T(8,128)S(1)} %fusion.13, f32[4,2,384,128,4]{3,2,4,1,0:T(8,128)S(1)} %bitcast.138, f32[4,2,4,128]{3,2,1,0:T(4,128)S(1)} %exponential_add_fusion, f32[4,2,4,128]{3,2,1,0:T(4,128)S(1)} %maximum_maximum_fusion, pred[2,128,384]{1,2,0:T(8,128)(4,1)S(1)} %fusion.36, ...), kind=kOutput, calls=%fused_computation.25 | convolution fusion | flops 210894848 | bytes 8388608 | tf_op jit(solution)/shard_map/vmap(ngij,njd->nigd)/dot_general | solution.py:142
  107.9 3.5 %multiply_reduce_fusion = (f32[256]{0:T(256)S(1)}, f32[256,2048]{1,0:T(8,128)S(1)}) fusion(bf16[256,1024]{0,1:T(8,128)(2,1)S(1)} %bitcast.148, bf16[1024,2048]{1,0:T(8,128)(2,1)} %param.22), kind=kOutput, calls=%fused_computation.21 | convolution fusion | flops 1074790144 | bytes 6816768 | tf_op jit(solution)/shard_map/dot_general | solution.py:222
  111.5 1.5 %fusion.11 = bf16[256,2048]{1,0:T(8,128)(2,1)} fusion(bf16[256,2048]{1,0:T(8,128)(2,1)S(1)} %copy-done.2, f32[256,2048]{1,0:T(8,128)S(1)} %get-tuple-element.39, f32[2048]{0:T(1024)S(1)} %copy-done.9, f32[256]{0:T(256)S(1)} %add_rsqrt_fusion, f32[2048]{0:T(1024)S(1)} %bitcast.152), kind=kLoop, calls=%fused_computation.20 | loop fusion | flops 3145728 | bytes 4211712 | tf_op jit(solution)/shard_map/convert_element_type | solution.py:228
  (87 shorter events, 8.8 us)
Async XLA Ops:
  0.0 34.1 %copy-start = (bf16[2048,256]{1,0:T(8,128)(2,1)S(1)}, bf16[2048,256]{1,0:T(8,128)(2,1)}, u32[]{:S(2)}) copy-start(bf16[2048,256]{1,0:T(8,128)(2,1)} %param.20) | copy-start | bytes 3145732
  0.0 34.1 %copy-start.6 = (bf16[64,2048]{1,0:T(8,128)(2,1)S(1)}, bf16[64,2048]{1,0:T(8,128)(2,1)}, u32[]{:S(2)}) copy-start(bf16[64,2048]{1,0:T(8,128)(2,1)} %param.14) | copy-start | bytes 786436
  0.0 34.5 %copy-start.1 = (bf16[256,2048]{1,0:T(8,128)(2,1)S(1)}, bf16[256,2048]{1,0:T(8,128)(2,1)}, u32[]{:S(2)}) copy-start(bf16[256,2048]{1,0:T(8,128)(2,1)} %param.12) | copy-start | bytes 3145732
  0.0 34.1 %copy-start.12 = (f32[2048]{0:T(1024)S(1)}, f32[2048]{0:T(1024)}, u32[]{:S(2)}) copy-start(f32[2048]{0:T(1024)} %param.17) | copy-start | bytes 24580
  5.5 14.4 %all-to-all-start = ((f32[16,1,2560]{2,1,0:T(1,128)}), f32[16,1,2560]{2,1,0:T(1,128)S(1)}, u32[]{:S(2)}, u32[]{:S(2)}) async-start(f32[16,1,2560]{2,1,0:T(1,128)} %broadcast_in_dim.12), calls=%async_computation | async-start | bytes 327680 | tf_op jit(solution)/shard_map/all_to_all | solution.py:18
  20.0 15.9 %copy-start.11 = (bf16[2048,256]{1,0:T(8,128)(2,1)S(1)}, bf16[2048,256]{1,0:T(8,128)(2,1)}, u32[]{:S(2)}) copy-start(bf16[2048,256]{1,0:T(8,128)(2,1)} %param.21) | copy-start | bytes 3145732
  34.5 2.3 %copy-start.10 = (bf16[2048,1024]{1,0:T(8,128)(2,1)S(1)}, bf16[2048,1024]{1,0:T(8,128)(2,1)}, u32[]{:S(2)}) copy-start(bf16[2048,1024]{1,0:T(8,128)(2,1)} %param.19) | copy-start | bytes 12582916
  38.1 0.8 copy-start.3
  42.3 31.0 %all-to-all-start.1 = ((bf16[16,64,512]{2,1,0:T(8,128)(2,1)}), bf16[16,64,512]{2,1,0:T(8,128)(2,1)S(1)}, u32[]{:S(2)}, u32[]{:S(2)}) async-start(bf16[16,64,512]{2,1,0:T(8,128)(2,1)} %broadcast_in_dim.15), calls=%async_computation.1 | async-start | bytes 2097152 | tf_op jit(solution)/shard_map/all_to_all | solution.py:18
  48.7 9.5 %collective-permute-start.1 = (bf16[128,512]{0,1:T(8,128)(2,1)S(1)}, bf16[128,512]{0,1:T(8,128)(2,1)S(1)}, u32[]{:S(2)}, u32[]{:S(2)}) collective-permute-start(bf16[128,512]{0,1:T(8,128)(2,1)S(1)} %get-tuple-element.20), channel_id=1, source_target_pairs={{2,0},{4,2},{6,4},{8,6},{10,8},{12,10},{14,12},{16,14},{18,16},{20... | collective-permute-start | bytes 393224 | tf_op jit(solution)/shard_map/ppermute | solution.py:61
  55.1 11.1 %collective-permute-start = (bf16[128,512]{0,1:T(8,128)(2,1)S(1)}, bf16[128,512]{0,1:T(8,128)(2,1)S(1)}, u32[]{:S(2)}, u32[]{:S(2)}) collective-permute-start(bf16[128,512]{0,1:T(8,128)(2,1)S(1)} %get-tuple-element.19), channel_id=1, source_target_pairs={{0,2},{2,4},{4,6},{6,8},{8,10},{10,12},{12,14},{14,16},{16,18},{18... | collective-permute-start | bytes 393224 | tf_op jit(solution)/shard_map/ppermute | solution.py:60
  58.2 10.4 %copy-start.5 = (bf16[256,16,32]{0,2,1:T(8,128)(2,1)S(1)}, bf16[256,16,32]{0,2,1:T(8,128)(2,1)}, u32[]{:S(2)}) copy-start(bf16[256,16,32]{0,2,1:T(8,128)(2,1)} %get-tuple-element.5) | copy-start | bytes 786436
  75.1 11.7 %slice-start = ((s8[6291456]{0:T(1024)(128)(4,1)}), s8[2097152]{0:T(1024)(128)(4,1)S(1)}, s32[]{:S(2)}) async-start(s8[6291456]{0:T(1024)(128)(4,1)} %bitcast.135), calls=%async_computation.2 | async-start | bytes 4194304
  77.3 9.6 %slice-start.1 = ((s8[6291456]{0:T(1024)(128)(4,1)}), s8[4194304]{0:T(1024)(128)(4,1)S(1)}, s32[]{:S(2)}) async-start(s8[6291456]{0:T(1024)(128)(4,1)} %bitcast.135), calls=%async_computation.3 | async-start | bytes 8388608
  88.3 8.9 %copy-start.4 = (bf16[1024,256]{0,1:T(8,128)(2,1)S(1)}, bf16[1024,256]{0,1:T(8,128)(2,1)}, u32[]{:S(2)}) copy-start(bf16[1024,256]{0,1:T(8,128)(2,1)} %copy.61) | copy-start | bytes 1572868
  88.3 16.9 %slice-start.2 = ((s8[6291456]{0:T(1024)(128)(4,1)}), s8[2097152]{0:T(1024)(128)(4,1)S(1)}, s32[]{:S(2)}) async-start(s8[6291456]{0:T(1024)(128)(4,1)} %bitcast.137), calls=%async_computation.4 | async-start | bytes 4194304
  97.2 8.0 %slice-start.3 = ((s8[6291456]{0:T(1024)(128)(4,1)}), s8[4194304]{0:T(1024)(128)(4,1)S(1)}, s32[]{:S(2)}) async-start(s8[6291456]{0:T(1024)(128)(4,1)} %bitcast.137), calls=%async_computation.5 | async-start | bytes 8388608
  97.2 8.0 %copy-start.7 = (bf16[4,2,128,64]{2,3,1,0:T(8,128)(2,1)S(1)}, bf16[4,2,128,64]{2,3,1,0:T(8,128)(2,1)}, u32[]{:S(2)}) copy-start(bf16[4,2,128,64]{2,3,1,0:T(8,128)(2,1)} %copy.75) | copy-start | bytes 393220
  97.2 8.0 %copy-start.8 = (bf16[4,2,128,64]{2,3,1,0:T(8,128)(2,1)S(1)}, bf16[4,2,128,64]{2,3,1,0:T(8,128)(2,1)}, u32[]{:S(2)}) copy-start(bf16[4,2,128,64]{2,3,1,0:T(8,128)(2,1)} %copy.74) | copy-start | bytes 393220
  107.6 3.9 %copy-start.2 = (bf16[256,2048]{1,0:T(8,128)(2,1)S(1)}, bf16[256,2048]{1,0:T(8,128)(2,1)}, u32[]{:S(2)}) copy-start(bf16[256,2048]{1,0:T(8,128)(2,1)} %param.12) | copy-start | bytes 3145732
  107.6 3.9 %copy-start.9 = (f32[2048]{0:T(1024)S(1)}, f32[2048]{0:T(1024)}, u32[]{:S(2)}) copy-start(f32[2048]{0:T(1024)} %param.18) | copy-start | bytes 24580
where the time goes:
time: 114 us; the launch traced here: 113 us
  matrix products  36.1 us (32%)
  starting transfers between devices  22 us (19%)
  other arithmetic  17.6 us (15%)
  local copies, waits for them, and re-layouts  14.5 us (13%)
  blocking collectives  12.3 us (11%)
  waiting for transfers between devices  10 us (9%)
    all_to_all x2, starting transfers between devices, sent_to_all(): lax.all_to_all(jnp.broadcast_to(x[None], (size, *x.shape)), axis, 0, 0, t...  13.5 us
    all_gather x1, blocking collectives, in_one_piece(): lax.all_gather(both, axis, axis=dim, tiled=True)  12.3 us
    reduce_sum x2, other arithmetic, band_attention(): denom = jnp.sum(exp_local, axis=-1) + jnp.sum(exp_ctx, axis=-1) + exp_sink  10.2 us
    dot_general x1, matrix products, band_attention(): jnp.einsum('nigd,cd->ngic', plain_blocks, key_ctx, preferred_element_type...  9.47 us
    ppermute x1, waiting for transfers between devices, with_halo(): lax.ppermute(last, axis, up)  8.02 us
    dot_general x1, matrix products, band_attention(): jnp.einsum('ngic,cd->nigd', weight_ctx, value_ctx, preferred_element_type...  7.93 us
    ppermute x1, starting transfers between devices, with_halo(): lax.ppermute(leading, axis, [(b, a) for a, b in up])  6.42 us
    dot_general x1, matrix products, band_attention(): jnp.einsum('nigd,njd->ngij', query_blocks, key_band, preferred_element_ty...  4.66 us
  transfers between devices with their start and end apart: 4, of which 2 were waited for; matrix products, arithmetic and copies ran while one was open for 12% of the time, Pallas kernels for 0%

commit v1 on v0

v1 whole, which is shorter than its diff:
```python
import jax
import jax.numpy as jnp
from jax import lax
from jax.experimental import pallas as pl
from jax.experimental.pallas import tpu as pltpu
from jax.sharding import PartitionSpec as P

HEAD_DIM = 64
WINDOW = 128
GRID_W = 64
EPSILON = 1e-06
NEG_BIG = -1e30
LOG2E = 1.4426950408889634
FACTOR = HEAD_DIM**-0.5 * LOG2E
F32 = jnp.float32
BF16 = jnp.bfloat16
VM = pltpu.MemorySpace.VMEM
SM = pltpu.MemorySpace.SMEM


def vspec(n):
    return [pl.BlockSpec(memory_space=VM)] * n


def dot(a, b):
    return jnp.dot(a, b, preferred_element_type=F32)


def dot_nt(a, b):
    return lax.dot_general(a, b, (((1,), (1,)), ((), ())), preferred_element_type=F32)


def iota(shape, dim):
    return lax.broadcasted_iota(jnp.int32, shape, dim)


def pick(h, cols, transposed):
    if transposed:
        out, inp = iota((cols, 256), 0), iota((cols, 256), 1)
    else:
        out, inp = iota((256, cols), 1), iota((256, cols), 0)
    return (inp == h * HEAD_DIM + (out & (HEAD_DIM - 1))).astype(F32).astype(BF16)


def swap_matrix():
    k, c = iota((256, 256), 0), iota((256, 256), 1)
    low = (c & 63) < 32
    neg = jnp.where(low & (k == c + 32), -1.0, 0.0)
    pos = jnp.where((~low) & (k == c - 32), 1.0, 0.0)
    return (neg + pos).astype(BF16)


def partials_kernel(vec_ref, mod_ref, out_ref):
    v = vec_ref[...]
    parts = [dot(v, mod_ref[i]) for i in range(3)]
    five = (parts[0][0:1], parts[0][1:2], parts[1][0:1], parts[1][1:2], parts[2][0:1])
    zero = jnp.zeros((1, 128), F32)
    rows = []
    for j in range(4):
        cut = [x[:, j * 128 : (j + 1) * 128] for x in five]
        rows.append(jnp.concatenate(cut[:3], axis=1))
        rows.append(jnp.concatenate(cut[3:] + [zero], axis=1))
    block = jnp.concatenate(rows, axis=0).astype(BF16)
    for i in range(out_ref.shape[0]):
        out_ref[i] = block


def normed(x, mult, shift):
    x = x.astype(F32)
    rs = lax.rsqrt(jnp.mean(x * x, axis=-1, keepdims=True) + EPSILON)
    return (x * rs * mult + shift).astype(BF16)


def context_kernel(recv_ref, gain_ref, ctx_ref, wk_ref, wv_ref, kv_ref, vec_ref):
    sums = []
    for t in range(4):
        acc = recv_ref[t].astype(F32)
        for s in range(1, 16):
            acc = acc + recv_ref[s * 4 + t].astype(F32)
        sums.append(acc)

    def vector(v):
        cuts = []
        for t in range(4):
            for j in range(4):
                r, c = 2 * j + v // 3, (v % 3) * 128
                cuts.append(sums[t][r : r + 1, c : c + 128])
        return jnp.concatenate(cuts, axis=1)

    gain = gain_ref[...]
    mult0 = gain * (1.0 + vector(2))
    mult1 = gain * (1.0 + vector(3))
    vec_ref[0:1, :] = mult0
    vec_ref[1:2, :] = vector(0)
    vec_ref[2:3, :] = vector(4)
    vec_ref[3:8, :] = jnp.zeros((5, 2048), F32)
    hidden = normed(ctx_ref[...], mult1, vector(1))
    k = dot(hidden, wk_ref[...]).astype(BF16)
    v = dot(hidden, wv_ref[...]).astype(BF16)
    for i in range(kv_ref.shape[0]):
        kv_ref[i, :, 0:256] = k
        kv_ref[i, :, 256:512] = v


def local_kernel(
    flags_ref, sink_ref, vec_ref, lo_ref, own_ref, hi_ref, wq_ref, wk_ref, wv_ref, cos_ref, sin_ref,
    q_ref, o_ref, l_ref, m_ref, hid_ref, key_ref, val_ref, rot_ref,
):
    mult, shift = vec_ref[0:1, :], vec_ref[1:2, :]
    hid_ref[128:384, :] = normed(own_ref[...], mult, shift)
    hid_ref[0:128, :] = normed(lo_ref[...], mult, shift)
    hid_ref[384:512, :] = normed(hi_ref[...], mult, shift)
    swap = swap_matrix()
    query = dot(hid_ref[128:384, :], wq_ref[...]).astype(BF16)
    q_ref[...] = query
    keys = dot(hid_ref[...], wk_ref[...]).astype(BF16)
    val_ref[...] = dot(hid_ref[...], wv_ref[...]).astype(BF16)
    cos, sin = cos_ref[...], sin_ref[...]
    key_ref[...] = (keys.astype(F32) * cos + dot(keys, swap) * sin).astype(BF16)
    for h in range(4):
        part = query[:, h * 256 : (h + 1) * 256]
        rot_ref[:, h * 256 : (h + 1) * 256] = (
            part.astype(F32) * cos[128:384] + dot(part, swap) * sin[128:384]
        ).astype(BF16)
    lane = iota((128, 256), 1) // HEAD_DIM
    first = iota((128, 128), 1) < HEAD_DIM
    row, col = iota((128, 128), 0), iota((128, 128), 1)
    low_bias = jnp.where(col >= row, 0.0, NEG_BIG)
    high_bias = jnp.where(col <= row, 0.0, NEG_BIG)
    low_edge = low_bias + jnp.where(flags_ref[0] > 0, 0.0, NEG_BIG)
    high_edge = high_bias + jnp.where(flags_ref[1] > 0, 0.0, NEG_BIG)
    ones = jnp.ones((512, 128), BF16)
    for h in range(4):
        kt = dot_nt(pick(h, 256, True), key_ref[...]).astype(BF16)
        va = jnp.concatenate([dot(val_ref[...], pick(h, 128, False)).astype(BF16), ones], axis=1)
        for b in range(2):
            q = rot_ref[b * 128 : (b + 1) * 128, h * 256 : (h + 1) * 256]
            stacked = jnp.concatenate(
                [jnp.where(lane == g, q, jnp.zeros_like(q)) for g in range(4)], axis=0
            )
            s = dot(stacked, kt[:, b * 128 : b * 128 + 384]) * FACTOR
            lb = low_edge if b == 0 else low_bias
            hb = high_edge if b == 1 else high_bias
            os, ls, ms = [], [], []
            for g in range(4):
                sg = s[g * 128 : (g + 1) * 128]
                s0, s1, s2 = sg[:, 0:128] + lb, sg[:, 128:256], sg[:, 256:384] + hb
                sink = sink_ref[h * 4 + g] * LOG2E
                m = jnp.max(jnp.maximum(jnp.maximum(s0, s1), s2), axis=-1, keepdims=True)
                m = jnp.maximum(m, sink)
                p = jnp.concatenate(
                    [jnp.exp2(s0 - m), jnp.exp2(s1 - m), jnp.exp2(s2 - m)], axis=1
                ).astype(BF16)
                o = dot(p, va[b * 128 : b * 128 + 384])
                mb = jnp.broadcast_to(m, (128, 128))
                os.append(o[:, 0:128])
                ls.append(o[:, 128:256] + jnp.exp2(sink - mb))
                ms.append(mb)
            for p2 in range(2):
                at = h * 256 + p2 * 128
                for ref, xs in ((o_ref, os), (l_ref, ls), (m_ref, ms)):
                    ref[b * 128 : (b + 1) * 128, at : at + 128] = jnp.where(
                        first, xs[2 * p2], xs[2 * p2 + 1]
                    )


def final_kernel(
    q_ref, kv_ref, o_ref, l_ref, m_ref, wo_ref, lat_ref, vec_ref, gain_ref, out_ref, mix_ref
):
    lane = iota((256, 256), 1) // HEAD_DIM
    first = iota((256, 128), 1) < HEAD_DIM
    keys = kv_ref[:, 0:256]
    vals = kv_ref[:, 256:512]
    ones = jnp.ones((1024, 128), BF16)
    for h in range(4):
        kt = dot_nt(pick(h, 256, True), keys).astype(BF16)
        va = jnp.concatenate([dot(vals, pick(h, 128, False)).astype(BF16), ones], axis=1)
        q = q_ref[:, h * 256 : (h + 1) * 256]
        for p2 in range(2):
            os, ls, ms = [], [], []
            for g in (2 * p2, 2 * p2 + 1):
                s = dot(jnp.where(lane == g, q, jnp.zeros_like(q)), kt) * FACTOR
                m = jnp.max(s, axis=-1, keepdims=True)
                p = jnp.exp2(s - m).astype(BF16)
                o = dot(p, va)
                os.append(o[:, 0:128])
                ls.append(o[:, 128:256])
                ms.append(jnp.broadcast_to(m, (256, 128)))
            at = h * 256 + p2 * 128
            oc, lc, mc = (jnp.where(first, x[0], x[1]) for x in (os, ls, ms))
            ml = m_ref[:, at : at + 128]
            top = jnp.maximum(ml, mc)
            wl, wc = jnp.exp2(ml - top), jnp.exp2(mc - top)
            num = wl * o_ref[:, at : at + 128] + wc * oc
            den = wl * l_ref[:, at : at + 128] + wc * lc
            mix_ref[:, at : at + 128] = (num / den).astype(BF16)
    projected = dot(mix_ref[...], wo_ref[...])
    rs = lax.rsqrt(jnp.mean(projected * projected, axis=-1, keepdims=True) + EPSILON)
    scale = vec_ref[2:3, :] * gain_ref[...]
    out_ref[...] = (lat_ref[...].astype(F32) + projected * rs * scale).astype(BF16)


def call(kernel, name, outs, scratch=(), specs=None, flops=0, moved=0, limit=32):
    return pl.pallas_call(
        kernel,
        out_shape=[jax.ShapeDtypeStruct(s, d) for s, d in outs],
        in_specs=specs,
        out_specs=vspec(len(outs)),
        scratch_shapes=[pltpu.VMEM(s, d) for s, d in scratch],
        compiler_params=pltpu.CompilerParams(vmem_limit_bytes=limit * 1024 * 1024),
        cost_estimate=pl.CostEstimate(flops=flops, bytes_accessed=moved, transcendentals=0),
        name=name,
    )


def shards(
    latent, cond, ctx_rows, ctx_cond, mod_weight, norm_gain, out_gain,
    w_query, w_key, w_value, w_out, sink,
):
    sp_size = lax.axis_size("sp")
    tp_size = lax.axis_size("tp")
    sp_index = lax.axis_index("sp")
    place = sp_index * tp_size + lax.axis_index("tp")
    both = ("sp", "tp")
    count = sp_size * tp_size
    piece = mod_weight.shape[1]
    rows = latent.shape[0]

    up = [(i, i + 1) for i in range(count - 1)]
    low = lax.ppermute(latent[rows - WINDOW :], both, up)
    high = lax.ppermute(latent[:WINDOW], both, [(b, a) for a, b in up])

    at = sp_index * piece
    raw = jnp.stack(
        [lax.dynamic_slice_in_dim(cond, at, piece), lax.dynamic_slice_in_dim(ctx_cond, at, piece)]
    )
    vectors = jax.nn.silu(raw.astype(F32)).astype(BF16)
    (parts,) = call(
        partials_kernel, "partials", [((count, 8, 384), BF16)], specs=vspec(2), flops=10**6, limit=4
    )(vectors, mod_weight)
    recv = lax.all_to_all(parts, both, 0, 0, tiled=True)
    gain_row = norm_gain.reshape(1, -1)
    kv_send, vecs = call(
        context_kernel,
        "context",
        [((sp_size, 64, 512), BF16), ((8, 2048), F32)],
        specs=vspec(5),
        flops=2 * 10**8,
        limit=12,
    )(recv, gain_row, ctx_rows, w_key, w_value)
    kv_ctx = lax.all_to_all(kv_send, "sp", 0, 0, tiled=True).reshape(sp_size * 64, 512)

    positions = place * rows - WINDOW + jnp.arange(rows + 2 * WINDOW, dtype=jnp.int32)
    freq = 10000.0 ** (-jnp.arange(HEAD_DIM // 4, dtype=F32) / (HEAD_DIM // 4))
    grid_row = (positions // GRID_W).astype(F32)
    grid_col = (positions % GRID_W).astype(F32)
    angles = jnp.concatenate([grid_row[:, None] * freq, grid_col[:, None] * freq], axis=-1)
    cosine, sine = jnp.tile(jnp.cos(angles), (1, 8)), jnp.tile(jnp.sin(angles), (1, 8))
    flags = jnp.stack([place > 0, place < count - 1]).astype(jnp.int32)
    smem = pl.BlockSpec(memory_space=SM)
    wide = (rows, 1024)
    query, o_loc, l_loc, m_loc = call(
        local_kernel,
        "local",
        [(wide, BF16), (wide, F32), (wide, F32), (wide, F32)],
        scratch=[((512, 2048), BF16), ((512, 256), BF16), ((512, 256), BF16), (wide, BF16)],
        specs=[smem, smem] + vspec(9),
        flops=6 * 10**9,
        limit=32,
    )(flags, sink, vecs, low, latent, high, w_query, w_key, w_value, cosine, sine)
    (updated,) = call(
        final_kernel,
        "final",
        [((rows, 2048), BF16)],
        scratch=[(wide, BF16)],
        specs=vspec(9),
        flops=6 * 10**9,
        limit=32,
    )(query, kv_ctx, o_loc, l_loc, m_loc, w_out, latent, vecs, out_gain.reshape(1, -1))
    return updated


def solution(mesh):
    placed = (
        P(("dp", "sp", "tp"), None),
        P("dp"),
        P(("dp", "sp"), None),
        P(),
        P(None, "sp", "tp"),
        P(),
        P(),
        P(),
        P(),
        P(),
        P(),
        P(),
    )
    return jax.shard_map(
        shards, mesh=mesh, in_specs=placed, out_specs=P(("dp", "sp", "tp"), None), check_vma=False
    )
```

time: 114 us -> 80.9 us (0.71)
  matrix products: 36.1 us -> 0 us
  Pallas kernels: 0 us -> 20.5 us
  other arithmetic: 17.6 us -> 0.43 us
  local copies, waits for them, and re-layouts: 14.5 us -> 28.2 us
  blocking collectives: 12.3 us -> 0 us
  waiting for transfers between devices: 10 us -> 5.34 us
  starting transfers between devices: 22 us -> 25.3 us
    dot_general x13 -> x0, matrix products: 36.1 us -> none  [the longest x1 9.47 us: band_attention(): jnp.einsum('nigd,cd->ngic', plain_blocks, key_ctx, preferred_element_type...]
    pallas_call x0 -> x4, Pallas kernels: none -> 20.5 us  [the longest x1 10.6 us: shards(): call(final_kernel, 'final', [((rows, 2048), BF16)], scratch=[(wide, BF16)...]
    unnamed x42 -> x46, local copies, waits for them, and re-layouts: 2.32 us -> 19.1 us
    reduce_sum x5 -> x0, other arithmetic: 12.9 us -> none  [the longest x2 10.2 us: band_attention(): denom = jnp.sum(exp_local, axis=-1) + jnp.sum(exp_ctx, axis=-1) + exp_sink]
    all_gather x1 -> x0, blocking collectives: 12.3 us -> none  [in_one_piece(): lax.all_gather(both, axis, axis=dim, tiled=True)]
    another operation x2 -> x5, local copies, waits for them, and re-layouts: 1.54 us -> 6.74 us  [the longest x2 2.92 us: shards(): jnp.tile(jnp.cos(angles), (1, 8))]
    all_to_all x2, starting transfers between devices: 13.5 us -> 16.7 us  [the longest x1 11.1 us: shards(): recv = lax.all_to_all(parts, both, 0, 0, tiled=True)]
    convert_element_type x3 -> x0, local copies, waits for them, and re-layouts: 2.78 us -> none  [the longest x1 1.24 us: rotate(): floats = values.astype(jnp.float32)]
  transfers between devices with their start and end apart: 4 -> 4, of which waited for: 2 -> 1; matrix products, arithmetic and copies ran while one was open for 12% -> 11% of each run, Pallas kernels for 0% -> 11%
where the time goes in v1:
time: 80.9 us; the launch traced here: 80 us
  local copies, waits for them, and re-layouts  28.2 us (35%)
  starting transfers between devices  25.3 us (31%)
  Pallas kernels  20.5 us (25%)
  waiting for transfers between devices  5.34 us (7%)
    unnamed x46, local copies, waits for them, and re-layouts  19.1 us
    all_to_all x1, starting transfers between devices, shards(): recv = lax.all_to_all(parts, both, 0, 0, tiled=True)  11.1 us
    pallas_call x1, Pallas kernels, shards(): call(final_kernel, 'final', [((rows, 2048), BF16)], scratch=[(wide, BF16)...  10.6 us
    pallas_call x1, Pallas kernels, shards(): call(local_kernel, 'local', [(wide, BF16), (wide, F32), (wide, F32), (wid...  8.34 us
    ppermute x1, starting transfers between devices, shards(): high = lax.ppermute(latent[:WINDOW], both, [(b, a) for a, b in up])  6.68 us
    all_to_all x1, starting transfers between devices, shards(): lax.all_to_all(kv_send, 'sp', 0, 0, tiled=True).reshape(sp_size * 64, 512)  5.65 us
    ppermute x1, waiting for transfers between devices, shards(): low = lax.ppermute(latent[rows - WINDOW:], both, up)  5.34 us
    another operation x2, local copies, waits for them, and re-layouts, shards(): jnp.tile(jnp.cos(angles), (1, 8))  2.92 us
  transfers between devices with their start and end apart: 4, of which 1 were waited for; matrix products, arithmetic and copies ran while one was open for 11% of the time, Pallas kernels for 11%

profile of v1, /device:TPU:32, one launch (start us, length us, event | category | flops | bytes accessed | tf_op | source)
XLA Modules:
  0.0 80.0 jit_solution(10443235825676479389)
XLA Ops:
  0.0 0.9 %dynamic-slice_bitcast_fusion = (bf16[1,128]{1,0:T(2,128)(2,1)S(1)}, bf16[1,128]{1,0:T(2,128)(2,1)S(1)}) fusion(bf16[2048]{0:T(1024)(128)(2,1)} %param.15, s32[]{:T(128)S(6)} %select_n.24, bf16[2048]{0:T(1024)(128)(2,1)} %param.13), kind=kLoop, calls=%fused_computation.24 | loop fusion | bytes 1028 | tf_op jit(solution)/shard_map/stack | solution.py:234
  1.0 1.0 %copy-done.6 = bf16[3,128,512]{2,1,0:T(8,128)(2,1)S(1)} copy-done((bf16[3,128,512]{2,1,0:T(8,128)(2,1)S(1)}, bf16[3,128,512]{2,1,0:T(8,128)(2,1)}, u32[]{:S(2)}) %copy-start.6) | copy-done | bytes 393240
  2.0 0.9 %partials.1 = bf16[64,8,384]{2,1,0:T(8,128)(2,1)} custom-call(bf16[2,128]{1,0:T(2,128)(2,1)S(1)} %fusion.9.vec_ref, bf16[3,128,512]{2,1,0:T(8,128)(2,1)S(1)} %copy-done.6), custom_call_target="tpu_custom_call" | custom-call | flops 1000000 | tf_op jit(solution)/shard_map/partials/pallas_call | solution.py:238
  2.9 11.1 %all-to-all-start = ((bf16[64,8,384]{2,1,0:T(8,128)(2,1)}), bf16[64,8,384]{2,1,0:T(8,128)(2,1)S(1)}, u32[]{:S(2)}, u32[]{:S(2)}) async-start(bf16[64,8,384]{2,1,0:T(8,128)(2,1)} %partials.1), calls=%async_computation | async-start | bytes 786432 | tf_op jit(solution)/shard_map/all_to_all | solution.py:241
  14.0 2.3 %fusion.10 = (bf16[128,2048]{1,0:T(8,128)(2,1)}, bf16[128,2048]{1,0:T(8,128)(2,1)}) fusion(bf16[256,2048]{1,0:T(8,128)(2,1)} %lat_ref.1), kind=kLoop, calls=%fused_computation.26 | loop fusion | bytes 2097152 | tf_op jit(solution)/shard_map/slice | solution.py:231
  16.3 6.7 %collective-permute-start.1 = (bf16[128,2048]{1,0:T(8,128)(2,1)}, bf16[128,2048]{1,0:T(8,128)(2,1)}, u32[]{:S(2)}, u32[]{:S(2)}) collective-permute-start(bf16[128,2048]{1,0:T(8,128)(2,1)} %get-tuple-element.17), channel_id=1, source_target_pairs={{2,0},{4,2},{6,4},{8,6},{10,8},{12,10},{14,12},{16,14},{18,16},{20... | collective-permute-start | bytes 1572872 | tf_op jit(solution)/shard_map/ppermute | solution.py:231
  23.0 1.9 %collective-permute-start = (bf16[128,2048]{1,0:T(8,128)(2,1)}, bf16[128,2048]{1,0:T(8,128)(2,1)}, u32[]{:S(2)}, u32[]{:S(2)}) collective-permute-start(bf16[128,2048]{1,0:T(8,128)(2,1)} %get-tuple-element.18), channel_id=1, source_target_pairs={{0,2},{2,4},{4,6},{6,8},{8,10},{10,12},{12,14},{14,16},{16,18},{18... | collective-permute-start | bytes 1572872 | tf_op jit(solution)/shard_map/ppermute | solution.py:230
  25.0 0.9 %copy-done.7 = bf16[64,2048]{1,0:T(8,128)(2,1)S(1)} copy-done((bf16[64,2048]{1,0:T(8,128)(2,1)S(1)}, bf16[64,2048]{1,0:T(8,128)(2,1)}, u32[]{:S(2)}) %copy-start.7) | copy-done | bytes 262168
  25.9 0.7 copy-done.8
  26.6 0.6 context.1
  27.3 1.0 %copy-done.3 = bf16[16,64,512]{2,1,0:T(8,128)(2,1)} copy-done((bf16[16,64,512]{2,1,0:T(8,128)(2,1)}, bf16[16,64,512]{2,1,0:T(8,128)(2,1)S(1)}, u32[]{:S(2)}) %copy-start.3) | copy-done | bytes 1048600
  28.2 0.6 copy-done.11
  28.9 5.7 %all-to-all-start.1 = ((bf16[16,64,512]{2,1,0:T(8,128)(2,1)}), bf16[16,64,512]{2,1,0:T(8,128)(2,1)}, u32[]{:S(2)}, u32[]{:S(2)}) async-start(bf16[16,64,512]{2,1,0:T(8,128)(2,1)} %copy-done.3), calls=%async_computation.1 | async-start | bytes 2097152 | tf_op jit(solution)/shard_map/all_to_all | solution.py:251
  34.8 0.9 %tile.20 = f32[512,8,32]{0,2,1:T(8,128)} broadcast(f32[512,32]{0,1:T(8,128)S(1)} %get-tuple-element.19), dimensions={0,2} | broadcast | bytes 589824 | tf_op jit(solution)/shard_map/tile | solution.py:258
  35.7 2.0 %copy.14.sin_ref = f32[512,256]{1,0:T(8,128)} copy(f32[512,256]{0,1:T(8,128)} %bitcast.13) | data formatting | bytes 1048576 | tf_op jit(solution)/shard_map/tile | solution.py:258
  37.7 0.9 %tile.8 = f32[512,8,32]{0,2,1:T(8,128)} broadcast(f32[512,32]{0,1:T(8,128)S(1)} %get-tuple-element.20), dimensions={0,2} | broadcast | bytes 589824 | tf_op jit(solution)/shard_map/tile | solution.py:258
  38.6 2.0 %copy.13.cos_ref = f32[512,256]{1,0:T(8,128)} copy(f32[512,256]{0,1:T(8,128)} %bitcast.14) | data formatting | bytes 1048576 | tf_op jit(solution)/shard_map/tile | solution.py:258
  40.7 5.3 %collective-permute-done.lo_ref = bf16[128,2048]{1,0:T(8,128)(2,1)} collective-permute-done((bf16[128,2048]{1,0:T(8,128)(2,1)}, bf16[128,2048]{1,0:T(8,128)(2,1)}, u32[]{:S(2)}, u32[]{:S(2)}) %collective-permute-start) | collective-permute-done | bytes 524320 | tf_op jit(solution)/shard_map/ppermute | solution.py:230
  46.1 1.0 %copy-done.4 = f32[512,256]{1,0:T(8,128)S(1)} copy-done((f32[512,256]{1,0:T(8,128)S(1)}, f32[512,256]{1,0:T(8,128)}, u32[]{:S(2)}) %copy-start.4) | copy-done | bytes 524312
  47.1 1.0 %copy-done.5 = f32[512,256]{1,0:T(8,128)S(1)} copy-done((f32[512,256]{1,0:T(8,128)S(1)}, f32[512,256]{1,0:T(8,128)}, u32[]{:S(2)}) %copy-start.5) | copy-done | bytes 524312
  48.2 2.2 %copy-done.9 = bf16[2048,1024]{1,0:T(8,128)(2,1)S(1)} copy-done((bf16[2048,1024]{1,0:T(8,128)(2,1)S(1)}, bf16[2048,1024]{1,0:T(8,128)(2,1)}, u32[]{:S(2)}) %copy-start.9) | copy-done | bytes 4194328
  50.3 8.3 %local.1 = (bf16[256,1024]{1,0:T(8,128)(2,1)S(1)}, f32[256,1024]{1,0:T(8,128)S(1)}, f32[256,1024]{1,0:T(8,128)S(1)}, f32[256,1024]{1,0:T(8,128)S(1)}) custom-call(s32[2]{0:T(128)S(1)} %add_convert_fusion.flags_ref, f32[16]{0:T(128)S(1)} %copy-done.14, f32[8,2048]{1,0:T(8,128)S(1)} %copy-done.12, bf16[128,2048]{1,0:T(8,128)(2,1)} %collective-permute-done.lo_ref, ...), custom_call_target="tpu_custom_call" | custom-call | flops 6000000000 | tf_op jit(solution)/shard_map/local/pallas_call | solution.py:262
  58.7 1.0 %copy-done.15 = f32[256,1024]{1,0:T(8,128)} copy-done((f32[256,1024]{1,0:T(8,128)}, f32[256,1024]{1,0:T(8,128)S(1)}, u32[]{:S(2)}) %copy-start.15) | copy-done | bytes 1048600
  59.7 1.0 %copy-done.17 = f32[256,1024]{1,0:T(8,128)} copy-done((f32[256,1024]{1,0:T(8,128)}, f32[256,1024]{1,0:T(8,128)S(1)}, u32[]{:S(2)}) %copy-start.17) | copy-done | bytes 1048600
  60.7 1.0 %copy-done.19 = f32[256,1024]{1,0:T(8,128)} copy-done((f32[256,1024]{1,0:T(8,128)}, f32[256,1024]{1,0:T(8,128)S(1)}, u32[]{:S(2)}) %copy-start.19) | copy-done | bytes 1048600
  61.6 0.8 %copy-done.21 = bf16[256,1024]{1,0:T(8,128)(2,1)} copy-done((bf16[256,1024]{1,0:T(8,128)(2,1)}, bf16[256,1024]{1,0:T(8,128)(2,1)S(1)}, u32[]{:S(2)}) %copy-start.21) | copy-done | bytes 524312
  62.5 2.2 %copy-done.10 = bf16[1024,2048]{1,0:T(8,128)(2,1)S(1)} copy-done((bf16[1024,2048]{1,0:T(8,128)(2,1)S(1)}, bf16[1024,2048]{1,0:T(8,128)(2,1)}, u32[]{:S(2)}) %copy-start.10) | copy-done | bytes 4194328
  64.6 1.2 %copy-done.16 = f32[256,1024]{1,0:T(8,128)S(1)} copy-done((f32[256,1024]{1,0:T(8,128)S(1)}, f32[256,1024]{1,0:T(8,128)}, u32[]{:S(2)}) %copy-start.16) | copy-done | bytes 1048600
  65.9 1.2 %copy-done.18 = f32[256,1024]{1,0:T(8,128)S(1)} copy-done((f32[256,1024]{1,0:T(8,128)S(1)}, f32[256,1024]{1,0:T(8,128)}, u32[]{:S(2)}) %copy-start.18) | copy-done | bytes 1048600
  67.1 1.2 %copy-done.20 = f32[256,1024]{1,0:T(8,128)S(1)} copy-done((f32[256,1024]{1,0:T(8,128)S(1)}, f32[256,1024]{1,0:T(8,128)}, u32[]{:S(2)}) %copy-start.20) | copy-done | bytes 1048600
  68.3 1.0 %copy-done.22 = bf16[256,1024]{1,0:T(8,128)(2,1)S(1)} copy-done((bf16[256,1024]{1,0:T(8,128)(2,1)S(1)}, bf16[256,1024]{1,0:T(8,128)(2,1)}, u32[]{:S(2)}) %copy-start.22) | copy-done | bytes 524312
  69.4 10.6 %final.1 = bf16[256,2048]{1,0:T(8,128)(2,1)} custom-call(bf16[256,1024]{1,0:T(8,128)(2,1)S(1)} %copy-done.22, bf16[1024,512]{1,0:T(8,128)(2,1)} %bitcast.7.kv_ref, f32[256,1024]{1,0:T(8,128)S(1)} %copy-done.16, f32[256,1024]{1,0:T(8,128)S(1)} %copy-done.18, f32[256,1024]{1,0:T(8,128)S(1)} %copy-done.20, bf16[1024,2048]{1,0:T(8,128)(2,1)S(1)} %copy-done.10, ...), custom_call_target="tpu_custom_call" | custom-call | flops 6000000000 | tf_op jit(solution)/shard_map/final/pallas_call | solution.py:271
  (38 shorter events, 0.5 us)
Async XLA Ops:
  0.0 24.9 %copy-start.1 = (bf16[2048,256]{1,0:T(8,128)(2,1)S(1)}, bf16[2048,256]{1,0:T(8,128)(2,1)}, u32[]{:S(2)}) copy-start(bf16[2048,256]{1,0:T(8,128)(2,1)} %wv_ref.3) | copy-start | bytes 3145732
  0.0 25.0 %copy-start = (bf16[2048,256]{1,0:T(8,128)(2,1)S(1)}, bf16[2048,256]{1,0:T(8,128)(2,1)}, u32[]{:S(2)}) copy-start(bf16[2048,256]{1,0:T(8,128)(2,1)} %wk_ref.3) | copy-start | bytes 3145732
  0.9 1.0 %copy-start.6 = (bf16[3,128,512]{2,1,0:T(8,128)(2,1)S(1)}, bf16[3,128,512]{2,1,0:T(8,128)(2,1)}, u32[]{:S(2)}) copy-start(bf16[3,128,512]{2,1,0:T(8,128)(2,1)} %mod_ref.1) | copy-start | bytes 1179652
  2.9 22.1 %all-to-all-start = ((bf16[64,8,384]{2,1,0:T(8,128)(2,1)}), bf16[64,8,384]{2,1,0:T(8,128)(2,1)S(1)}, u32[]{:S(2)}, u32[]{:S(2)}) async-start(bf16[64,8,384]{2,1,0:T(8,128)(2,1)} %partials.1), calls=%async_computation | async-start | bytes 786432 | tf_op jit(solution)/shard_map/all_to_all | solution.py:241
  16.3 24.5 %collective-permute-start.1 = (bf16[128,2048]{1,0:T(8,128)(2,1)}, bf16[128,2048]{1,0:T(8,128)(2,1)}, u32[]{:S(2)}, u32[]{:S(2)}) collective-permute-start(bf16[128,2048]{1,0:T(8,128)(2,1)} %get-tuple-element.17), channel_id=1, source_target_pairs={{2,0},{4,2},{6,4},{8,6},{10,8},{12,10},{14,12},{16,14},{18,16},{20... | collective-permute-start | bytes 1572872 | tf_op jit(solution)/shard_map/ppermute | solution.py:231
  23.0 23.1 %collective-permute-start = (bf16[128,2048]{1,0:T(8,128)(2,1)}, bf16[128,2048]{1,0:T(8,128)(2,1)}, u32[]{:S(2)}, u32[]{:S(2)}) collective-permute-start(bf16[128,2048]{1,0:T(8,128)(2,1)} %get-tuple-element.18), channel_id=1, source_target_pairs={{0,2},{2,4},{4,6},{6,8},{8,10},{10,12},{12,14},{14,16},{16,18},{18... | collective-permute-start | bytes 1572872 | tf_op jit(solution)/shard_map/ppermute | solution.py:230
  25.0 1.0 %copy-start.7 = (bf16[64,2048]{1,0:T(8,128)(2,1)S(1)}, bf16[64,2048]{1,0:T(8,128)(2,1)}, u32[]{:S(2)}) copy-start(bf16[64,2048]{1,0:T(8,128)(2,1)} %ctx_ref.1) | copy-start | bytes 786436
  25.9 0.7 copy-start.8
  26.6 19.4 %copy-start.2 = (bf16[256,2048]{1,0:T(8,128)(2,1)S(1)}, bf16[256,2048]{1,0:T(8,128)(2,1)}, u32[]{:S(2)}) copy-start(bf16[256,2048]{1,0:T(8,128)(2,1)} %lat_ref.1) | copy-start | bytes 3145732
  26.6 19.4 %copy-start.14 = (f32[16]{0:T(128)S(1)}, f32[16]{0:T(128)}, u32[]{:S(2)}) copy-start(f32[16]{0:T(128)} %sink_ref.1) | copy-start | bytes 196
  27.3 1.0 %copy-start.3 = (bf16[16,64,512]{2,1,0:T(8,128)(2,1)}, bf16[16,64,512]{2,1,0:T(8,128)(2,1)S(1)}, u32[]{:S(2)}) copy-start(bf16[16,64,512]{2,1,0:T(8,128)(2,1)S(1)} %get-tuple-element.13) | copy-start | bytes 3145732
  28.2 0.6 copy-start.11
  28.9 17.2 %copy-start.12 = (f32[8,2048]{1,0:T(8,128)S(1)}, f32[8,2048]{1,0:T(8,128)}, u32[]{:S(2)}) copy-start(f32[8,2048]{1,0:T(8,128)} %copy-done.11) | copy-start | bytes 196612
  28.9 33.6 %all-to-all-start.1 = ((bf16[16,64,512]{2,1,0:T(8,128)(2,1)}), bf16[16,64,512]{2,1,0:T(8,128)(2,1)}, u32[]{:S(2)}, u32[]{:S(2)}) async-start(bf16[16,64,512]{2,1,0:T(8,128)(2,1)} %copy-done.3), calls=%async_computation.1 | async-start | bytes 2097152 | tf_op jit(solution)/shard_map/all_to_all | solution.py:251
  46.1 1.0 %copy-start.4 = (f32[512,256]{1,0:T(8,128)S(1)}, f32[512,256]{1,0:T(8,128)}, u32[]{:S(2)}) copy-start(f32[512,256]{1,0:T(8,128)} %copy.14.sin_ref) | copy-start | bytes 1572868
  47.1 1.0 %copy-start.5 = (f32[512,256]{1,0:T(8,128)S(1)}, f32[512,256]{1,0:T(8,128)}, u32[]{:S(2)}) copy-start(f32[512,256]{1,0:T(8,128)} %copy.13.cos_ref) | copy-start | bytes 1572868
  48.2 2.2 %copy-start.9 = (bf16[2048,1024]{1,0:T(8,128)(2,1)S(1)}, bf16[2048,1024]{1,0:T(8,128)(2,1)}, u32[]{:S(2)}) copy-start(bf16[2048,1024]{1,0:T(8,128)(2,1)} %wq_ref.1) | copy-start | bytes 12582916
  50.3 12.1 %copy-start.13 = (f32[2048]{0:T(1024)S(1)}, f32[2048]{0:T(1024)}, u32[]{:S(2)}) copy-start(f32[2048]{0:T(1024)} %param.18) | copy-start | bytes 24580
  58.7 1.0 %copy-start.15 = (f32[256,1024]{1,0:T(8,128)}, f32[256,1024]{1,0:T(8,128)S(1)}, u32[]{:S(2)}) copy-start(f32[256,1024]{1,0:T(8,128)S(1)} %get-tuple-element.14.o_ref) | copy-start | bytes 3145732
  59.7 1.0 %copy-start.17 = (f32[256,1024]{1,0:T(8,128)}, f32[256,1024]{1,0:T(8,128)S(1)}, u32[]{:S(2)}) copy-start(f32[256,1024]{1,0:T(8,128)S(1)} %get-tuple-element.15.l_ref) | copy-start | bytes 3145732
  60.6 1.0 %copy-start.19 = (f32[256,1024]{1,0:T(8,128)}, f32[256,1024]{1,0:T(8,128)S(1)}, u32[]{:S(2)}) copy-start(f32[256,1024]{1,0:T(8,128)S(1)} %get-tuple-element.16.m_ref) | copy-start | bytes 3145732
  61.6 0.8 %copy-start.21 = (bf16[256,1024]{1,0:T(8,128)(2,1)}, bf16[256,1024]{1,0:T(8,128)(2,1)S(1)}, u32[]{:S(2)}) copy-start(bf16[256,1024]{1,0:T(8,128)(2,1)S(1)} %get-tuple-element.12.q_ref) | copy-start | bytes 1572868
  62.4 2.2 %copy-start.10 = (bf16[1024,2048]{1,0:T(8,128)(2,1)S(1)}, bf16[1024,2048]{1,0:T(8,128)(2,1)}, u32[]{:S(2)}) copy-start(bf16[1024,2048]{1,0:T(8,128)(2,1)} %wo_ref.1) | copy-start | bytes 12582916
  64.6 1.2 %copy-start.16 = (f32[256,1024]{1,0:T(8,128)S(1)}, f32[256,1024]{1,0:T(8,128)}, u32[]{:S(2)}) copy-start(f32[256,1024]{1,0:T(8,128)} %copy-done.15) | copy-start | bytes 3145732
  65.9 1.2 %copy-start.18 = (f32[256,1024]{1,0:T(8,128)S(1)}, f32[256,1024]{1,0:T(8,128)}, u32[]{:S(2)}) copy-start(f32[256,1024]{1,0:T(8,128)} %copy-done.17) | copy-start | bytes 3145732
  67.1 1.2 %copy-start.20 = (f32[256,1024]{1,0:T(8,128)S(1)}, f32[256,1024]{1,0:T(8,128)}, u32[]{:S(2)}) copy-start(f32[256,1024]{1,0:T(8,128)} %copy-done.19) | copy-start | bytes 3145732
  68.3 1.0 %copy-start.22 = (bf16[256,1024]{1,0:T(8,128)(2,1)S(1)}, bf16[256,1024]{1,0:T(8,128)(2,1)}, u32[]{:S(2)}) copy-start(bf16[256,1024]{1,0:T(8,128)(2,1)} %copy-done.21) | copy-start | bytes 1572868

commit v2 on v1

v2 whole, which is shorter than its diff:
```python
import jax
import numpy as np
import jax.numpy as jnp
from jax import lax
from jax.experimental import pallas as pl
from jax.experimental.pallas import tpu as pltpu
from jax.sharding import PartitionSpec as P

HEAD_DIM = 64
WINDOW = 128
GRID_W = 64
EPSILON = 1e-06
NEG_BIG = -1e30
LOG2E = 1.4426950408889634
FACTOR = HEAD_DIM**-0.5 * LOG2E
F32 = jnp.float32
BF16 = jnp.bfloat16
VM = pltpu.MemorySpace.VMEM
HB = pltpu.MemorySpace.HBM
SM = pltpu.MemorySpace.SMEM


def spec(kinds):
    return [pl.BlockSpec(memory_space={"v": VM, "h": HB, "s": SM}[k]) for k in kinds]


def place_of():
    return lax.axis_index("sp") * lax.axis_size("tp") + lax.axis_index("tp")


def dot(a, b):
    return jnp.dot(a, b, preferred_element_type=F32)


def dot_nt(a, b):
    return lax.dot_general(a, b, (((1,), (1,)), ((), ())), preferred_element_type=F32)


def iota(shape, dim):
    return lax.broadcasted_iota(jnp.int32, shape, dim)


def pick(h, cols, transposed):
    if transposed:
        out, inp = iota((cols, 256), 0), iota((cols, 256), 1)
    else:
        out, inp = iota((256, cols), 1), iota((256, cols), 0)
    return (inp == h * HEAD_DIM + (out & (HEAD_DIM - 1))).astype(F32).astype(BF16)


def swap_matrix():
    k, c = iota((256, 256), 0), iota((256, 256), 1)
    low = (c & 63) < 32
    neg = jnp.where(low & (k == c + 32), -1.0, 0.0)
    pos = jnp.where((~low) & (k == c - 32), 1.0, 0.0)
    return (neg + pos).astype(BF16)


def normed(x, mult, shift):
    x = x.astype(F32)
    rs = lax.rsqrt(jnp.mean(x * x, axis=-1, keepdims=True) + EPSILON)
    return (x * rs * mult + shift).astype(BF16)


def entry_kernel(
    cond_ref, cctx_ref, mod_ref, lat_ref, ctx_ref, gain_ref,
    parts_ref, one_ref, two_ref, ng_ref,
    cond_v, cctx_v, mod_v, lat_v, ctx_v, gain_v, block_v, sems,
):
    sp = lax.axis_index("sp")
    odd = place_of() & 1
    copy = pltpu.make_async_copy
    ins = [
        copy(src, dst, sems.at[i])
        for i, (src, dst) in enumerate(
            (
                (cond_ref, cond_v),
                (cctx_ref, cctx_v),
                (mod_ref, mod_v),
                (lat_ref, lat_v),
                (ctx_ref, ctx_v),
                (gain_ref, gain_v),
            )
        )
    ]
    for c in ins:
        c.start()
    ins[0].wait()
    ins[1].wait()
    here = iota((16, 128), 0) == sp
    rows = []
    for ref in (cond_v, cctx_v):
        x = jnp.sum(jnp.where(here, ref[...].astype(F32), 0.0), axis=0, keepdims=True)
        rows.append(x / (1.0 + jnp.exp(-x)))
    v = jnp.concatenate(rows + [jnp.zeros((6, 128), F32)], axis=0).astype(BF16)
    ins[2].wait()
    parts = [dot(v, mod_v[i]) for i in range(3)]
    five = (parts[0][0:1], parts[0][1:2], parts[1][0:1], parts[1][1:2], parts[2][0:1])
    zero = jnp.zeros((1, 128), F32)
    rows = []
    for j in range(4):
        cut = [x[:, j * 128 : (j + 1) * 128] for x in five]
        rows.append(jnp.concatenate(cut[:3], axis=1))
        rows.append(jnp.concatenate(cut[3:] + [zero], axis=1))
    block = jnp.concatenate(rows, axis=0).astype(BF16)
    for i in range(block_v.shape[0]):
        block_v[i] = block
    outs = [copy(block_v, parts_ref, sems.at[6])]
    outs[0].start()
    ins[3].wait()
    outs.append(copy(lat_v.at[pl.ds((1 - odd) * 128, 128)], one_ref, sems.at[7]))
    outs.append(copy(lat_v.at[pl.ds(odd * 128, 128)], two_ref, sems.at[8]))
    outs[1].start()
    outs[2].start()
    ins[4].wait()
    ins[5].wait()
    x = ctx_v[...].astype(F32)
    gain = gain_v[...]
    rs = lax.rsqrt(jnp.mean(x * x, axis=-1, keepdims=True) + EPSILON)
    ng_ref[0:64, :] = x * rs * gain
    ng_ref[64:72, :] = jnp.broadcast_to(gain, (8, 2048))
    for c in outs:
        c.wait()


def context_kernel(recv_ref, ng_ref, wk_ref, wv_ref, send_ref, vec_ref, kv_v, vec_v, sems):
    sums = []
    for t in range(4):
        acc = recv_ref[t].astype(F32)
        for s in range(1, 16):
            acc = acc + recv_ref[s * 4 + t].astype(F32)
        sums.append(acc)

    def vector(v):
        cuts = []
        for t in range(4):
            for j in range(4):
                r, c = 2 * j + v // 3, (v % 3) * 128
                cuts.append(sums[t][r : r + 1, c : c + 128])
        return jnp.concatenate(cuts, axis=1)

    hidden = (ng_ref[0:64, :] * (1.0 + vector(3)) + vector(1)).astype(BF16)
    kv_v[:, 0:256] = dot(hidden, wk_ref[...]).astype(BF16)
    kv_v[:, 256:512] = dot(hidden, wv_ref[...]).astype(BF16)
    copy = pltpu.make_async_copy
    outs = [copy(kv_v, send_ref.at[i], sems.at[i]) for i in range(16)]
    for c in outs:
        c.start()
    vec_v[...] = jnp.zeros((8, 2048), F32)
    vec_v[0:1, :] = ng_ref[64:65, :] * (1.0 + vector(2))
    vec_v[1:2, :] = vector(0)
    vec_v[2:3, :] = vector(4)
    outs.append(copy(vec_v, vec_ref, sems.at[16]))
    outs[16].start()
    for c in outs:
        c.wait()


def softmax_parts(s_list, floor, va, shape):
    m = s_list[0]
    for s in s_list[1:]:
        m = jnp.maximum(m, s)
    m = jnp.max(m, axis=-1, keepdims=True)
    if floor is not None:
        m = jnp.maximum(m, floor)
    p = [jnp.exp2(s - m).astype(BF16) for s in s_list]
    p = p[0] if len(p) == 1 else jnp.concatenate(p, axis=1)
    o = dot(p, va)
    return o[:, 0:128], o[:, 128:256], jnp.broadcast_to(m, shape)


def masked_heads(q, lane):
    return [jnp.where(lane == g, q, jnp.zeros_like(q)) for g in range(4)]


def rotated(x, cos, sin, swap):
    return (x.astype(F32) * cos + dot(x, swap) * sin).astype(BF16)


def own_kernel(
    sink_ref, vec_ref, lat_ref, wq_ref, wk_ref, wv_ref, rowc_ref, rows_ref, colc_ref, cols_ref,
    q_ref, rot_ref, o_ref, l_ref, m_ref,
    vec_v, lat_v, wq_v, hid_v, q_v, sems,
):
    copy = pltpu.make_async_copy
    ins = [copy(vec_ref, vec_v, sems.at[0]), copy(lat_ref, lat_v, sems.at[1])]
    for h in range(4):
        cols = pl.ds(h * 256, 256)
        ins.append(copy(wq_ref.at[:, cols], wq_v.at[h], sems.at[2 + h]))
    for c in ins:
        c.start()
    swap = swap_matrix()
    cos = jnp.concatenate([colc_ref[...] + rowc_ref[r : r + 1, :] for r in range(2, 6)], axis=0)
    sin = jnp.concatenate([cols_ref[...] + rows_ref[r : r + 1, :] for r in range(2, 6)], axis=0)
    ins[0].wait()
    ins[1].wait()
    hid_v[...] = normed(lat_v[...], vec_v[0:1, :], vec_v[1:2, :])
    keys = rotated(dot(hid_v[...], wk_ref[...]).astype(BF16), cos, sin, swap)
    vals = dot(hid_v[...], wv_ref[...]).astype(BF16)
    lane = iota((128, 256), 1) // HEAD_DIM
    first = iota((128, 128), 1) < HEAD_DIM
    row, col = iota((128, 128), 0), iota((128, 128), 1)
    bias = (jnp.where(col <= row, 0.0, NEG_BIG), jnp.where(col >= row, 0.0, NEG_BIG))
    ones = jnp.ones((256, 128), BF16)
    outs = []
    for h in range(4):
        ins[2 + h].wait()
        at = h * 256
        query = dot(hid_v[...], wq_v[h]).astype(BF16)
        q_v[:, at : at + 256] = query
        cols = pl.ds(at, 256)
        outs.append(copy(q_v.at[:, cols], q_ref.at[:, cols], sems.at[6 + h]))
        outs[h].start()
        turned = rotated(query, cos, sin, swap)
        rot_ref[:, at : at + 256] = turned
        kt = dot_nt(pick(h, 256, True), keys).astype(BF16)
        va = jnp.concatenate([dot(vals, pick(h, 128, False)).astype(BF16), ones], axis=1)
        for b in range(2):
            rows = slice(b * 128, b * 128 + 128)
            s = dot(jnp.concatenate(masked_heads(turned[rows], lane), axis=0), kt) * FACTOR
            got = []
            for g in range(4):
                near = s[g * 128 : (g + 1) * 128, b * 128 : b * 128 + 128]
                far = s[g * 128 : (g + 1) * 128, (1 - b) * 128 : (1 - b) * 128 + 128] + bias[b]
                both = [near, far] if b == 0 else [far, near]
                sink = sink_ref[h * 4 + g] * LOG2E
                o, l, m = softmax_parts(both, sink, va, (128, 128))
                got.append((o, l + jnp.exp2(sink - m), m))
            for pair in range(2):
                to = slice(at + pair * 128, at + pair * 128 + 128)
                for ref, x, y in zip((o_ref, l_ref, m_ref), got[2 * pair], got[2 * pair + 1]):
                    ref[rows, to] = jnp.where(first, x, y)
    for c in outs:
        c.wait()


def halo_kernel(
    vec_ref, one_ref, two_ref, wk_ref, wv_ref, rowc_ref, rows_ref, colc_ref, cols_ref,
    rot_ref, o_ref, l_ref, m_ref,
    oo_ref, ll_ref, mm_ref,
    vec_v, raw_v, hid_v, o_v, l_v, m_v, sems,
):
    place = place_of()
    odd = place & 1
    copy = pltpu.make_async_copy
    ins = [
        copy(vec_ref, vec_v, sems.at[0]),
        copy(one_ref, raw_v.at[1 - odd], sems.at[1]),
        copy(two_ref, raw_v.at[odd], sems.at[2]),
    ]
    for c in ins:
        c.start()
    swap = swap_matrix()
    pick_rows = (0, 1, 6, 7)
    cos = jnp.concatenate([colc_ref[...] + rowc_ref[r : r + 1, :] for r in pick_rows], axis=0)
    sin = jnp.concatenate([cols_ref[...] + rows_ref[r : r + 1, :] for r in pick_rows], axis=0)
    for c in ins:
        c.wait()
    for b in range(2):
        hid_v[b * 128 : b * 128 + 128, :] = normed(raw_v[b], vec_v[0:1, :], vec_v[1:2, :])
    keys = rotated(dot(hid_v[...], wk_ref[...]).astype(BF16), cos, sin, swap)
    vals = dot(hid_v[...], wv_ref[...]).astype(BF16)
    lane = iota((128, 256), 1) // HEAD_DIM
    first = iota((128, 128), 1) < HEAD_DIM
    row, col = iota((128, 128), 0), iota((128, 128), 1)
    last = lax.axis_size("sp") * lax.axis_size("tp") - 1
    bias = (
        jnp.where((col >= row) & (place > 0), 0.0, NEG_BIG),
        jnp.where((col <= row) & (place < last), 0.0, NEG_BIG),
    )
    ones = jnp.ones((256, 128), BF16)
    outs = []
    for h in range(4):
        at = h * 256
        kt = dot_nt(pick(h, 256, True), keys).astype(BF16)
        va = jnp.concatenate([dot(vals, pick(h, 128, False)).astype(BF16), ones], axis=1)
        for b in range(2):
            rows = slice(b * 128, b * 128 + 128)
            turned = rot_ref[rows, at : at + 256]
            s = dot(jnp.concatenate(masked_heads(turned, lane), axis=0), kt[:, rows]) * FACTOR
            got = []
            for g in range(4):
                part = s[g * 128 : (g + 1) * 128] + bias[b]
                got.append(softmax_parts([part], None, va[rows], (128, 128)))
            for pair in range(2):
                to = slice(at + pair * 128, at + pair * 128 + 128)
                o, l, m = (
                    jnp.where(first, x, y) for x, y in zip(got[2 * pair], got[2 * pair + 1])
                )
                old = m_ref[rows, to]
                top = jnp.maximum(old, m)
                wo, wn = jnp.exp2(old - top), jnp.exp2(m - top)
                o_v[rows, to] = o_ref[rows, to] * wo + o * wn
                l_v[rows, to] = l_ref[rows, to] * wo + l * wn
                m_v[rows, to] = top
        cols = pl.ds(at, 256)
        for i, (src, dst) in enumerate(((o_v, oo_ref), (l_v, ll_ref), (m_v, mm_ref))):
            outs.append(copy(src.at[:, cols], dst.at[:, cols], sems.at[3 + 3 * h + i]))
            outs[-1].start()
    for c in outs:
        c.wait()


def final_kernel(
    q_ref, kv_ref, o_ref, l_ref, m_ref, wo_ref, lat_ref, vec_ref, gain_ref, out_ref,
    q_v, kv_v, o_v, l_v, m_v, wo_v, lat_v, vec_v, gain_v, mix_v, out_v, sems,
):
    copy = pltpu.make_async_copy
    pairs = (
        (kv_ref, kv_v), (q_ref, q_v), (o_ref, o_v), (l_ref, l_v), (m_ref, m_v),
        (wo_ref, wo_v), (lat_ref, lat_v), (vec_ref, vec_v), (gain_ref, gain_v),
    )
    ins = [copy(src, dst, sems.at[i]) for i, (src, dst) in enumerate(pairs)]
    for c in ins:
        c.start()
    lane = iota((256, 256), 1) // HEAD_DIM
    first = iota((256, 128), 1) < HEAD_DIM
    ones = jnp.ones((1024, 128), BF16)
    ins[0].wait()
    ins[1].wait()
    keys = kv_v[:, 0:256]
    vals = kv_v[:, 256:512]
    for h in range(4):
        kt = dot_nt(pick(h, 256, True), keys).astype(BF16)
        va = jnp.concatenate([dot(vals, pick(h, 128, False)).astype(BF16), ones], axis=1)
        q = q_v[:, h * 256 : (h + 1) * 256]
        for pair in range(2):
            got = []
            for g in (2 * pair, 2 * pair + 1):
                s = dot(jnp.where(lane == g, q, jnp.zeros_like(q)), kt) * FACTOR
                got.append(softmax_parts([s], None, va, (256, 128)))
            if h == 0 and pair == 0:
                for c in ins[2:5]:
                    c.wait()
            to = slice(h * 256 + pair * 128, h * 256 + pair * 128 + 128)
            oc, lc, mc = (jnp.where(first, x, y) for x, y in zip(got[0], got[1]))
            ml = m_v[:, to]
            top = jnp.maximum(ml, mc)
            wl, wc = jnp.exp2(ml - top), jnp.exp2(mc - top)
            num = wl * o_v[:, to] + wc * oc
            den = wl * l_v[:, to] + wc * lc
            mix_v[:, to] = (num / den).astype(BF16)
    for c in ins[5:]:
        c.wait()
    scale = vec_v[2:3, :] * gain_v[...]
    outs = []
    for b in range(2):
        rows = slice(b * 128, b * 128 + 128)
        projected = dot(mix_v[rows, :], wo_v[...])
        rs = lax.rsqrt(jnp.mean(projected * projected, axis=-1, keepdims=True) + EPSILON)
        out_v[rows, :] = (lat_v[rows, :].astype(F32) + projected * rs * scale).astype(BF16)
        there = pl.ds(b * 128, 128)
        outs.append(copy(out_v.at[there], out_ref.at[there], sems.at[9 + b]))
        outs[b].start()
    for c in outs:
        c.wait()


def call(kernel, name, ins, outs, scratch, copies, args, flops, limit):
    return pl.pallas_call(
        kernel,
        out_shape=[jax.ShapeDtypeStruct(s, d) for _, s, d in outs],
        in_specs=spec(ins),
        out_specs=spec([k for k, _, _ in outs]),
        scratch_shapes=[pltpu.VMEM(s, d) for s, d in scratch]
        + [pltpu.SemaphoreType.DMA((copies,))],
        compiler_params=pltpu.CompilerParams(vmem_limit_bytes=limit * 1024 * 1024),
        cost_estimate=pl.CostEstimate(flops=flops, bytes_accessed=0, transcendentals=0),
        name=name,
    )(*args)


def shards(
    latent, cond, ctx_rows, ctx_cond, mod_weight, norm_gain, out_gain,
    w_query, w_key, w_value, w_out, sink,
):
    sp_size = lax.axis_size("sp")
    count = sp_size * lax.axis_size("tp")
    both = ("sp", "tp")
    rows, width = latent.shape
    half = (WINDOW, width)
    wide = (rows, 1024)
    rest = (8, width)
    line = (1, width)
    square = (16, 128)

    parts, one, two, ng = call(
        entry_kernel,
        "entry",
        "hhhhhh",
        [
            ("h", (count, 8, 384), BF16),
            ("h", half, BF16),
            ("h", half, BF16),
            ("v", (72, width), F32),
        ],
        [
            (square, BF16),
            (square, BF16),
            (mod_weight.shape, BF16),
            (latent.shape, BF16),
            (ctx_rows.shape, BF16),
            (line, F32),
            ((count, 8, 384), BF16),
        ],
        9,
        (
            cond.reshape(square),
            ctx_cond.reshape(square),
            mod_weight,
            latent,
            ctx_rows,
            norm_gain.reshape(line),
        ),
        10**6,
        8,
    )
    recv = lax.all_to_all(parts, both, 0, 0, tiled=True)
    swap_one = [(i, i ^ 1) for i in range(count)]
    swap_two = [(i, i + 1 if i % 2 else i - 1) for i in range(1, count - 1)]
    one = lax.ppermute(one, both, swap_one)
    two = lax.ppermute(two, both, swap_two)
    send, vecs = call(
        context_kernel,
        "context",
        "vvvv",
        [("h", (sp_size, 64, 512), BF16), ("h", rest, F32)],
        [((64, 512), BF16), (rest, F32)],
        17,
        (recv, ng, w_key, w_value),
        10**6,
        6,
    )
    kv_ctx = lax.all_to_all(send, "sp", 0, 0, tiled=True).reshape(sp_size * 64, 512)

    lanes = np.arange(256) % 32
    freq = 10000.0 ** (-(lanes % 16) / 16.0)
    by_row = (lanes < 16).astype(np.float32)
    angle = np.arange(GRID_W)[:, None] * freq
    colc = jnp.asarray(np.cos(angle) * (1.0 - by_row), F32)
    cols = jnp.asarray(np.sin(angle) * (1.0 - by_row), F32)
    grid_row = place_of() * (rows // GRID_W) - WINDOW // GRID_W + jnp.arange(8, dtype=jnp.int32)
    angle = grid_row.astype(F32)[:, None] * jnp.asarray(freq, F32)[None, :]
    tables = (jnp.cos(angle) * by_row, jnp.sin(angle) * by_row, colc, cols)

    query, turned, o, l, m = call(
        own_kernel,
        "own",
        "shhhvvvvvv",
        [("h", wide, BF16), ("v", wide, BF16), ("v", wide, F32), ("v", wide, F32), ("v", wide, F32)],
        [(rest, F32), (latent.shape, BF16), ((4, width, 256), BF16), (latent.shape, BF16), (wide, BF16)],
        10,
        (sink, vecs, latent, w_query, w_key, w_value, *tables),
        10**10,
        16,
    )
    o, l, m = call(
        halo_kernel,
        "halo",
        "hhhvvvvvvvvvv",
        [("h", wide, F32)] * 3,
        [(rest, F32), ((2, WINDOW, width), BF16), (latent.shape, BF16), (wide, F32), (wide, F32), (wide, F32)],
        15,
        (vecs, one, two, w_key, w_value, *tables, turned, o, l, m),
        10**9,
        12,
    )
    (updated,) = call(
        final_kernel,
        "final",
        "hhhhhhhhh",
        [("h", latent.shape, BF16)],
        [
            (wide, BF16),
            (kv_ctx.shape, BF16),
            (wide, F32),
            (wide, F32),
            (wide, F32),
            (w_out.shape, BF16),
            (latent.shape, BF16),
            (rest, F32),
            (line, F32),
            (wide, BF16),
            (latent.shape, BF16),
        ],
        11,
        (query, kv_ctx, o, l, m, w_out, latent, vecs, out_gain.reshape(line)),
        10**10,
        28,
    )
    return updated


def solution(mesh):
    placed = (
        P(("dp", "sp", "tp"), None),
        P("dp"),
        P(("dp", "sp"), None),
        P(),
        P(None, "sp", "tp"),
        P(),
        P(),
        P(),
        P(),
        P(),
        P(),
        P(),
    )
    return jax.shard_map(
        shards, mesh=mesh, in_specs=placed, out_specs=P(("dp", "sp", "tp"), None), check_vma=False
    )
```

time: 80.9 us -> 89.7 us (1.11)
  the two profiles are of different devices: /device:TPU:32 before, /device:TPU:0 now
where the time goes in v2:
time: 89.7 us; the launch traced here: 88.7 us
  Pallas kernels  31.7 us (35%)
  local copies, waits for them, and re-layouts  27.3 us (30%)
  starting transfers between devices  19.2 us (21%)
  waiting for transfers between devices  9.41 us (10%)
    pallas_call x5, Pallas kernels, call(): pl.pallas_call(kernel, out_shape=[jax.ShapeDtypeStruct(s, d) for _, s, d...  31.7 us
    unnamed x62, local copies, waits for them, and re-layouts  27.3 us
    all_to_all x1, starting transfers between devices, shards(): recv = lax.all_to_all(parts, both, 0, 0, tiled=True)  11.5 us
    all_to_all x1, waiting for transfers between devices, shards(): recv = lax.all_to_all(parts, both, 0, 0, tiled=True)  9.4 us
    all_to_all x1, starting transfers between devices, shards(): lax.all_to_all(send, 'sp', 0, 0, tiled=True).reshape(sp_size * 64, 512)  4.53 us
  transfers between devices with their start and end apart: 4, of which 1 were waited for; matrix products, arithmetic and copies ran while one was open for 1% of the time, Pallas kernels for 21%

profile of v2, /device:TPU:0, one launch (start us, length us, event | category | flops | bytes accessed | tf_op | source)
XLA Modules:
  0.0 88.7 jit_solution(18254963586358840868)
XLA Ops:
  0.0 1.4 %copy-done.4 = bf16[256,2048]{1,0:T(8,128)(2,1)S(1)} copy-done((bf16[256,2048]{1,0:T(8,128)(2,1)S(1)}, bf16[256,2048]{1,0:T(8,128)(2,1)}, u32[]{:S(2)}) %copy-start.4) | copy-done | bytes 1048600
  1.4 1.0 %copy-done.9 = bf16[3,128,512]{2,1,0:T(8,128)(2,1)S(1)} copy-done((bf16[3,128,512]{2,1,0:T(8,128)(2,1)S(1)}, bf16[3,128,512]{2,1,0:T(8,128)(2,1)}, u32[]{:S(2)}) %copy-start.9) | copy-done | bytes 393240
  2.4 0.9 %copy-done.10 = bf16[64,2048]{1,0:T(8,128)(2,1)S(1)} copy-done((bf16[64,2048]{1,0:T(8,128)(2,1)S(1)}, bf16[64,2048]{1,0:T(8,128)(2,1)}, u32[]{:S(2)}) %copy-start.10) | copy-done | bytes 262168
  5.4 1.7 %entry.1 = (bf16[64,8,384]{2,1,0:T(8,128)(2,1)}, bf16[128,2048]{1,0:T(8,128)(2,1)}, bf16[128,2048]{1,0:T(8,128)(2,1)}, f32[72,2048]{1,0:T(8,128)S(1)}) custom-call(bf16[16,128]{1,0:T(8,128)(2,1)S(1)} %bitcast.6, bf16[16,128]{1,0:T(8,128)(2,1)S(1)} %bitcast.7, bf16[3,128,512]{2,1,0:T(8,128)(2,1)S(1)} %copy-done.9, bf16[256,2048]{1,0:T(8,128)(2,1)S(1)} %copy-done.4, ...), custom_call_target="tpu_custom_call" | custom-call | flops 1000000 | tf_op jit(solution)/shard_map/entry/pallas_call | solution.py:360
  7.1 0.8 copy-done.7
  7.9 11.5 %all-to-all-start = ((bf16[64,8,384]{2,1,0:T(8,128)(2,1)}), bf16[64,8,384]{2,1,0:T(8,128)(2,1)S(1)}, u32[]{:S(2)}, u32[]{:S(2)}) async-start(bf16[64,8,384]{2,1,0:T(8,128)(2,1)} %get-tuple-element.19), calls=%async_computation | async-start | bytes 786432 | tf_op jit(solution)/shard_map/all_to_all | solution.py:418
  19.4 1.6 %collective-permute-start = (bf16[128,2048]{1,0:T(8,128)(2,1)}, bf16[128,2048]{1,0:T(8,128)(2,1)}, u32[]{:S(2)}, u32[]{:S(2)}) collective-permute-start(bf16[128,2048]{1,0:T(8,128)(2,1)} %get-tuple-element.24), channel_id=1, source_target_pairs={{0,2},{2,0},{4,6},{6,4},{8,10},{10,8},{12,14},{14,12},{16,18},{18,... | collective-permute-start | bytes 1572872 | tf_op jit(solution)/shard_map/ppermute | solution.py:421
  21.1 1.5 %collective-permute-start.1 = (bf16[128,2048]{1,0:T(8,128)(2,1)}, bf16[128,2048]{1,0:T(8,128)(2,1)}, u32[]{:S(2)}, u32[]{:S(2)}) collective-permute-start(bf16[128,2048]{1,0:T(8,128)(2,1)} %get-tuple-element.25), channel_id=1, source_target_pairs={{2,4},{4,2},{6,8},{8,6},{10,12},{12,10},{14,16},{16,14},{18,20},{2... | collective-permute-start | bytes 1572872 | tf_op jit(solution)/shard_map/ppermute | solution.py:422
  22.5 0.8 fusion.1
  23.4 9.4 %all-to-all-done.recv_ref = bf16[64,8,384]{2,1,0:T(8,128)(2,1)S(1)} async-done(((bf16[64,8,384]{2,1,0:T(8,128)(2,1)}), bf16[64,8,384]{2,1,0:T(8,128)(2,1)S(1)}, u32[]{:S(2)}, u32[]{:S(2)}) %all-to-all-start) | async-done | bytes 393248 | tf_op jit(solution)/shard_map/all_to_all | solution.py:418
  32.8 1.2 %copy-done = bf16[2048,256]{1,0:T(8,128)(2,1)S(1)} copy-done((bf16[2048,256]{1,0:T(8,128)(2,1)S(1)}, bf16[2048,256]{1,0:T(8,128)(2,1)}, u32[]{:S(2)}) %copy-start) | copy-done | bytes 1048600
  34.0 1.2 %copy-done.2 = bf16[2048,256]{1,0:T(8,128)(2,1)S(1)} copy-done((bf16[2048,256]{1,0:T(8,128)(2,1)S(1)}, bf16[2048,256]{1,0:T(8,128)(2,1)}, u32[]{:S(2)}) %copy-start.2) | copy-done | bytes 1048600
  35.2 1.1 %copy-done.8 = f32[72,2048]{1,0:T(8,128)S(1)} copy-done((f32[72,2048]{1,0:T(8,128)S(1)}, f32[72,2048]{1,0:T(8,128)}, u32[]{:S(2)}) %copy-start.8) | copy-done | bytes 589848
  36.3 2.1 %context.1 = (bf16[16,64,512]{2,1,0:T(8,128)(2,1)S(1)}, f32[8,2048]{1,0:T(8,128)S(1)}) custom-call(bf16[64,8,384]{2,1,0:T(8,128)(2,1)S(1)} %all-to-all-done.recv_ref, f32[72,2048]{1,0:T(8,128)S(1)} %copy-done.8, bf16[2048,256]{1,0:T(8,128)(2,1)S(1)} %copy-done, bf16[2048,256]{1,0:T(8,128)(2,1)S(1)} %copy-done.2), custom_call_target="tpu_custom_call" | custom-call | flops 1000000 | tf_op jit(solution)/shard_map/context/pallas_call | solution.py:360
  38.4 1.0 %copy-done.6 = bf16[16,64,512]{2,1,0:T(8,128)(2,1)} copy-done((bf16[16,64,512]{2,1,0:T(8,128)(2,1)}, bf16[16,64,512]{2,1,0:T(8,128)(2,1)S(1)}, u32[]{:S(2)}) %copy-start.6) | copy-done | bytes 1048600
  40.0 4.5 %all-to-all-start.1 = ((bf16[16,64,512]{2,1,0:T(8,128)(2,1)}), bf16[16,64,512]{2,1,0:T(8,128)(2,1)}, u32[]{:S(2)}, u32[]{:S(2)}) async-start(bf16[16,64,512]{2,1,0:T(8,128)(2,1)} %copy-done.6), calls=%async_computation.1 | async-start | bytes 2097152 | tf_op jit(solution)/shard_map/all_to_all | solution.py:434
  44.6 0.8 copy-done.11
  45.4 0.8 copy-done.12
  46.2 0.8 copy-done.14
  47.1 2.2 %copy-done.19 = bf16[2048,1024]{1,0:T(8,128)(2,1)S(1)} copy-done((bf16[2048,1024]{1,0:T(8,128)(2,1)S(1)}, bf16[2048,1024]{1,0:T(8,128)(2,1)}, u32[]{:S(2)}) %copy-start.19) | copy-done | bytes 4194328
  49.9 10.1 %own.1 = (bf16[256,1024]{1,0:T(8,128)(2,1)S(1)}, bf16[256,1024]{1,0:T(8,128)(2,1)S(1)}, f32[256,1024]{1,0:T(8,128)S(1)}, f32[256,1024]{1,0:T(8,128)S(1)}, f32[256,1024]{1,0:T(8,128)S(1)}) custom-call(f32[16]{0:T(128)S(1)} %copy-done.28, f32[8,2048]{1,0:T(8,128)S(1)} %copy-done.14, bf16[256,2048]{1,0:T(8,128)(2,1)S(1)} %copy-done.5, ...), custom_call_target="tpu_custom_call" | custom-call | flops 10000000000 | tf_op jit(solution)/shard_map/own/pallas_call | solution.py:360
  60.0 0.8 copy-done.29
  60.8 6.7 %halo.1 = (f32[256,1024]{1,0:T(8,128)S(1)}, f32[256,1024]{1,0:T(8,128)S(1)}, f32[256,1024]{1,0:T(8,128)S(1)}) custom-call(f32[8,2048]{1,0:T(8,128)S(1)} %copy-done.14, bf16[128,2048]{1,0:T(8,128)(2,1)} %collective-permute-done.one_ref, bf16[128,2048]{1,0:T(8,128)(2,1)} %collective-permute-done.1.two_ref, bf16[2048,256]{1,0:T(8,128)(2,1)S(1)} %copy-done.1, ...), custom_call_target="tpu_custom_call" | custom-call | flops 1000000000 | tf_op jit(solution)/shard_map/halo/pallas_call | solution.py:360
  67.5 1.0 %copy-done.21 = f32[256,1024]{1,0:T(8,128)} copy-done((f32[256,1024]{1,0:T(8,128)}, f32[256,1024]{1,0:T(8,128)S(1)}, u32[]{:S(2)}) %copy-start.21) | copy-done | bytes 1048600
  68.5 1.0 %copy-done.23 = f32[256,1024]{1,0:T(8,128)} copy-done((f32[256,1024]{1,0:T(8,128)}, f32[256,1024]{1,0:T(8,128)S(1)}, u32[]{:S(2)}) %copy-start.23) | copy-done | bytes 1048600
  69.5 1.0 %copy-done.25 = f32[256,1024]{1,0:T(8,128)} copy-done((f32[256,1024]{1,0:T(8,128)}, f32[256,1024]{1,0:T(8,128)S(1)}, u32[]{:S(2)}) %copy-start.25) | copy-done | bytes 1048600
  70.5 2.2 %copy-done.20 = bf16[1024,2048]{1,0:T(8,128)(2,1)S(1)} copy-done((bf16[1024,2048]{1,0:T(8,128)(2,1)S(1)}, bf16[1024,2048]{1,0:T(8,128)(2,1)}, u32[]{:S(2)}) %copy-start.20) | copy-done | bytes 4194328
  72.7 1.2 %copy-done.22 = f32[256,1024]{1,0:T(8,128)S(1)} copy-done((f32[256,1024]{1,0:T(8,128)S(1)}, f32[256,1024]{1,0:T(8,128)}, u32[]{:S(2)}) %copy-start.22) | copy-done | bytes 1048600
  73.9 1.2 %copy-done.24 = f32[256,1024]{1,0:T(8,128)S(1)} copy-done((f32[256,1024]{1,0:T(8,128)S(1)}, f32[256,1024]{1,0:T(8,128)}, u32[]{:S(2)}) %copy-start.24) | copy-done | bytes 1048600
  75.1 1.2 %copy-done.26 = f32[256,1024]{1,0:T(8,128)S(1)} copy-done((f32[256,1024]{1,0:T(8,128)S(1)}, f32[256,1024]{1,0:T(8,128)}, u32[]{:S(2)}) %copy-start.26) | copy-done | bytes 1048600
  76.4 1.0 %copy-done.30 = bf16[256,1024]{1,0:T(8,128)(2,1)S(1)} copy-done((bf16[256,1024]{1,0:T(8,128)(2,1)S(1)}, bf16[256,1024]{1,0:T(8,128)(2,1)}, u32[]{:S(2)}) %copy-start.30) | copy-done | bytes 524312
  77.4 11.1 %final.1 = bf16[256,2048]{1,0:T(8,128)(2,1)} custom-call(bf16[256,1024]{1,0:T(8,128)(2,1)S(1)} %copy-done.30, bf16[1024,512]{1,0:T(8,128)(2,1)} %bitcast.3.kv_ref, f32[256,1024]{1,0:T(8,128)S(1)} %copy-done.22, f32[256,1024]{1,0:T(8,128)S(1)} %copy-done.24, f32[256,1024]{1,0:T(8,128)S(1)} %copy-done.26, bf16[1024,2048]{1,0:T(8,128)(2,1)S(1)} %copy-done.20, ...), custom_call_target="tpu_custom_call" | custom-call | flops 10000000000 | tf_op jit(solution)/shard_map/final/pallas_call | solution.py:360
  (45 shorter events, 3.4 us)
Async XLA Ops:
  0.0 44.5 %copy-start.3 = (bf16[2048,256]{1,0:T(8,128)(2,1)S(1)}, bf16[2048,256]{1,0:T(8,128)(2,1)}, u32[]{:S(2)}) copy-start(bf16[2048,256]{1,0:T(8,128)(2,1)} %wv_ref.5) | copy-start | bytes 3145732
  0.0 44.5 %copy-start.1 = (bf16[2048,256]{1,0:T(8,128)(2,1)S(1)}, bf16[2048,256]{1,0:T(8,128)(2,1)}, u32[]{:S(2)}) copy-start(bf16[2048,256]{1,0:T(8,128)(2,1)} %wk_ref.5) | copy-start | bytes 3145732
  0.0 1.4 %copy-start.4 = (bf16[256,2048]{1,0:T(8,128)(2,1)S(1)}, bf16[256,2048]{1,0:T(8,128)(2,1)}, u32[]{:S(2)}) copy-start(bf16[256,2048]{1,0:T(8,128)(2,1)} %lat_ref.5) | copy-start | bytes 3145732
  1.4 1.0 %copy-start.9 = (bf16[3,128,512]{2,1,0:T(8,128)(2,1)S(1)}, bf16[3,128,512]{2,1,0:T(8,128)(2,1)}, u32[]{:S(2)}) copy-start(bf16[3,128,512]{2,1,0:T(8,128)(2,1)} %mod_ref.1) | copy-start | bytes 1179652
  2.4 0.9 %copy-start.10 = (bf16[64,2048]{1,0:T(8,128)(2,1)S(1)}, bf16[64,2048]{1,0:T(8,128)(2,1)}, u32[]{:S(2)}) copy-start(bf16[64,2048]{1,0:T(8,128)(2,1)} %ctx_ref.1) | copy-start | bytes 786436
  3.3 0.7 copy-start.16
  4.0 0.7 copy-start.17
  7.1 0.8 copy-start.7
  7.9 24.9 %all-to-all-start = ((bf16[64,8,384]{2,1,0:T(8,128)(2,1)}), bf16[64,8,384]{2,1,0:T(8,128)(2,1)S(1)}, u32[]{:S(2)}, u32[]{:S(2)}) async-start(bf16[64,8,384]{2,1,0:T(8,128)(2,1)} %get-tuple-element.19), calls=%async_computation | async-start | bytes 786432 | tf_op jit(solution)/shard_map/all_to_all | solution.py:418
  19.4 41.4 %collective-permute-start = (bf16[128,2048]{1,0:T(8,128)(2,1)}, bf16[128,2048]{1,0:T(8,128)(2,1)}, u32[]{:S(2)}, u32[]{:S(2)}) collective-permute-start(bf16[128,2048]{1,0:T(8,128)(2,1)} %get-tuple-element.24), channel_id=1, source_target_pairs={{0,2},{2,0},{4,6},{6,4},{8,10},{10,8},{12,14},{14,12},{16,18},{18,... | collective-permute-start | bytes 1572872 | tf_op jit(solution)/shard_map/ppermute | solution.py:421
  21.1 39.7 %collective-permute-start.1 = (bf16[128,2048]{1,0:T(8,128)(2,1)}, bf16[128,2048]{1,0:T(8,128)(2,1)}, u32[]{:S(2)}, u32[]{:S(2)}) collective-permute-start(bf16[128,2048]{1,0:T(8,128)(2,1)} %get-tuple-element.25), channel_id=1, source_target_pairs={{2,4},{4,2},{6,8},{8,6},{10,12},{12,10},{14,16},{16,14},{18,20},{2... | collective-permute-start | bytes 1572872 | tf_op jit(solution)/shard_map/ppermute | solution.py:422
  32.8 1.2 %copy-start = (bf16[2048,256]{1,0:T(8,128)(2,1)S(1)}, bf16[2048,256]{1,0:T(8,128)(2,1)}, u32[]{:S(2)}) copy-start(bf16[2048,256]{1,0:T(8,128)(2,1)} %wk_ref.5) | copy-start | bytes 3145732
  34.0 1.2 %copy-start.2 = (bf16[2048,256]{1,0:T(8,128)(2,1)S(1)}, bf16[2048,256]{1,0:T(8,128)(2,1)}, u32[]{:S(2)}) copy-start(bf16[2048,256]{1,0:T(8,128)(2,1)} %wv_ref.5) | copy-start | bytes 3145732
  35.2 1.1 %copy-start.8 = (f32[72,2048]{1,0:T(8,128)S(1)}, f32[72,2048]{1,0:T(8,128)}, u32[]{:S(2)}) copy-start(f32[72,2048]{1,0:T(8,128)} %copy-done.7) | copy-start | bytes 1769476
  36.3 8.3 %copy-start.5 = (bf16[256,2048]{1,0:T(8,128)(2,1)S(1)}, bf16[256,2048]{1,0:T(8,128)(2,1)}, u32[]{:S(2)}) copy-start(bf16[256,2048]{1,0:T(8,128)(2,1)} %lat_ref.5) | copy-start | bytes 3145732
  38.4 1.0 %copy-start.6 = (bf16[16,64,512]{2,1,0:T(8,128)(2,1)}, bf16[16,64,512]{2,1,0:T(8,128)(2,1)S(1)}, u32[]{:S(2)}) copy-start(bf16[16,64,512]{2,1,0:T(8,128)(2,1)S(1)} %get-tuple-element.23) | copy-start | bytes 3145732
  40.0 30.5 %all-to-all-start.1 = ((bf16[16,64,512]{2,1,0:T(8,128)(2,1)}), bf16[16,64,512]{2,1,0:T(8,128)(2,1)}, u32[]{:S(2)}, u32[]{:S(2)}) async-start(bf16[16,64,512]{2,1,0:T(8,128)(2,1)} %copy-done.6), calls=%async_computation.1 | async-start | bytes 2097152 | tf_op jit(solution)/shard_map/all_to_all | solution.py:434
  44.6 0.8 copy-start.11
  45.4 0.8 copy-start.12
  46.2 0.8 copy-start.14
  47.1 2.2 %copy-start.19 = (bf16[2048,1024]{1,0:T(8,128)(2,1)S(1)}, bf16[2048,1024]{1,0:T(8,128)(2,1)}, u32[]{:S(2)}) copy-start(bf16[2048,1024]{1,0:T(8,128)(2,1)} %wq_ref.1) | copy-start | bytes 12582916
  60.0 0.8 copy-start.29
  60.8 9.7 %copy-start.15 = (f32[8,2048]{1,0:T(8,128)S(1)}, f32[8,2048]{1,0:T(8,128)}, u32[]{:S(2)}) copy-start(f32[8,2048]{1,0:T(8,128)} %copy-done.13) | copy-start | bytes 196612
  60.8 9.7 %copy-start.27 = (f32[2048]{0:T(1024)S(1)}, f32[2048]{0:T(1024)}, u32[]{:S(2)}) copy-start(f32[2048]{0:T(1024)} %param.22) | copy-start | bytes 24580
  67.5 1.0 %copy-start.21 = (f32[256,1024]{1,0:T(8,128)}, f32[256,1024]{1,0:T(8,128)S(1)}, u32[]{:S(2)}) copy-start(f32[256,1024]{1,0:T(8,128)S(1)} %get-tuple-element.30.o_ref) | copy-start | bytes 3145732
  68.5 1.0 %copy-start.23 = (f32[256,1024]{1,0:T(8,128)}, f32[256,1024]{1,0:T(8,128)S(1)}, u32[]{:S(2)}) copy-start(f32[256,1024]{1,0:T(8,128)S(1)} %get-tuple-element.31.l_ref) | copy-start | bytes 3145732
  69.5 1.0 %copy-start.25 = (f32[256,1024]{1,0:T(8,128)}, f32[256,1024]{1,0:T(8,128)S(1)}, u32[]{:S(2)}) copy-start(f32[256,1024]{1,0:T(8,128)S(1)} %get-tuple-element.32.m_ref) | copy-start | bytes 3145732
  70.5 2.2 %copy-start.20 = (bf16[1024,2048]{1,0:T(8,128)(2,1)S(1)}, bf16[1024,2048]{1,0:T(8,128)(2,1)}, u32[]{:S(2)}) copy-start(bf16[1024,2048]{1,0:T(8,128)(2,1)} %wo_ref.1) | copy-start | bytes 12582916
  72.7 1.2 %copy-start.22 = (f32[256,1024]{1,0:T(8,128)S(1)}, f32[256,1024]{1,0:T(8,128)}, u32[]{:S(2)}) copy-start(f32[256,1024]{1,0:T(8,128)} %copy-done.21) | copy-start | bytes 3145732
  73.9 1.2 %copy-start.24 = (f32[256,1024]{1,0:T(8,128)S(1)}, f32[256,1024]{1,0:T(8,128)}, u32[]{:S(2)}) copy-start(f32[256,1024]{1,0:T(8,128)} %copy-done.23) | copy-start | bytes 3145732
  75.1 1.2 %copy-start.26 = (f32[256,1024]{1,0:T(8,128)S(1)}, f32[256,1024]{1,0:T(8,128)}, u32[]{:S(2)}) copy-start(f32[256,1024]{1,0:T(8,128)} %copy-done.25) | copy-start | bytes 3145732
  76.4 1.0 %copy-start.30 = (bf16[256,1024]{1,0:T(8,128)(2,1)S(1)}, bf16[256,1024]{1,0:T(8,128)(2,1)}, u32[]{:S(2)}) copy-start(bf16[256,1024]{1,0:T(8,128)(2,1)} %copy-done.29) | copy-start | bytes 1572868
  (3 other events, 2.0 us)

commit v3 on v2

--- a/solution.py
+++ b/solution.py
@@ -180,14 +180,15 @@
 def own_kernel(
     sink_ref, vec_ref, lat_ref, wq_ref, wk_ref, wv_ref, rowc_ref, rows_ref, colc_ref, cols_ref,
     q_ref, rot_ref, o_ref, l_ref, m_ref,
-    vec_v, lat_v, wq_v, hid_v, q_v, sems,
+    vec_v, lat_v, wq_v, hid_v, q_v, wk_v, wv_v, sems,
 ):
     copy = pltpu.make_async_copy
     ins = [copy(vec_ref, vec_v, sems.at[0]), copy(lat_ref, lat_v, sems.at[1])]
+    more = [copy(wk_ref, wk_v, sems.at[10]), copy(wv_ref, wv_v, sems.at[11])]
     for h in range(4):
         cols = pl.ds(h * 256, 256)
         ins.append(copy(wq_ref.at[:, cols], wq_v.at[h], sems.at[2 + h]))
-    for c in ins:
+    for c in ins[:2] + more + ins[2:]:
         c.start()
     swap = swap_matrix()
     cos = jnp.concatenate([colc_ref[...] + rowc_ref[r : r + 1, :] for r in range(2, 6)], axis=0)
@@ -195,8 +196,10 @@
     ins[0].wait()
     ins[1].wait()
     hid_v[...] = normed(lat_v[...], vec_v[0:1, :], vec_v[1:2, :])
-    keys = rotated(dot(hid_v[...], wk_ref[...]).astype(BF16), cos, sin, swap)
-    vals = dot(hid_v[...], wv_ref[...]).astype(BF16)
+    for c in more:
+        c.wait()
+    keys = rotated(dot(hid_v[...], wk_v[...]).astype(BF16), cos, sin, swap)
+    vals = dot(hid_v[...], wv_v[...]).astype(BF16)
     lane = iota((128, 256), 1) // HEAD_DIM
     first = iota((128, 128), 1) < HEAD_DIM
     row, col = iota((128, 128), 0), iota((128, 128), 1)
@@ -238,7 +241,7 @@
     vec_ref, one_ref, two_ref, wk_ref, wv_ref, rowc_ref, rows_ref, colc_ref, cols_ref,
     rot_ref, o_ref, l_ref, m_ref,
     oo_ref, ll_ref, mm_ref,
-    vec_v, raw_v, hid_v, o_v, l_v, m_v, sems,
+    vec_v, raw_v, hid_v, o_v, l_v, m_v, wk_v, wv_v, sems,
 ):
     place = place_of()
     odd = place & 1
@@ -247,6 +250,8 @@
         copy(vec_ref, vec_v, sems.at[0]),
         copy(one_ref, raw_v.at[1 - odd], sems.at[1]),
         copy(two_ref, raw_v.at[odd], sems.at[2]),
+        copy(wk_ref, wk_v, sems.at[15]),
+        copy(wv_ref, wv_v, sems.at[16]),
     ]
     for c in ins:
         c.start()
@@ -258,8 +263,8 @@
         c.wait()
     for b in range(2):
         hid_v[b * 128 : b * 128 + 128, :] = normed(raw_v[b], vec_v[0:1, :], vec_v[1:2, :])
-    keys = rotated(dot(hid_v[...], wk_ref[...]).astype(BF16), cos, sin, swap)
-    vals = dot(hid_v[...], wv_ref[...]).astype(BF16)
+    keys = rotated(dot(hid_v[...], wk_v[...]).astype(BF16), cos, sin, swap)
+    vals = dot(hid_v[...], wv_v[...]).astype(BF16)
     lane = iota((128, 256), 1) // HEAD_DIM
     first = iota((128, 128), 1) < HEAD_DIM
     row, col = iota((128, 128), 0), iota((128, 128), 1)
@@ -359,7 +364,7 @@
 def call(kernel, name, ins, outs, scratch, copies, args, flops, limit):
     return pl.pallas_call(
         kernel,
-        out_shape=[jax.ShapeDtypeStruct(s, d) for _, s, d in outs],
+        out_shape=[HB(s, d) if k == "h" else jax.ShapeDtypeStruct(s, d) for k, s, d in outs],
         in_specs=spec(ins),
         out_specs=spec([k for k, _, _ in outs]),
         scratch_shapes=[pltpu.VMEM(s, d) for s, d in scratch]
@@ -367,7 +372,7 @@
         compiler_params=pltpu.CompilerParams(vmem_limit_bytes=limit * 1024 * 1024),
         cost_estimate=pl.CostEstimate(flops=flops, bytes_accessed=0, transcendentals=0),
         name=name,
-    )(*args)
+    )(*[pltpu.with_memory_space_constraint(x, HB) if k == "h" else x for k, x in zip(ins, args)])
 
 
 def shards(
@@ -446,10 +451,10 @@
     query, turned, o, l, m = call(
         own_kernel,
         "own",
-        "shhhvvvvvv",
+        "shhhhhvvvv",
         [("h", wide, BF16), ("v", wide, BF16), ("v", wide, F32), ("v", wide, F32), ("v", wide, F32)],
-        [(rest, F32), (latent.shape, BF16), ((4, width, 256), BF16), (latent.shape, BF16), (wide, BF16)],
-        10,
+        [(rest, F32), (latent.shape, BF16), ((4, width, 256), BF16), (latent.shape, BF16), (wide, BF16), (w_key.shape, BF16), (w_key.shape, BF16)],
+        12,
         (sink, vecs, latent, w_query, w_key, w_value, *tables),
         10**10,
         16,
@@ -457,10 +462,10 @@
     o, l, m = call(
         halo_kernel,
         "halo",
-        "hhhvvvvvvvvvv",
+        "hhhhhvvvvvvvv",
         [("h", wide, F32)] * 3,
-        [(rest, F32), ((2, WINDOW, width), BF16), (latent.shape, BF16), (wide, F32), (wide, F32), (wide, F32)],
-        15,
+        [(rest, F32), ((2, WINDOW, width), BF16), (latent.shape, BF16), (wide, F32), (wide, F32), (wide, F32), (w_key.shape, BF16), (w_key.shape, BF16)],
+        17,
         (vecs, one, two, w_key, w_value, *tables, turned, o, l, m),
         10**9,
         12,

time: 89.7 us -> 67.1 us (0.75)
  local copies, waits for them, and re-layouts: 27.3 us -> 4.43 us
  Pallas kernels: 31.7 us -> 33.3 us
  starting transfers between devices: 19.2 us -> 17.7 us
    unnamed x62 -> x16, local copies, waits for them, and re-layouts: 27.3 us -> 4.43 us
    pallas_call x5, Pallas kernels: 31.7 us -> 33.3 us  [call(): pl.pallas_call(kernel, out_shape=[HB(s, d) if k == 'h' else jax.ShapeDtyp...]
  transfers between devices with their start and end apart: 4 -> 4, of which waited for: 1 -> 1; matrix products, arithmetic and copies ran while one was open for 1% -> 1% of each run, Pallas kernels for 21% -> 29%
where the time goes in v3:
time: 67.1 us; the launch traced here: 66.7 us
  Pallas kernels  33.3 us (50%)
  starting transfers between devices  17.7 us (26%)
  waiting for transfers between devices  10.2 us (15%)
  local copies, waits for them, and re-layouts  4.43 us (7%)
  other arithmetic  0.82 us (1%)
    pallas_call x5, Pallas kernels, call(): pl.pallas_call(kernel, out_shape=[HB(s, d) if k == 'h' else jax.ShapeDtyp...  33.3 us
    all_to_all x1, starting transfers between devices, shards(): recv = lax.all_to_all(parts, both, 0, 0, tiled=True)  11.5 us
    all_to_all x1, waiting for transfers between devices, shards(): recv = lax.all_to_all(parts, both, 0, 0, tiled=True)  10.1 us
    unnamed x16, local copies, waits for them, and re-layouts  4.43 us
    all_to_all x1, starting transfers between devices, shards(): lax.all_to_all(send, 'sp', 0, 0, tiled=True).reshape(sp_size * 64, 512)  3.85 us
    ppermute x1, starting transfers between devices, shards(): one = lax.ppermute(one, both, swap_one)  1.65 us
  transfers between devices with their start and end apart: 4, of which 1 were waited for; matrix products, arithmetic and copies ran while one was open for 1% of the time, Pallas kernels for 29%

profile of v3, /device:TPU:0, one launch (start us, length us, event | category | flops | bytes accessed | tf_op | source)
XLA Modules:
  0.0 66.7 jit_solution(12852194369726013691)
XLA Ops:
  0.0 0.0 copy-start.2
  0.0 0.0 copy-start.3
  0.0 0.0 copy-start.4
  0.0 2.5 %entry.1 = (bf16[64,8,384]{2,1,0:T(8,128)(2,1)}, bf16[128,2048]{1,0:T(8,128)(2,1)}, bf16[128,2048]{1,0:T(8,128)(2,1)}, f32[72,2048]{1,0:T(8,128)S(1)}) custom-call(bf16[16,128]{1,0:T(8,128)(2,1)} %bitcast.7, bf16[16,128]{1,0:T(8,128)(2,1)} %bitcast.8, bf16[3,128,512]{2,1,0:T(8,128)(2,1)} %mod_ref.1, bf16[256,2048]{1,0:T(8,128)(2,1)} %lat_ref.5, ...), custom_call_target="tpu_custom_call" | custom-call | flops 1000000 | tf_op jit(solution)/shard_map/entry/pallas_call | solution.py:365
  2.5 11.5 %all-to-all-start = ((bf16[64,8,384]{2,1,0:T(8,128)(2,1)}), bf16[64,8,384]{2,1,0:T(8,128)(2,1)S(1)}, u32[]{:S(2)}, u32[]{:S(2)}) async-start(bf16[64,8,384]{2,1,0:T(8,128)(2,1)} %get-tuple-element.19), calls=%async_computation | async-start | bytes 786432 | tf_op jit(solution)/shard_map/all_to_all | solution.py:423
  14.0 1.6 %collective-permute-start = (bf16[128,2048]{1,0:T(8,128)(2,1)}, bf16[128,2048]{1,0:T(8,128)(2,1)S(1)}, u32[]{:S(2)}, u32[]{:S(2)}) collective-permute-start(bf16[128,2048]{1,0:T(8,128)(2,1)} %get-tuple-element.24), channel_id=1, source_target_pairs={{0,2},{2,0},{4,6},{6,4},{8,10},{10,8},{12,14},{14,12},{16,18},{18,... | collective-permute-start | bytes 1572872 | tf_op jit(solution)/shard_map/ppermute | solution.py:426
  15.7 0.7 %collective-permute-start.1 = (bf16[128,2048]{1,0:T(8,128)(2,1)}, bf16[128,2048]{1,0:T(8,128)(2,1)S(1)}, u32[]{:S(2)}, u32[]{:S(2)}) collective-permute-start(bf16[128,2048]{1,0:T(8,128)(2,1)} %get-tuple-element.25), channel_id=1, source_target_pairs={{2,4},{4,2},{6,8},{8,6},{10,12},{12,10},{14,16},{16,14},{18,20},{2... | collective-permute-start | bytes 1572872 | tf_op jit(solution)/shard_map/ppermute | solution.py:427
  16.4 0.8 %fusion.1 = (f32[8,256]{1,0:T(8,128)S(1)}, f32[8,256]{1,0:T(8,128)S(1)}) fusion(f32[256]{0:T(256)} %constant.27.clone, f32[256]{0:T(256)} %constant.26.clone, f32[8]{0:T(128)S(1)} %add_convert_fusion), kind=kLoop, calls=%fused_computation.3 | loop fusion | flops 6144 | bytes 18464 | tf_op jit(solution)/shard_map/mul | solution.py:449
  17.2 10.1 %all-to-all-done.recv_ref = bf16[64,8,384]{2,1,0:T(8,128)(2,1)S(1)} async-done(((bf16[64,8,384]{2,1,0:T(8,128)(2,1)}), bf16[64,8,384]{2,1,0:T(8,128)(2,1)S(1)}, u32[]{:S(2)}, u32[]{:S(2)}) %all-to-all-start) | async-done | bytes 393248 | tf_op jit(solution)/shard_map/all_to_all | solution.py:423
  27.3 0.0 copy-start
  27.3 1.2 %copy-done = bf16[2048,256]{1,0:T(8,128)(2,1)S(1)} copy-done((bf16[2048,256]{1,0:T(8,128)(2,1)S(1)}, bf16[2048,256]{1,0:T(8,128)(2,1)}, u32[]{:S(2)}) %copy-start) | copy-done | bytes 1048600
  28.6 0.0 copy-start.1
  28.6 1.2 %copy-done.1 = bf16[2048,256]{1,0:T(8,128)(2,1)S(1)} copy-done((bf16[2048,256]{1,0:T(8,128)(2,1)S(1)}, bf16[2048,256]{1,0:T(8,128)(2,1)}, u32[]{:S(2)}) %copy-start.1) | copy-done | bytes 1048600
  29.8 1.6 %context.1 = (bf16[16,64,512]{2,1,0:T(8,128)(2,1)}, f32[8,2048]{1,0:T(8,128)}) custom-call(bf16[64,8,384]{2,1,0:T(8,128)(2,1)S(1)} %all-to-all-done.recv_ref, f32[72,2048]{1,0:T(8,128)S(1)} %get-tuple-element.20.ng_ref, bf16[2048,256]{1,0:T(8,128)(2,1)S(1)} %copy-done, bf16[2048,256]{1,0:T(8,128)(2,1)S(1)} %copy-done.1), custom_call_target="tpu_custom_call" | custom-call | flops 1000000 | tf_op jit(solution)/shard_map/context/pallas_call | solution.py:365
  31.4 3.8 %all-to-all-start.1 = ((bf16[16,64,512]{2,1,0:T(8,128)(2,1)}), bf16[16,64,512]{2,1,0:T(8,128)(2,1)S(1)}, u32[]{:S(2)}, u32[]{:S(2)}) async-start(bf16[16,64,512]{2,1,0:T(8,128)(2,1)} %get-tuple-element.23), calls=%async_computation.1 | async-start | bytes 2097152 | tf_op jit(solution)/shard_map/all_to_all | solution.py:439
  35.3 0.0 copy-done.2
  35.3 0.0 copy-done.3
  35.3 0.0 copy-done.4
  35.3 11.0 %own.1 = (bf16[256,1024]{1,0:T(8,128)(2,1)}, bf16[256,1024]{1,0:T(8,128)(2,1)S(1)}, f32[256,1024]{1,0:T(8,128)S(1)}, f32[256,1024]{1,0:T(8,128)S(1)}, f32[256,1024]{1,0:T(8,128)S(1)}) custom-call(f32[16]{0:T(128)S(1)} %copy-done.4, f32[8,2048]{1,0:T(8,128)} %get-tuple-element.21.vec_ref, bf16[256,2048]{1,0:T(8,128)(2,1)} %lat_ref.5, ...), custom_call_target="tpu_custom_call" | custom-call | flops 10000000000 | tf_op jit(solution)/shard_map/own/pallas_call | solution.py:365
  46.3 0.0 collective-permute-done.one_ref
  46.3 0.0 copy-start.6
  46.3 0.0 collective-permute-done.1.two_ref
  46.3 0.0 copy-start.7
  46.3 0.8 %copy-done.6 = bf16[128,2048]{1,0:T(8,128)(2,1)} copy-done((bf16[128,2048]{1,0:T(8,128)(2,1)}, bf16[128,2048]{1,0:T(8,128)(2,1)S(1)}, u32[]{:S(2)}) %copy-start.6) | copy-done | bytes 524312
  47.1 0.2 copy-done.7
  47.3 6.7 %halo.1 = (f32[256,1024]{1,0:T(8,128)}, f32[256,1024]{1,0:T(8,128)}, f32[256,1024]{1,0:T(8,128)}) custom-call(f32[8,2048]{1,0:T(8,128)} %get-tuple-element.21.vec_ref, bf16[128,2048]{1,0:T(8,128)(2,1)} %copy-done.6, bf16[128,2048]{1,0:T(8,128)(2,1)} %copy-done.7, bf16[2048,256]{1,0:T(8,128)(2,1)} %wk_ref.5, bf16[2048,256]{1,0:T(8,128)(2,1)} %wv_ref.5, ...), custom_call_target="tpu_custom_call" | custom-call | flops 1000000000 | tf_op jit(solution)/shard_map/halo/pallas_call | solution.py:365
  54.1 0.0 all-to-all-done.1
  54.1 0.0 copy-start.5
  54.1 1.0 %copy-done.5 = bf16[16,64,512]{2,1,0:T(8,128)(2,1)} copy-done((bf16[16,64,512]{2,1,0:T(8,128)(2,1)}, bf16[16,64,512]{2,1,0:T(8,128)(2,1)S(1)}, u32[]{:S(2)}) %copy-start.5) | copy-done | bytes 1048600
  55.1 11.5 %final.1 = bf16[256,2048]{1,0:T(8,128)(2,1)} custom-call(bf16[256,1024]{1,0:T(8,128)(2,1)} %get-tuple-element.22.q_ref, bf16[1024,512]{1,0:T(8,128)(2,1)} %bitcast.5, f32[256,1024]{1,0:T(8,128)} %get-tuple-element.30.o_ref, f32[256,1024]{1,0:T(8,128)} %get-tuple-element.31.l_ref, f32[256,1024]{1,0:T(8,128)} %get-tuple-element.32.m_ref, ...), custom_call_target="tpu_custom_call" | custom-call | flops 10000000000 | tf_op jit(solution)/shard_map/final/pallas_call | solution.py:365
  (1 shorter events, 0.0 us)
Async XLA Ops:
  0.0 35.3 %copy-start.2 = (f32[64,256]{1,0:T(8,128)S(1)}, f32[64,256]{1,0:T(8,128)}, u32[]{:S(2)}) copy-start(f32[64,256]{1,0:T(8,128)} %constant.25.clone.cols_ref) | copy-start | bytes 196612
  0.0 35.3 %copy-start.3 = (f32[64,256]{1,0:T(8,128)S(1)}, f32[64,256]{1,0:T(8,128)}, u32[]{:S(2)}) copy-start(f32[64,256]{1,0:T(8,128)} %constant.24.clone.colc_ref) | copy-start | bytes 196612
  0.0 35.3 %copy-start.4 = (f32[16]{0:T(128)S(1)}, f32[16]{0:T(128)}, u32[]{:S(2)}) copy-start(f32[16]{0:T(128)} %sink_ref.1) | copy-start | bytes 196
  2.5 24.9 %all-to-all-start = ((bf16[64,8,384]{2,1,0:T(8,128)(2,1)}), bf16[64,8,384]{2,1,0:T(8,128)(2,1)S(1)}, u32[]{:S(2)}, u32[]{:S(2)}) async-start(bf16[64,8,384]{2,1,0:T(8,128)(2,1)} %get-tuple-element.19), calls=%async_computation | async-start | bytes 786432 | tf_op jit(solution)/shard_map/all_to_all | solution.py:423
  14.0 32.3 %collective-permute-start = (bf16[128,2048]{1,0:T(8,128)(2,1)}, bf16[128,2048]{1,0:T(8,128)(2,1)S(1)}, u32[]{:S(2)}, u32[]{:S(2)}) collective-permute-start(bf16[128,2048]{1,0:T(8,128)(2,1)} %get-tuple-element.24), channel_id=1, source_target_pairs={{0,2},{2,0},{4,6},{6,4},{8,10},{10,8},{12,14},{14,12},{16,18},{18,... | collective-permute-start | bytes 1572872 | tf_op jit(solution)/shard_map/ppermute | solution.py:426
  15.7 30.7 %collective-permute-start.1 = (bf16[128,2048]{1,0:T(8,128)(2,1)}, bf16[128,2048]{1,0:T(8,128)(2,1)S(1)}, u32[]{:S(2)}, u32[]{:S(2)}) collective-permute-start(bf16[128,2048]{1,0:T(8,128)(2,1)} %get-tuple-element.25), channel_id=1, source_target_pairs={{2,4},{4,2},{6,8},{8,6},{10,12},{12,10},{14,16},{16,14},{18,20},{2... | collective-permute-start | bytes 1572872 | tf_op jit(solution)/shard_map/ppermute | solution.py:427
  27.3 1.2 %copy-start = (bf16[2048,256]{1,0:T(8,128)(2,1)S(1)}, bf16[2048,256]{1,0:T(8,128)(2,1)}, u32[]{:S(2)}) copy-start(bf16[2048,256]{1,0:T(8,128)(2,1)} %wk_ref.5) | copy-start | bytes 3145732
  28.6 1.2 %copy-start.1 = (bf16[2048,256]{1,0:T(8,128)(2,1)S(1)}, bf16[2048,256]{1,0:T(8,128)(2,1)}, u32[]{:S(2)}) copy-start(bf16[2048,256]{1,0:T(8,128)(2,1)} %wv_ref.5) | copy-start | bytes 3145732
  31.4 22.7 %all-to-all-start.1 = ((bf16[16,64,512]{2,1,0:T(8,128)(2,1)}), bf16[16,64,512]{2,1,0:T(8,128)(2,1)S(1)}, u32[]{:S(2)}, u32[]{:S(2)}) async-start(bf16[16,64,512]{2,1,0:T(8,128)(2,1)} %get-tuple-element.23), calls=%async_computation.1 | async-start | bytes 2097152 | tf_op jit(solution)/shard_map/all_to_all | solution.py:439
  46.3 0.8 %copy-start.6 = (bf16[128,2048]{1,0:T(8,128)(2,1)}, bf16[128,2048]{1,0:T(8,128)(2,1)S(1)}, u32[]{:S(2)}) copy-start(bf16[128,2048]{1,0:T(8,128)(2,1)S(1)} %collective-permute-done.one_ref) | copy-start | bytes 1572868
  46.3 1.0 %copy-start.7 = (bf16[128,2048]{1,0:T(8,128)(2,1)}, bf16[128,2048]{1,0:T(8,128)(2,1)S(1)}, u32[]{:S(2)}) copy-start(bf16[128,2048]{1,0:T(8,128)(2,1)S(1)} %collective-permute-done.1.two_ref) | copy-start | bytes 1572868
  54.1 1.0 %copy-start.5 = (bf16[16,64,512]{2,1,0:T(8,128)(2,1)}, bf16[16,64,512]{2,1,0:T(8,128)(2,1)S(1)}, u32[]{:S(2)}) copy-start(bf16[16,64,512]{2,1,0:T(8,128)(2,1)S(1)} %all-to-all-done.1) | copy-start | bytes 3145732

commit v4 on v3

v4 whole, which is shorter than its diff:
```python
import jax
import numpy as np
import jax.numpy as jnp
from jax import lax
from jax.experimental import pallas as pl
from jax.experimental.pallas import tpu as pltpu
from jax.sharding import PartitionSpec as P

HEAD_DIM = 64
WINDOW = 128
GRID_W = 64
EPSILON = 1e-06
NEG_BIG = -1e30
LOG2E = 1.4426950408889634
FACTOR = HEAD_DIM**-0.5 * LOG2E
F32 = jnp.float32
BF16 = jnp.bfloat16
VM = pltpu.MemorySpace.VMEM
HB = pltpu.MemorySpace.HBM
SM = pltpu.MemorySpace.SMEM


def place_of():
    return lax.axis_index("sp") * lax.axis_size("tp") + lax.axis_index("tp")


def dot(a, b):
    return jnp.dot(a, b, preferred_element_type=F32)


def dot_nt(a, b):
    return lax.dot_general(a, b, (((1,), (1,)), ((), ())), preferred_element_type=F32)


def iota(shape, dim):
    return lax.broadcasted_iota(jnp.int32, shape, dim)


def swap_matrix():
    k, c = iota((256, 256), 0), iota((256, 256), 1)
    low = (c & 63) < 32
    neg = jnp.where(low & (k == c + 32), -1.0, 0.0)
    pos = jnp.where((~low) & (k == c - 32), 1.0, 0.0)
    return (neg + pos).astype(BF16)


def normed(x, mult, shift):
    x = x.astype(F32)
    rs = lax.rsqrt(jnp.mean(x * x, axis=-1, keepdims=True) + EPSILON)
    return (x * rs * mult + shift).astype(BF16)


def entry_kernel(
    cond_ref, cctx_ref, mod_ref, lat_ref,
    parts_ref, one_ref, two_ref,
    cond_v, cctx_v, mod_v, lat_v, block_v, sems,
):
    sp = lax.axis_index("sp")
    odd = place_of() & 1
    copy = pltpu.make_async_copy
    pairs = ((mod_ref, mod_v), (cond_ref, cond_v), (cctx_ref, cctx_v), (lat_ref, lat_v))
    ins = [copy(src, dst, sems.at[i]) for i, (src, dst) in enumerate(pairs)]
    for c in ins:
        c.start()
    ins[1].wait()
    ins[2].wait()
    here = iota((16, 128), 0) == sp
    rows = []
    for ref in (cond_v, cctx_v):
        x = jnp.sum(jnp.where(here, ref[...].astype(F32), 0.0), axis=0, keepdims=True)
        rows.append(x / (1.0 + jnp.exp(-x)))
    v = jnp.concatenate(rows + [jnp.zeros((6, 128), F32)], axis=0).astype(BF16)
    ins[0].wait()
    parts = [dot(v, mod_v[i]) for i in range(3)]
    five = (parts[0][0:1], parts[0][1:2], parts[1][0:1], parts[1][1:2], parts[2][0:1])
    zero = jnp.zeros((1, 128), F32)
    rows = []
    for j in range(4):
        cut = [x[:, j * 128 : (j + 1) * 128] for x in five]
        rows.append(jnp.concatenate(cut[:3], axis=1))
        rows.append(jnp.concatenate(cut[3:] + [zero], axis=1))
    block = jnp.concatenate(rows, axis=0).astype(BF16)
    for i in range(block_v.shape[0]):
        block_v[i] = block
    outs = [copy(block_v, parts_ref, sems.at[4])]
    outs[0].start()
    ins[3].wait()
    outs.append(copy(lat_v.at[pl.ds((1 - odd) * 128, 128)], one_ref, sems.at[5]))
    outs.append(copy(lat_v.at[pl.ds(odd * 128, 128)], two_ref, sems.at[6]))
    outs[1].start()
    outs[2].start()
    for c in outs:
        c.wait()


def prep_kernel(
    after_ref, ctx_ref, gain_ref, wk_ref, wv_ref, ng_ref, wk_out, wv_out, ctx_v, gain_v, sems
):
    copy = pltpu.make_async_copy
    pairs = ((ctx_ref, ctx_v), (gain_ref, gain_v), (wk_ref, wk_out), (wv_ref, wv_out))
    ins = [copy(src, dst, sems.at[i]) for i, (src, dst) in enumerate(pairs)]
    for c in ins:
        c.start()
    ins[0].wait()
    ins[1].wait()
    x = ctx_v[...].astype(F32)
    gain = gain_v[...]
    rs = lax.rsqrt(jnp.mean(x * x, axis=-1, keepdims=True) + EPSILON)
    ng_ref[0:64, :] = x * rs * gain
    ng_ref[64:72, :] = jnp.broadcast_to(gain, (8, 2048))
    ins[2].wait()
    ins[3].wait()


def context_kernel(recv_ref, ng_ref, wk_ref, wv_ref, send_ref, vec_ref, kv_v, vec_v, sems):
    sums = []
    for t in range(4):
        acc = recv_ref[t].astype(F32)
        for s in range(1, 16):
            acc = acc + recv_ref[s * 4 + t].astype(F32)
        sums.append(acc)

    def vector(v):
        cuts = []
        for t in range(4):
            for j in range(4):
                r, c = 2 * j + v // 3, (v % 3) * 128
                cuts.append(sums[t][r : r + 1, c : c + 128])
        return jnp.concatenate(cuts, axis=1)

    hidden = (ng_ref[0:64, :] * (1.0 + vector(3)) + vector(1)).astype(BF16)
    kv_v[:, 0:256] = dot(hidden, wk_ref[...]).astype(BF16)
    kv_v[:, 256:512] = dot(hidden, wv_ref[...]).astype(BF16)
    copy = pltpu.make_async_copy
    outs = [copy(kv_v, send_ref.at[i], sems.at[i]) for i in range(16)]
    for c in outs:
        c.start()
    vec_v[...] = jnp.zeros((8, 2048), F32)
    vec_v[0:1, :] = ng_ref[64:65, :] * (1.0 + vector(2))
    vec_v[1:2, :] = vector(0)
    vec_v[2:3, :] = vector(4)
    outs.append(copy(vec_v, vec_ref, sems.at[16]))
    outs[16].start()
    for c in outs:
        c.wait()


def rotated(x, cos, sin, swap):
    return x.astype(F32) * cos + dot(x, swap) * sin


def paired(a, b, low):
    turned_a, turned_b = pltpu.roll(a, 64, 1), pltpu.roll(b, 64, 1)
    return jnp.where(low, a, turned_b).astype(BF16), jnp.where(low, turned_a, b).astype(BF16)


def split_pair(q, low):
    zero = jnp.zeros_like(q)
    return [jnp.where(low, q, zero), jnp.where(low, zero, q)]


def identity():
    return (iota((256, 256), 0) == iota((256, 256), 1)).astype(F32).astype(BF16)


def local_kernel(
    sink_ref, vec_ref, lat_ref, one_ref, two_ref, wq_ref, wk_ref, wv_ref,
    rowc_ref, rows_ref, colc_ref, cols_ref,
    q_ref, o_ref, l_ref, m_ref,
    vec_v, lat_v, wq_v, wk_v, wv_v, hid_v, rot_v, o_v, l_v, m_v, sems,
):
    place = place_of()
    odd = place & 1
    last = lax.axis_size("sp") * lax.axis_size("tp") - 1
    copy = pltpu.make_async_copy
    ins = [
        copy(vec_ref, vec_v, sems.at[0]),
        copy(lat_ref, lat_v.at[pl.ds(128, 256)], sems.at[1]),
        copy(one_ref, lat_v.at[pl.ds((1 - odd) * 384, 128)], sems.at[2]),
        copy(two_ref, lat_v.at[pl.ds(odd * 384, 128)], sems.at[3]),
        copy(wk_ref, wk_v, sems.at[4]),
        copy(wv_ref, wv_v, sems.at[5]),
    ]
    for h in range(4):
        cols = pl.ds(h * 256, 256)
        ins.append(copy(wq_ref.at[:, cols], wq_v.at[h], sems.at[6 + h]))
    for c in ins:
        c.start()
    swap = swap_matrix()
    cos = jnp.concatenate([colc_ref[...] + rowc_ref[r : r + 1, :] for r in range(8)], axis=0)
    sin = jnp.concatenate([cols_ref[...] + rows_ref[r : r + 1, :] for r in range(8)], axis=0)
    for c in ins[:4]:
        c.wait()
    mult, shift = vec_v[0:1, :], vec_v[1:2, :]
    for r in range(4):
        rows = slice(r * 128, r * 128 + 128)
        hid_v[rows, :] = normed(lat_v[rows, :], mult, shift)
    ins[4].wait()
    ins[5].wait()
    keys = rotated(dot(hid_v[...], wk_v[...]).astype(BF16), cos, sin, swap).astype(BF16)
    kt = dot_nt(identity(), keys).astype(BF16)
    vals = dot(hid_v[...], wv_v[...]).astype(BF16)
    ones = jnp.ones((512, 128), BF16)
    low_own = iota((256, 128), 1) < HEAD_DIM
    low = iota((128, 128), 1) < HEAD_DIM
    row, col = iota((128, 128), 0), iota((128, 128), 1)
    from_low = jnp.where(col >= row, 0.0, NEG_BIG)
    from_high = jnp.where(col <= row, 0.0, NEG_BIG)
    bias = (
        (from_low + jnp.where(place > 0, 0.0, NEG_BIG), from_high),
        (from_low, from_high + jnp.where(place < last, 0.0, NEG_BIG)),
    )
    outs = []
    for a in range(2):
        plain, turned = [], []
        for h in (2 * a, 2 * a + 1):
            ins[6 + h].wait()
            q = dot(hid_v[128:384, :], wq_v[h]).astype(BF16)
            plain.append(q.astype(F32))
            turned.append(rotated(q, cos[128:384], sin[128:384], swap))
        for p in range(2):
            piece = slice(p * 128, p * 128 + 128)
            at = a * 512 + p * 256
            for ref, x in ((q_ref, plain), (rot_v, turned)):
                one, two = paired(x[0][:, piece], x[1][:, piece], low_own)
                ref[:, at : at + 128] = one
                ref[:, at + 128 : at + 256] = two
        va = jnp.concatenate([vals[:, a * 128 : a * 128 + 128], ones], axis=1)
        for b in range(2):
            rows = slice(b * 128, b * 128 + 128)
            seen = slice(b * 128, b * 128 + 384)
            stacked = []
            for g in range(4):
                stacked += split_pair(rot_v[rows, a * 512 + g * 128 : a * 512 + g * 128 + 128], low)
            s = dot(jnp.concatenate(stacked, axis=0), kt[a * 128 : a * 128 + 128, seen])
            ps, ms = [], []
            for i in range(8):
                si = s[i * 128 : i * 128 + 128]
                s0, s1, s2 = si[:, 0:128] + bias[b][0], si[:, 128:256], si[:, 256:384] + bias[b][1]
                sink = sink_ref[(2 * a + i % 2) * 4 + i // 2] * LOG2E
                m = jnp.max(jnp.maximum(jnp.maximum(s0, s1), s2), axis=-1, keepdims=True)
                m = jnp.maximum(m * FACTOR, sink)
                p = [jnp.exp2(x * FACTOR - m).astype(BF16) for x in (s0, s1, s2)]
                ps.append(jnp.concatenate(p, axis=1))
                ms.append((jnp.broadcast_to(m, (128, 128)), sink))
            o = dot(jnp.concatenate(ps, axis=0), va[seen])
            for g in range(4):
                to = slice(a * 512 + g * 128, a * 512 + g * 128 + 128)
                x, y = o[g * 256 : g * 256 + 128], o[g * 256 + 128 : g * 256 + 256]
                (mx, sx), (my, sy) = ms[2 * g], ms[2 * g + 1]
                m = jnp.where(low, mx, my)
                o_v[rows, to] = jnp.where(low, x[:, 0:128], y[:, 0:128])
                l_v[rows, to] = jnp.where(low, x[:, 128:256], y[:, 128:256]) + jnp.exp2(
                    jnp.where(low, sx, sy) - m
                )
                m_v[rows, to] = m
        cols = pl.ds(a * 512, 512)
        for i, (src, dst) in enumerate(((o_v, o_ref), (l_v, l_ref), (m_v, m_ref))):
            outs.append(copy(src.at[:, cols], dst.at[:, cols], sems.at[10 + 3 * a + i]))
            outs[-1].start()
    for c in outs:
        c.wait()


def final_kernel(
    q_ref, kv_ref, o_ref, l_ref, m_ref, wo_ref, lat_ref, vec_ref, gain_ref, out_ref,
    o_v, l_v, m_v, wo_v, lat_v, vec_v, gain_v, mix_v, out_v, sems,
):
    copy = pltpu.make_async_copy
    pairs = [
        (o_ref, o_v), (l_ref, l_v), (m_ref, m_v), (lat_ref, lat_v), (vec_ref, vec_v), (gain_ref, gain_v),
    ]
    for a in range(2):
        for g in range(4):
            for i in range(2):
                head = (2 * a + i) * 4 + g
                to = ((a * 4 + g) * 2 + i) * HEAD_DIM
                pairs.append((wo_ref.at[pl.ds(head * 64, 64)], wo_v.at[pl.ds(to, 64)]))
    ins = [copy(src, dst, sems.at[i]) for i, (src, dst) in enumerate(pairs)]
    for c in ins:
        c.start()
    low = iota((256, 128), 1) < HEAD_DIM
    ones = jnp.ones((1024, 128), BF16)
    kt = dot_nt(identity(), kv_ref[:, 0:256]).astype(BF16)
    for a in range(2):
        va = jnp.concatenate([kv_ref[:, 256 + a * 128 : 384 + a * 128], ones], axis=1)
        for g in range(4):
            to = slice(a * 512 + g * 128, a * 512 + g * 128 + 128)
            stacked = jnp.concatenate(split_pair(q_ref[:, to], low), axis=0)
            s = dot(stacked, kt[a * 128 : a * 128 + 128, :])
            m = jnp.max(s, axis=-1, keepdims=True) * FACTOR
            o = dot(jnp.exp2(s * FACTOR - m).astype(BF16), va)
            m = jnp.broadcast_to(m, (512, 128))
            if a == 0 and g == 0:
                for c in ins[:3]:
                    c.wait()
            mc = jnp.where(low, m[0:256], m[256:512])
            oc = jnp.where(low, o[0:256, 0:128], o[256:512, 0:128])
            lc = jnp.where(low, o[0:256, 128:256], o[256:512, 128:256])
            ml = m_v[:, to]
            top = jnp.maximum(ml, mc)
            wl, wc = jnp.exp2(ml - top), jnp.exp2(mc - top)
            num = wl * o_v[:, to] + wc * oc
            den = wl * l_v[:, to] + wc * lc
            mix_v[:, to] = (num / den).astype(BF16)
    for c in ins[3:]:
        c.wait()
    scale = vec_v[2:3, :] * gain_v[...]
    outs = []
    for b in range(2):
        rows = slice(b * 128, b * 128 + 128)
        projected = dot(mix_v[rows, :], wo_v[...])
        rs = lax.rsqrt(jnp.mean(projected * projected, axis=-1, keepdims=True) + EPSILON)
        out_v[rows, :] = (lat_v[rows, :].astype(F32) + projected * rs * scale).astype(BF16)
        there = pl.ds(b * 128, 128)
        outs.append(copy(out_v.at[there], out_ref.at[there], sems.at[len(ins) + b]))
        outs[b].start()
    for c in outs:
        c.wait()


KINDS = {"v": VM, "V": VM, "h": HB, "s": SM}
FIXED = {"V": VM, "h": HB}


def spec(kinds):
    return [pl.BlockSpec(memory_space=KINDS[k]) for k in kinds]


def call(kernel, name, ins, outs, scratch, copies, args, flops, limit):
    return pl.pallas_call(
        kernel,
        out_shape=[FIXED.get(k, jax.ShapeDtypeStruct)(s, d) for k, s, d in outs],
        in_specs=spec(ins),
        out_specs=spec([k for k, _, _ in outs]),
        scratch_shapes=[pltpu.VMEM(s, d) for s, d in scratch]
        + [pltpu.SemaphoreType.DMA((copies,))],
        compiler_params=pltpu.CompilerParams(vmem_limit_bytes=limit * 1024 * 1024),
        cost_estimate=pl.CostEstimate(flops=flops, bytes_accessed=0, transcendentals=0),
        name=name,
    )(
        *[
            pltpu.with_memory_space_constraint(x, FIXED[k]) if k in FIXED else x
            for k, x in zip(ins, args)
        ]
    )


def shards(
    latent, cond, ctx_rows, ctx_cond, mod_weight, norm_gain, out_gain,
    w_query, w_key, w_value, w_out, sink,
):
    sp_size = lax.axis_size("sp")
    count = sp_size * lax.axis_size("tp")
    both = ("sp", "tp")
    rows, width = latent.shape
    half = (WINDOW, width)
    wide = (rows, 1024)
    rest = (8, width)
    line = (1, width)
    square = (16, 128)
    small = w_key.shape

    parts, one, two = call(
        entry_kernel,
        "entry",
        "hhhh",
        [("h", (count, 8, 384), BF16), ("h", half, BF16), ("h", half, BF16)],
        [
            (square, BF16),
            (square, BF16),
            (mod_weight.shape, BF16),
            (latent.shape, BF16),
            ((count, 8, 384), BF16),
        ],
        7,
        (cond.reshape(square), ctx_cond.reshape(square), mod_weight, latent),
        10**6,
        8,
    )
    ng, wk_near, wv_near = call(
        prep_kernel,
        "prep",
        "hhhhh",
        [("V", (72, width), F32), ("V", small, BF16), ("V", small, BF16)],
        [(ctx_rows.shape, BF16), (line, F32)],
        4,
        (one, ctx_rows, norm_gain.reshape(line), w_key, w_value),
        2 * 10**9,
        4,
    )
    recv = lax.all_to_all(parts, both, 0, 0, tiled=True)
    swap_one = [(i, i ^ 1) for i in range(count)]
    swap_two = [(i, i + 1 if i % 2 else i - 1) for i in range(1, count - 1)]
    one = lax.ppermute(one, both, swap_one)
    two = lax.ppermute(two, both, swap_two)
    send, vecs = call(
        context_kernel,
        "context",
        "vVVV",
        [("h", (sp_size, 64, 512), BF16), ("h", rest, F32)],
        [((64, 512), BF16), (rest, F32)],
        17,
        (recv, ng, wk_near, wv_near),
        10**6,
        6,
    )
    kv_ctx = lax.all_to_all(send, "sp", 0, 0, tiled=True).reshape(sp_size * 64, 512)

    lanes = np.arange(256) % 32
    freq = 10000.0 ** (-(lanes % 16) / 16.0)
    by_row = (lanes < 16).astype(np.float32)
    angle = np.arange(GRID_W)[:, None] * freq
    colc = jnp.asarray(np.cos(angle) * (1.0 - by_row), F32)
    cols = jnp.asarray(np.sin(angle) * (1.0 - by_row), F32)
    grid_row = place_of() * (rows // GRID_W) - WINDOW // GRID_W + jnp.arange(8, dtype=jnp.int32)
    angle = grid_row.astype(F32)[:, None] * jnp.asarray(freq, F32)[None, :]
    tables = (jnp.cos(angle) * by_row, jnp.sin(angle) * by_row, colc, cols)

    query, o, l, m = call(
        local_kernel,
        "local",
        "shhhhhhhvvvv",
        [("V", wide, BF16), ("h", wide, F32), ("h", wide, F32), ("h", wide, F32)],
        [
            (rest, F32),
            ((2 * rows, width), BF16),
            ((4, width, 256), BF16),
            (small, BF16),
            (small, BF16),
            ((2 * rows, width), BF16),
            (wide, BF16),
            (wide, F32),
            (wide, F32),
            (wide, F32),
        ],
        16,
        (sink, vecs, latent, one, two, w_query, w_key, w_value, *tables),
        10**10,
        26,
    )
    (updated,) = call(
        final_kernel,
        "final",
        "VVhhhhhhh",
        [("h", latent.shape, BF16)],
        [
            (wide, F32),
            (wide, F32),
            (wide, F32),
            (w_out.shape, BF16),
            (latent.shape, BF16),
            (rest, F32),
            (line, F32),
            (wide, BF16),
            (latent.shape, BF16),
        ],
        24,
        (query, kv_ctx, o, l, m, w_out, latent, vecs, out_gain.reshape(line)),
        10**10,
        28,
    )
    return updated


def solution(mesh):
    placed = (
        P(("dp", "sp", "tp"), None),
        P("dp"),
        P(("dp", "sp"), None),
        P(),
        P(None, "sp", "tp"),
        P(),
        P(),
        P(),
        P(),
        P(),
        P(),
        P(),
    )
    return jax.shard_map(
        shards, mesh=mesh, in_specs=placed, out_specs=P(("dp", "sp", "tp"), None), check_vma=False
    )
```

time: 67.1 us -> 59.6 us (0.89)
  local copies, waits for them, and re-layouts: 4.43 us -> 0.03 us
  starting transfers between devices: 17.7 us -> 20.9 us
  Pallas kernels: 33.3 us -> 30.1 us
  waiting for transfers between devices: 10.2 us -> 7.74 us
  other arithmetic: 0.82 us -> 0.12 us
    all_to_all x1, waiting for transfers between devices: 10.1 us -> 5.21 us  [shards(): recv = lax.all_to_all(parts, both, 0, 0, tiled=True)]
    unnamed x16 -> x10, local copies, waits for them, and re-layouts: 4.43 us -> 0.03 us
    pallas_call x5, Pallas kernels: 33.3 us -> 30.1 us  [call(): pl.pallas_call(kernel, out_shape=[FIXED.get(k, jax.ShapeDtypeStruct)(s, d...]
    all_to_all x1, waiting for transfers between devices: 0.01 us -> 2.53 us  [shards(): lax.all_to_all(send, 'sp', 0, 0, tiled=True).reshape(sp_size * 64, 512)]
    ppermute x1, starting transfers between devices: 1.65 us -> 3.57 us  [shards(): one = lax.ppermute(one, both, swap_one)]
    ppermute x1, starting transfers between devices: 0.68 us -> 1.46 us  [shards(): two = lax.ppermute(two, both, swap_two)]
    mul x1, other arithmetic: 0.82 us -> 0.12 us  [shards(): tables = (jnp.cos(angle) * by_row, jnp.sin(angle) * by_row, colc, cols)]
  transfers between devices with their start and end apart: 4 -> 4, of which waited for: 1 -> 2; matrix products, arithmetic and copies ran while one was open for 1% -> 0% of each run, Pallas kernels for 29% -> 29%
where the time goes in v4:
time: 59.6 us; the launch traced here: 59.3 us
  Pallas kernels  30.1 us (51%)
  starting transfers between devices  20.9 us (35%)
  waiting for transfers between devices  7.74 us (13%)
    pallas_call x5, Pallas kernels, call(): pl.pallas_call(kernel, out_shape=[FIXED.get(k, jax.ShapeDtypeStruct)(s, d...  30.1 us
    all_to_all x1, starting transfers between devices, shards(): recv = lax.all_to_all(parts, both, 0, 0, tiled=True)  11.5 us
    all_to_all x1, waiting for transfers between devices, shards(): recv = lax.all_to_all(parts, both, 0, 0, tiled=True)  5.21 us
    all_to_all x1, starting transfers between devices, shards(): lax.all_to_all(send, 'sp', 0, 0, tiled=True).reshape(sp_size * 64, 512)  4.34 us
    ppermute x1, starting transfers between devices, shards(): one = lax.ppermute(one, both, swap_one)  3.57 us
    all_to_all x1, waiting for transfers between devices, shards(): lax.all_to_all(send, 'sp', 0, 0, tiled=True).reshape(sp_size * 64, 512)  2.53 us
    ppermute x1, starting transfers between devices, shards(): two = lax.ppermute(two, both, swap_two)  1.46 us
  transfers between devices with their start and end apart: 4, of which 2 were waited for; matrix products, arithmetic and copies ran while one was open for 0% of the time, Pallas kernels for 29%

profile of v4, /device:TPU:0, one launch (start us, length us, event | category | flops | bytes accessed | tf_op | source)
XLA Modules:
  0.0 59.3 jit_solution(7823990785922608659)
XLA Ops:
  0.0 2.4 %entry.1 = (bf16[64,8,384]{2,1,0:T(8,128)(2,1)}, bf16[128,2048]{1,0:T(8,128)(2,1)}, bf16[128,2048]{1,0:T(8,128)(2,1)}) custom-call(bf16[16,128]{1,0:T(8,128)(2,1)} %bitcast.6, bf16[16,128]{1,0:T(8,128)(2,1)} %bitcast.7, bf16[3,128,512]{2,1,0:T(8,128)(2,1)} %mod_ref.1, bf16[256,2048]{1,0:T(8,128)(2,1)} %lat_ref.5), custom_call_target="tpu_custom_call" | custom-call | flops 1000000 | tf_op jit(solution)/shard_map/entry/pallas_call | solution.py:331
  2.4 11.5 %all-to-all-start = ((bf16[64,8,384]{2,1,0:T(8,128)(2,1)}), bf16[64,8,384]{2,1,0:T(8,128)(2,1)S(1)}, u32[]{:S(2)}, u32[]{:S(2)}) async-start(bf16[64,8,384]{2,1,0:T(8,128)(2,1)} %get-tuple-element.17), calls=%async_computation | async-start | bytes 786432 | tf_op jit(solution)/shard_map/all_to_all | solution.py:392
  14.0 1.5 %collective-permute-start.1 = (bf16[128,2048]{1,0:T(8,128)(2,1)}, bf16[128,2048]{1,0:T(8,128)(2,1)}, u32[]{:S(2)}, u32[]{:S(2)}) collective-permute-start(bf16[128,2048]{1,0:T(8,128)(2,1)} %get-tuple-element.23), channel_id=1, source_target_pairs={{2,4},{4,2},{6,8},{8,6},{10,12},{12,10},{14,16},{16,14},{18,20},{2... | collective-permute-start | bytes 1572872 | tf_op jit(solution)/shard_map/ppermute | solution.py:396
  15.4 3.6 %collective-permute-start = (bf16[128,2048]{1,0:T(8,128)(2,1)}, bf16[128,2048]{1,0:T(8,128)(2,1)}, u32[]{:S(2)}, u32[]{:S(2)}) collective-permute-start(bf16[128,2048]{1,0:T(8,128)(2,1)} %get-tuple-element.18.after_ref), channel_id=1, source_target_pairs={{0,2},{2,0},{4,6},{6,4},{8,10},{10,8},{12,14},{14,12},{16,18},{18,... | collective-permute-start | bytes 1572872 | tf_op jit(solution)/shard_map/ppermute | solution.py:395
  19.0 1.7 %prep.1 = (f32[72,2048]{1,0:T(8,128)S(1)}, bf16[2048,256]{1,0:T(8,128)(2,1)S(1)}, bf16[2048,256]{1,0:T(8,128)(2,1)S(1)}) custom-call(bf16[128,2048]{1,0:T(8,128)(2,1)} %get-tuple-element.18.after_ref, bf16[64,2048]{1,0:T(8,128)(2,1)} %ctx_ref.1, f32[1,2048]{1,0:T(1,128)} %bitcast.8, bf16[2048,256]{1,0:T(8,128)(2,1)} %wk_ref.3, bf16[2048,256]{1,0:T(8,128)(2,1)} %wv_ref.3), custom_call_target="tpu_custom_call" | custom-call | flops 2000000000 | tf_op jit(solution)/shard_map/prep/pallas_call | solution.py:331
  20.7 0.0 copy-start.3
  20.7 0.0 copy-start.4
  20.7 0.0 copy-start
  20.7 0.0 copy-start.1
  20.7 0.0 copy-start.2
  20.8 5.2 %all-to-all-done.recv_ref = bf16[64,8,384]{2,1,0:T(8,128)(2,1)S(1)} async-done(((bf16[64,8,384]{2,1,0:T(8,128)(2,1)}), bf16[64,8,384]{2,1,0:T(8,128)(2,1)S(1)}, u32[]{:S(2)}, u32[]{:S(2)}) %all-to-all-start) | async-done | bytes 393248 | tf_op jit(solution)/shard_map/all_to_all | solution.py:392
  26.0 1.6 %context.1 = (bf16[16,64,512]{2,1,0:T(8,128)(2,1)}, f32[8,2048]{1,0:T(8,128)}) custom-call(bf16[64,8,384]{2,1,0:T(8,128)(2,1)S(1)} %all-to-all-done.recv_ref, f32[72,2048]{1,0:T(8,128)S(1)} %get-tuple-element.19.ng_ref, bf16[2048,256]{1,0:T(8,128)(2,1)S(1)} %get-tuple-element.20.wk_ref, bf16[2048,256]{1,0:T(8,128)(2,1)S(1)} %get-tuple-element.21.wv_ref), custom_call_target="tpu_custom_call" | custom-call | flops 1000000 | tf_op jit(solution)/shard_map/context/pallas_call | solution.py:331
  27.6 4.3 %all-to-all-start.1 = ((bf16[16,64,512]{2,1,0:T(8,128)(2,1)}), bf16[16,64,512]{2,1,0:T(8,128)(2,1)S(1)}, u32[]{:S(2)}, u32[]{:S(2)}) async-start(bf16[16,64,512]{2,1,0:T(8,128)(2,1)} %get-tuple-element.25), calls=%async_computation.1 | async-start | bytes 2097152 | tf_op jit(solution)/shard_map/all_to_all | solution.py:408
  31.9 0.0 copy-done.3
  31.9 0.0 copy-done.4
  31.9 0.1 fusion.1
  32.1 0.0 collective-permute-done.1.two_ref
  32.1 0.0 collective-permute-done.one_ref
  32.1 0.0 copy-done
  32.1 0.0 copy-done.1
  32.1 0.0 copy-done.2
  32.1 14.0 %local.1 = (bf16[256,1024]{1,0:T(8,128)(2,1)S(1)}, f32[256,1024]{1,0:T(8,128)}, f32[256,1024]{1,0:T(8,128)}, f32[256,1024]{1,0:T(8,128)}) custom-call(f32[16]{0:T(128)S(1)} %copy-done, f32[8,2048]{1,0:T(8,128)} %get-tuple-element.22.vec_ref, bf16[256,2048]{1,0:T(8,128)(2,1)} %lat_ref.5, bf16[128,2048]{1,0:T(8,128)(2,1)} %collective-permute-done.one_ref, ...), custom_call_target="tpu_custom_call" | custom-call | flops 10000000000 | tf_op jit(solution)/shard_map/local/pallas_call | solution.py:331
  46.1 2.5 %all-to-all-done.1 = bf16[16,64,512]{2,1,0:T(8,128)(2,1)S(1)} async-done(((bf16[16,64,512]{2,1,0:T(8,128)(2,1)}), bf16[16,64,512]{2,1,0:T(8,128)(2,1)S(1)}, u32[]{:S(2)}, u32[]{:S(2)}) %all-to-all-start.1) | async-done | bytes 1048608 | tf_op jit(solution)/shard_map/all_to_all | solution.py:408
  48.6 10.4 %final.1 = bf16[256,2048]{1,0:T(8,128)(2,1)} custom-call(bf16[256,1024]{1,0:T(8,128)(2,1)S(1)} %get-tuple-element.24.q_ref, bf16[1024,512]{1,0:T(8,128)(2,1)S(1)} %bitcast.5, f32[256,1024]{1,0:T(8,128)} %get-tuple-element.26.o_ref, f32[256,1024]{1,0:T(8,128)} %get-tuple-element.27.l_ref, f32[256,1024]{1,0:T(8,128)} %get-tuple-element.28.m_ref, ...), custom_call_target="tpu_custom_call" | custom-call | flops 10000000000 | tf_op jit(solution)/shard_map/final/pallas_call | solution.py:331
  (1 shorter events, 0.0 us)
Async XLA Ops:
  2.4 23.5 %all-to-all-start = ((bf16[64,8,384]{2,1,0:T(8,128)(2,1)}), bf16[64,8,384]{2,1,0:T(8,128)(2,1)S(1)}, u32[]{:S(2)}, u32[]{:S(2)}) async-start(bf16[64,8,384]{2,1,0:T(8,128)(2,1)} %get-tuple-element.17), calls=%async_computation | async-start | bytes 786432 | tf_op jit(solution)/shard_map/all_to_all | solution.py:392
  14.0 18.1 %collective-permute-start.1 = (bf16[128,2048]{1,0:T(8,128)(2,1)}, bf16[128,2048]{1,0:T(8,128)(2,1)}, u32[]{:S(2)}, u32[]{:S(2)}) collective-permute-start(bf16[128,2048]{1,0:T(8,128)(2,1)} %get-tuple-element.23), channel_id=1, source_target_pairs={{2,4},{4,2},{6,8},{8,6},{10,12},{12,10},{14,16},{16,14},{18,20},{2... | collective-permute-start | bytes 1572872 | tf_op jit(solution)/shard_map/ppermute | solution.py:396
  15.4 16.6 %collective-permute-start = (bf16[128,2048]{1,0:T(8,128)(2,1)}, bf16[128,2048]{1,0:T(8,128)(2,1)}, u32[]{:S(2)}, u32[]{:S(2)}) collective-permute-start(bf16[128,2048]{1,0:T(8,128)(2,1)} %get-tuple-element.18.after_ref), channel_id=1, source_target_pairs={{0,2},{2,0},{4,6},{6,4},{8,10},{10,8},{12,14},{14,12},{16,18},{18,... | collective-permute-start | bytes 1572872 | tf_op jit(solution)/shard_map/ppermute | solution.py:395
  20.7 11.2 %copy-start.3 = (f32[256]{0:T(256)S(1)}, f32[256]{0:T(256)}, u32[]{:S(2)}) copy-start(f32[256]{0:T(256)} %constant.27.clone) | copy-start | bytes 3076
  20.7 11.2 %copy-start.4 = (f32[256]{0:T(256)S(1)}, f32[256]{0:T(256)}, u32[]{:S(2)}) copy-start(f32[256]{0:T(256)} %constant.26.clone) | copy-start | bytes 3076
  20.7 11.4 %copy-start = (f32[16]{0:T(128)S(1)}, f32[16]{0:T(128)}, u32[]{:S(2)}) copy-start(f32[16]{0:T(128)} %sink_ref.1) | copy-start | bytes 196
  20.7 11.4 %copy-start.1 = (f32[64,256]{1,0:T(8,128)S(1)}, f32[64,256]{1,0:T(8,128)}, u32[]{:S(2)}) copy-start(f32[64,256]{1,0:T(8,128)} %constant.25.clone.cols_ref) | copy-start | bytes 196612
  20.7 11.4 %copy-start.2 = (f32[64,256]{1,0:T(8,128)S(1)}, f32[64,256]{1,0:T(8,128)}, u32[]{:S(2)}) copy-start(f32[64,256]{1,0:T(8,128)} %constant.24.clone.colc_ref) | copy-start | bytes 196612
  27.6 21.1 %all-to-all-start.1 = ((bf16[16,64,512]{2,1,0:T(8,128)(2,1)}), bf16[16,64,512]{2,1,0:T(8,128)(2,1)S(1)}, u32[]{:S(2)}, u32[]{:S(2)}) async-start(bf16[16,64,512]{2,1,0:T(8,128)(2,1)} %get-tuple-element.25), calls=%async_computation.1 | async-start | bytes 2097152 | tf_op jit(solution)/shard_map/all_to_all | solution.py:408

commit v5 on v4

--- a/solution.py
+++ b/solution.py
@@ -167,39 +167,49 @@
     sink_ref, vec_ref, lat_ref, one_ref, two_ref, wq_ref, wk_ref, wv_ref,
     rowc_ref, rows_ref, colc_ref, cols_ref,
     q_ref, o_ref, l_ref, m_ref,
-    vec_v, lat_v, wq_v, wk_v, wv_v, hid_v, rot_v, o_v, l_v, m_v, sems,
+    vec_v, lat_v, wq_v, wkv_v, hid_v, o_v, l_v, m_v, sems,
 ):
     place = place_of()
     odd = place & 1
     last = lax.axis_size("sp") * lax.axis_size("tp") - 1
     copy = pltpu.make_async_copy
-    ins = [
+    own = [
         copy(vec_ref, vec_v, sems.at[0]),
         copy(lat_ref, lat_v.at[pl.ds(128, 256)], sems.at[1]),
+    ]
+    halo = [
         copy(one_ref, lat_v.at[pl.ds((1 - odd) * 384, 128)], sems.at[2]),
         copy(two_ref, lat_v.at[pl.ds(odd * 384, 128)], sems.at[3]),
-        copy(wk_ref, wk_v, sems.at[4]),
-        copy(wv_ref, wv_v, sems.at[5]),
     ]
-    for h in range(4):
-        cols = pl.ds(h * 256, 256)
-        ins.append(copy(wq_ref.at[:, cols], wq_v.at[h], sems.at[6 + h]))
-    for c in ins:
+    weights = [
+        copy(wk_ref, wkv_v.at[:, pl.ds(0, 256)], sems.at[4]),
+        copy(wv_ref, wkv_v.at[:, pl.ds(256, 256)], sems.at[5]),
+        copy(wq_ref.at[:, pl.ds(0, 512)], wq_v.at[0], sems.at[6]),
+        copy(wq_ref.at[:, pl.ds(512, 512)], wq_v.at[1], sems.at[7]),
+    ]
+    for c in own + halo:
         c.start()
     swap = swap_matrix()
     cos = jnp.concatenate([colc_ref[...] + rowc_ref[r : r + 1, :] for r in range(8)], axis=0)
     sin = jnp.concatenate([cols_ref[...] + rows_ref[r : r + 1, :] for r in range(8)], axis=0)
-    for c in ins[:4]:
-        c.wait()
+    for c in own:
+        c.wait()
+    for c in weights:
+        c.start()
     mult, shift = vec_v[0:1, :], vec_v[1:2, :]
-    for r in range(4):
+    for r in (1, 2):
         rows = slice(r * 128, r * 128 + 128)
         hid_v[rows, :] = normed(lat_v[rows, :], mult, shift)
-    ins[4].wait()
-    ins[5].wait()
-    keys = rotated(dot(hid_v[...], wk_v[...]).astype(BF16), cos, sin, swap).astype(BF16)
+    for c in halo:
+        c.wait()
+    for r in (0, 3):
+        rows = slice(r * 128, r * 128 + 128)
+        hid_v[rows, :] = normed(lat_v[rows, :], mult, shift)
+    for c in weights:
+        c.wait()
+    kv = dot(hid_v[...], wkv_v[...]).astype(BF16)
+    keys = rotated(kv[:, 0:256], cos, sin, swap).astype(BF16)
     kt = dot_nt(identity(), keys).astype(BF16)
-    vals = dot(hid_v[...], wv_v[...]).astype(BF16)
     ones = jnp.ones((512, 128), BF16)
     low_own = iota((256, 128), 1) < HEAD_DIM
     low = iota((128, 128), 1) < HEAD_DIM
@@ -210,28 +220,29 @@
         (from_low + jnp.where(place > 0, 0.0, NEG_BIG), from_high),
         (from_low, from_high + jnp.where(place < last, 0.0, NEG_BIG)),
     )
-    outs = []
+    slabs = []
     for a in range(2):
+        q = dot(hid_v[128:384, :], wq_v[a]).astype(BF16)
         plain, turned = [], []
-        for h in (2 * a, 2 * a + 1):
-            ins[6 + h].wait()
-            q = dot(hid_v[128:384, :], wq_v[h]).astype(BF16)
-            plain.append(q.astype(F32))
-            turned.append(rotated(q, cos[128:384], sin[128:384], swap))
+        for h in range(2):
+            part = q[:, h * 256 : h * 256 + 256]
+            plain.append(part.astype(F32))
+            turned.append(rotated(part, cos[128:384], sin[128:384], swap))
         for p in range(2):
             piece = slice(p * 128, p * 128 + 128)
             at = a * 512 + p * 256
-            for ref, x in ((q_ref, plain), (rot_v, turned)):
-                one, two = paired(x[0][:, piece], x[1][:, piece], low_own)
-                ref[:, at : at + 128] = one
-                ref[:, at + 128 : at + 256] = two
-        va = jnp.concatenate([vals[:, a * 128 : a * 128 + 128], ones], axis=1)
+            one, two = paired(plain[0][:, piece], plain[1][:, piece], low_own)
+            q_ref[:, at : at + 128] = one
+            q_ref[:, at + 128 : at + 256] = two
+            slabs += paired(turned[0][:, piece], turned[1][:, piece], low_own)
+    for a in range(2):
+        va = jnp.concatenate([kv[:, 256 + a * 128 : 384 + a * 128], ones], axis=1)
         for b in range(2):
             rows = slice(b * 128, b * 128 + 128)
             seen = slice(b * 128, b * 128 + 384)
             stacked = []
             for g in range(4):
-                stacked += split_pair(rot_v[rows, a * 512 + g * 128 : a * 512 + g * 128 + 128], low)
+                stacked += split_pair(slabs[a * 4 + g][rows], low)
             s = dot(jnp.concatenate(stacked, axis=0), kt[a * 128 : a * 128 + 128, seen])
             ps, ms = [], []
             for i in range(8):
@@ -254,17 +265,19 @@
                     jnp.where(low, sx, sy) - m
                 )
                 m_v[rows, to] = m
-        cols = pl.ds(a * 512, 512)
-        for i, (src, dst) in enumerate(((o_v, o_ref), (l_v, l_ref), (m_v, m_ref))):
-            outs.append(copy(src.at[:, cols], dst.at[:, cols], sems.at[10 + 3 * a + i]))
-            outs[-1].start()
+    outs = [
+        copy(src, dst, sems.at[8 + i])
+        for i, (src, dst) in enumerate(((o_v, o_ref), (l_v, l_ref), (m_v, m_ref)))
+    ]
+    for c in outs:
+        c.start()
     for c in outs:
         c.wait()
 
 
 def final_kernel(
     q_ref, kv_ref, o_ref, l_ref, m_ref, wo_ref, lat_ref, vec_ref, gain_ref, out_ref,
-    o_v, l_v, m_v, wo_v, lat_v, vec_v, gain_v, mix_v, out_v, sems,
+    o_v, l_v, m_v, wo_v, lat_v, vec_v, gain_v, oc_v, lc_v, mc_v, out_v, sems,
 ):
     copy = pltpu.make_async_copy
     pairs = [
@@ -282,34 +295,39 @@
     low = iota((256, 128), 1) < HEAD_DIM
     ones = jnp.ones((1024, 128), BF16)
     kt = dot_nt(identity(), kv_ref[:, 0:256]).astype(BF16)
-    for a in range(2):
+    slabs = [slice(i * 128, i * 128 + 128) for i in range(8)]
+
+    def scores(i):
+        stacked = jnp.concatenate(split_pair(q_ref[:, slabs[i]], low), axis=0)
+        return dot(stacked, kt[(i // 4) * 128 : (i // 4) * 128 + 128, :])
+
+    s = scores(0)
+    for i in range(8):
+        coming = scores(i + 1) if i < 7 else None
+        a = i // 4
         va = jnp.concatenate([kv_ref[:, 256 + a * 128 : 384 + a * 128], ones], axis=1)
-        for g in range(4):
-            to = slice(a * 512 + g * 128, a * 512 + g * 128 + 128)
-            stacked = jnp.concatenate(split_pair(q_ref[:, to], low), axis=0)
-            s = dot(stacked, kt[a * 128 : a * 128 + 128, :])
-            m = jnp.max(s, axis=-1, keepdims=True) * FACTOR
-            o = dot(jnp.exp2(s * FACTOR - m).astype(BF16), va)
-            m = jnp.broadcast_to(m, (512, 128))
-            if a == 0 and g == 0:
-                for c in ins[:3]:
-                    c.wait()
-            mc = jnp.where(low, m[0:256], m[256:512])
-            oc = jnp.where(low, o[0:256, 0:128], o[256:512, 0:128])
-            lc = jnp.where(low, o[0:256, 128:256], o[256:512, 128:256])
-            ml = m_v[:, to]
-            top = jnp.maximum(ml, mc)
-            wl, wc = jnp.exp2(ml - top), jnp.exp2(mc - top)
-            num = wl * o_v[:, to] + wc * oc
-            den = wl * l_v[:, to] + wc * lc
-            mix_v[:, to] = (num / den).astype(BF16)
-    for c in ins[3:]:
+        m = jnp.max(s, axis=-1, keepdims=True) * FACTOR
+        o = dot(jnp.exp2(s * FACTOR - m).astype(BF16), va)
+        m = jnp.broadcast_to(m, (512, 128))
+        mc_v[:, slabs[i]] = jnp.where(low, m[0:256], m[256:512])
+        oc_v[:, slabs[i]] = jnp.where(low, o[0:256, 0:128], o[256:512, 0:128])
+        lc_v[:, slabs[i]] = jnp.where(low, o[0:256, 128:256], o[256:512, 128:256])
+        s = coming
+    for c in ins:
         c.wait()
     scale = vec_v[2:3, :] * gain_v[...]
     outs = []
     for b in range(2):
         rows = slice(b * 128, b * 128 + 128)
-        projected = dot(mix_v[rows, :], wo_v[...])
+        mixed = []
+        for to in slabs:
+            ml, mc = m_v[rows, to], mc_v[rows, to]
+            top = jnp.maximum(ml, mc)
+            wl, wc = jnp.exp2(ml - top), jnp.exp2(mc - top)
+            num = wl * o_v[rows, to] + wc * oc_v[rows, to]
+            den = wl * l_v[rows, to] + wc * lc_v[rows, to]
+            mixed.append((num / den).astype(BF16))
+        projected = dot(jnp.concatenate(mixed, axis=1), wo_v[...])
         rs = lax.rsqrt(jnp.mean(projected * projected, axis=-1, keepdims=True) + EPSILON)
         out_v[rows, :] = (lat_v[rows, :].astype(F32) + projected * rs * scale).astype(BF16)
         there = pl.ds(b * 128, 128)
@@ -425,16 +443,14 @@
         [
             (rest, F32),
             ((2 * rows, width), BF16),
-            ((4, width, 256), BF16),
-            (small, BF16),
-            (small, BF16),
+            ((2, width, 512), BF16),
+            ((width, 512), BF16),
             ((2 * rows, width), BF16),
-            (wide, BF16),
             (wide, F32),
             (wide, F32),
             (wide, F32),
         ],
-        16,
+        11,
         (sink, vecs, latent, one, two, w_query, w_key, w_value, *tables),
         10**10,
         26,
@@ -452,7 +468,9 @@
             (latent.shape, BF16),
             (rest, F32),
             (line, F32),
-            (wide, BF16),
+            (wide, F32),
+            (wide, F32),
+            (wide, F32),
             (latent.shape, BF16),
         ],
         24,

time: 59.6 us -> 61 us (1.023)
  waiting for transfers between devices: 7.74 us -> 9.51 us
    all_to_all x1, waiting for transfers between devices: 2.53 us -> 4.29 us  [shards(): lax.all_to_all(send, 'sp', 0, 0, tiled=True).reshape(sp_size * 64, 512)]
  transfers between devices with their start and end apart: 4 -> 4, of which waited for: 2 -> 2; matrix products, arithmetic and copies ran while one was open for 0% -> 0% of each run, Pallas kernels for 29% -> 26%
where the time goes in v5:
time: 61 us; the launch traced here: 60.6 us
  Pallas kernels  29.7 us (49%)
  starting transfers between devices  20.9 us (34%)
  waiting for transfers between devices  9.51 us (16%)
    pallas_call x5, Pallas kernels, call(): pl.pallas_call(kernel, out_shape=[FIXED.get(k, jax.ShapeDtypeStruct)(s, d...  29.7 us
    all_to_all x1, starting transfers between devices, shards(): recv = lax.all_to_all(parts, both, 0, 0, tiled=True)  11.5 us
    all_to_all x1, waiting for transfers between devices, shards(): recv = lax.all_to_all(parts, both, 0, 0, tiled=True)  5.21 us
    all_to_all x1, starting transfers between devices, shards(): lax.all_to_all(send, 'sp', 0, 0, tiled=True).reshape(sp_size * 64, 512)  4.34 us
    all_to_all x1, waiting for transfers between devices, shards(): lax.all_to_all(send, 'sp', 0, 0, tiled=True).reshape(sp_size * 64, 512)  4.29 us
    ppermute x1, starting transfers between devices, shards(): one = lax.ppermute(one, both, swap_one)  3.57 us
    ppermute x1, starting transfers between devices, shards(): two = lax.ppermute(two, both, swap_two)  1.46 us
  transfers between devices with their start and end apart: 4, of which 2 were waited for; matrix products, arithmetic and copies ran while one was open for 0% of the time, Pallas kernels for 26%

profile of v5, /device:TPU:0, one launch (start us, length us, event | category | flops | bytes accessed | tf_op | source)
XLA Modules:
  0.0 60.6 jit_solution(12762761118671946366)
XLA Ops:
  0.0 2.4 %entry.1 = (bf16[64,8,384]{2,1,0:T(8,128)(2,1)}, bf16[128,2048]{1,0:T(8,128)(2,1)}, bf16[128,2048]{1,0:T(8,128)(2,1)}) custom-call(bf16[16,128]{1,0:T(8,128)(2,1)} %bitcast.6, bf16[16,128]{1,0:T(8,128)(2,1)} %bitcast.7, bf16[3,128,512]{2,1,0:T(8,128)(2,1)} %mod_ref.1, bf16[256,2048]{1,0:T(8,128)(2,1)} %lat_ref.5), custom_call_target="tpu_custom_call" | custom-call | flops 1000000 | tf_op jit(solution)/shard_map/entry/pallas_call | solution.py:349
  2.4 11.5 %all-to-all-start = ((bf16[64,8,384]{2,1,0:T(8,128)(2,1)}), bf16[64,8,384]{2,1,0:T(8,128)(2,1)S(1)}, u32[]{:S(2)}, u32[]{:S(2)}) async-start(bf16[64,8,384]{2,1,0:T(8,128)(2,1)} %get-tuple-element.17), calls=%async_computation | async-start | bytes 786432 | tf_op jit(solution)/shard_map/all_to_all | solution.py:410
  14.0 1.5 %collective-permute-start.1 = (bf16[128,2048]{1,0:T(8,128)(2,1)}, bf16[128,2048]{1,0:T(8,128)(2,1)}, u32[]{:S(2)}, u32[]{:S(2)}) collective-permute-start(bf16[128,2048]{1,0:T(8,128)(2,1)} %get-tuple-element.23), channel_id=1, source_target_pairs={{2,4},{4,2},{6,8},{8,6},{10,12},{12,10},{14,16},{16,14},{18,20},{2... | collective-permute-start | bytes 1572872 | tf_op jit(solution)/shard_map/ppermute | solution.py:414
  15.4 3.6 %collective-permute-start = (bf16[128,2048]{1,0:T(8,128)(2,1)}, bf16[128,2048]{1,0:T(8,128)(2,1)}, u32[]{:S(2)}, u32[]{:S(2)}) collective-permute-start(bf16[128,2048]{1,0:T(8,128)(2,1)} %get-tuple-element.18.after_ref), channel_id=1, source_target_pairs={{0,2},{2,0},{4,6},{6,4},{8,10},{10,8},{12,14},{14,12},{16,18},{18,... | collective-permute-start | bytes 1572872 | tf_op jit(solution)/shard_map/ppermute | solution.py:413
  19.0 1.7 %prep.1 = (f32[72,2048]{1,0:T(8,128)S(1)}, bf16[2048,256]{1,0:T(8,128)(2,1)S(1)}, bf16[2048,256]{1,0:T(8,128)(2,1)S(1)}) custom-call(bf16[128,2048]{1,0:T(8,128)(2,1)} %get-tuple-element.18.after_ref, bf16[64,2048]{1,0:T(8,128)(2,1)} %ctx_ref.1, f32[1,2048]{1,0:T(1,128)} %bitcast.8, bf16[2048,256]{1,0:T(8,128)(2,1)} %wk_ref.3, bf16[2048,256]{1,0:T(8,128)(2,1)} %wv_ref.3), custom_call_target="tpu_custom_call" | custom-call | flops 2000000000 | tf_op jit(solution)/shard_map/prep/pallas_call | solution.py:349
  20.7 0.0 copy-start.3
  20.7 0.0 copy-start.4
  20.7 0.0 copy-start
  20.7 0.0 copy-start.1
  20.7 0.0 copy-start.2
  20.8 5.2 %all-to-all-done.recv_ref = bf16[64,8,384]{2,1,0:T(8,128)(2,1)S(1)} async-done(((bf16[64,8,384]{2,1,0:T(8,128)(2,1)}), bf16[64,8,384]{2,1,0:T(8,128)(2,1)S(1)}, u32[]{:S(2)}, u32[]{:S(2)}) %all-to-all-start) | async-done | bytes 393248 | tf_op jit(solution)/shard_map/all_to_all | solution.py:410
  26.0 1.6 %context.1 = (bf16[16,64,512]{2,1,0:T(8,128)(2,1)}, f32[8,2048]{1,0:T(8,128)}) custom-call(bf16[64,8,384]{2,1,0:T(8,128)(2,1)S(1)} %all-to-all-done.recv_ref, f32[72,2048]{1,0:T(8,128)S(1)} %get-tuple-element.19.ng_ref, bf16[2048,256]{1,0:T(8,128)(2,1)S(1)} %get-tuple-element.20.wk_ref, bf16[2048,256]{1,0:T(8,128)(2,1)S(1)} %get-tuple-element.21.wv_ref), custom_call_target="tpu_custom_call" | custom-call | flops 1000000 | tf_op jit(solution)/shard_map/context/pallas_call | solution.py:349
  27.6 4.3 %all-to-all-start.1 = ((bf16[16,64,512]{2,1,0:T(8,128)(2,1)}), bf16[16,64,512]{2,1,0:T(8,128)(2,1)S(1)}, u32[]{:S(2)}, u32[]{:S(2)}) async-start(bf16[16,64,512]{2,1,0:T(8,128)(2,1)} %get-tuple-element.25), calls=%async_computation.1 | async-start | bytes 2097152 | tf_op jit(solution)/shard_map/all_to_all | solution.py:426
  31.9 0.0 copy-done.3
  31.9 0.0 copy-done.4
  31.9 0.1 fusion.1
  32.1 0.0 collective-permute-done.1.two_ref
  32.1 0.0 collective-permute-done.one_ref
  32.1 0.0 copy-done
  32.1 0.0 copy-done.1
  32.1 0.0 copy-done.2
  32.1 12.2 %local.1 = (bf16[256,1024]{1,0:T(8,128)(2,1)S(1)}, f32[256,1024]{1,0:T(8,128)}, f32[256,1024]{1,0:T(8,128)}, f32[256,1024]{1,0:T(8,128)}) custom-call(f32[16]{0:T(128)S(1)} %copy-done, f32[8,2048]{1,0:T(8,128)} %get-tuple-element.22.vec_ref, bf16[256,2048]{1,0:T(8,128)(2,1)} %lat_ref.5, bf16[128,2048]{1,0:T(8,128)(2,1)} %collective-permute-done.one_ref, ...), custom_call_target="tpu_custom_call" | custom-call | flops 10000000000 | tf_op jit(solution)/shard_map/local/pallas_call | solution.py:349
  44.4 4.3 %all-to-all-done.1 = bf16[16,64,512]{2,1,0:T(8,128)(2,1)S(1)} async-done(((bf16[16,64,512]{2,1,0:T(8,128)(2,1)}), bf16[16,64,512]{2,1,0:T(8,128)(2,1)S(1)}, u32[]{:S(2)}, u32[]{:S(2)}) %all-to-all-start.1) | async-done | bytes 1048608 | tf_op jit(solution)/shard_map/all_to_all | solution.py:426
  48.6 11.8 %final.1 = bf16[256,2048]{1,0:T(8,128)(2,1)} custom-call(bf16[256,1024]{1,0:T(8,128)(2,1)S(1)} %get-tuple-element.24.q_ref, bf16[1024,512]{1,0:T(8,128)(2,1)S(1)} %bitcast.5, f32[256,1024]{1,0:T(8,128)} %get-tuple-element.26.o_ref, f32[256,1024]{1,0:T(8,128)} %get-tuple-element.27.l_ref, f32[256,1024]{1,0:T(8,128)} %get-tuple-element.28.m_ref, ...), custom_call_target="tpu_custom_call" | custom-call | flops 10000000000 | tf_op jit(solution)/shard_map/final/pallas_call | solution.py:349
  (1 shorter events, 0.0 us)
Async XLA Ops:
  2.4 23.5 %all-to-all-start = ((bf16[64,8,384]{2,1,0:T(8,128)(2,1)}), bf16[64,8,384]{2,1,0:T(8,128)(2,1)S(1)}, u32[]{:S(2)}, u32[]{:S(2)}) async-start(bf16[64,8,384]{2,1,0:T(8,128)(2,1)} %get-tuple-element.17), calls=%async_computation | async-start | bytes 786432 | tf_op jit(solution)/shard_map/all_to_all | solution.py:410
  14.0 18.1 %collective-permute-start.1 = (bf16[128,2048]{1,0:T(8,128)(2,1)}, bf16[128,2048]{1,0:T(8,128)(2,1)}, u32[]{:S(2)}, u32[]{:S(2)}) collective-permute-start(bf16[128,2048]{1,0:T(8,128)(2,1)} %get-tuple-element.23), channel_id=1, source_target_pairs={{2,4},{4,2},{6,8},{8,6},{10,12},{12,10},{14,16},{16,14},{18,20},{2... | collective-permute-start | bytes 1572872 | tf_op jit(solution)/shard_map/ppermute | solution.py:414
  15.4 16.6 %collective-permute-start = (bf16[128,2048]{1,0:T(8,128)(2,1)}, bf16[128,2048]{1,0:T(8,128)(2,1)}, u32[]{:S(2)}, u32[]{:S(2)}) collective-permute-start(bf16[128,2048]{1,0:T(8,128)(2,1)} %get-tuple-element.18.after_ref), channel_id=1, source_target_pairs={{0,2},{2,0},{4,6},{6,4},{8,10},{10,8},{12,14},{14,12},{16,18},{18,... | collective-permute-start | bytes 1572872 | tf_op jit(solution)/shard_map/ppermute | solution.py:413
  20.7 11.2 %copy-start.3 = (f32[256]{0:T(256)S(1)}, f32[256]{0:T(256)}, u32[]{:S(2)}) copy-start(f32[256]{0:T(256)} %constant.27.clone) | copy-start | bytes 3076
  20.7 11.2 %copy-start.4 = (f32[256]{0:T(256)S(1)}, f32[256]{0:T(256)}, u32[]{:S(2)}) copy-start(f32[256]{0:T(256)} %constant.26.clone) | copy-start | bytes 3076
  20.7 11.4 %copy-start = (f32[16]{0:T(128)S(1)}, f32[16]{0:T(128)}, u32[]{:S(2)}) copy-start(f32[16]{0:T(128)} %sink_ref.1) | copy-start | bytes 196
  20.7 11.4 %copy-start.1 = (f32[64,256]{1,0:T(8,128)S(1)}, f32[64,256]{1,0:T(8,128)}, u32[]{:S(2)}) copy-start(f32[64,256]{1,0:T(8,128)} %constant.25.clone.cols_ref) | copy-start | bytes 196612
  20.7 11.4 %copy-start.2 = (f32[64,256]{1,0:T(8,128)S(1)}, f32[64,256]{1,0:T(8,128)}, u32[]{:S(2)}) copy-start(f32[64,256]{1,0:T(8,128)} %constant.24.clone.colc_ref) | copy-start | bytes 196612
  27.6 21.1 %all-to-all-start.1 = ((bf16[16,64,512]{2,1,0:T(8,128)(2,1)}), bf16[16,64,512]{2,1,0:T(8,128)(2,1)S(1)}, u32[]{:S(2)}, u32[]{:S(2)}) async-start(bf16[16,64,512]{2,1,0:T(8,128)(2,1)} %get-tuple-element.25), calls=%async_computation.1 | async-start | bytes 2097152 | tf_op jit(solution)/shard_map/all_to_all | solution.py:426

commit v6 on v5

--- a/solution.py
+++ b/solution.py
@@ -51,14 +51,11 @@
 
 
 def entry_kernel(
-    cond_ref, cctx_ref, mod_ref, lat_ref,
-    parts_ref, one_ref, two_ref,
-    cond_v, cctx_v, mod_v, lat_v, block_v, sems,
+    cond_ref, cctx_ref, mod_ref, parts_ref, cond_v, cctx_v, mod_v, block_v, sems
 ):
     sp = lax.axis_index("sp")
-    odd = place_of() & 1
     copy = pltpu.make_async_copy
-    pairs = ((mod_ref, mod_v), (cond_ref, cond_v), (cctx_ref, cctx_v), (lat_ref, lat_v))
+    pairs = ((mod_ref, mod_v), (cond_ref, cond_v), (cctx_ref, cctx_v))
     ins = [copy(src, dst, sems.at[i]) for i, (src, dst) in enumerate(pairs)]
     for c in ins:
         c.start()
@@ -82,24 +79,30 @@
     block = jnp.concatenate(rows, axis=0).astype(BF16)
     for i in range(block_v.shape[0]):
         block_v[i] = block
-    outs = [copy(block_v, parts_ref, sems.at[4])]
-    outs[0].start()
-    ins[3].wait()
-    outs.append(copy(lat_v.at[pl.ds((1 - odd) * 128, 128)], one_ref, sems.at[5]))
-    outs.append(copy(lat_v.at[pl.ds(odd * 128, 128)], two_ref, sems.at[6]))
-    outs[1].start()
-    outs[2].start()
-    for c in outs:
-        c.wait()
+    out = copy(block_v, parts_ref, sems.at[3])
+    out.start()
+    out.wait()
 
 
 def prep_kernel(
-    after_ref, ctx_ref, gain_ref, wk_ref, wv_ref, ng_ref, wk_out, wv_out, ctx_v, gain_v, sems
+    after_ref, ctx_ref, gain_ref, wk_ref, wv_ref, lat_ref,
+    ng_ref, wk_out, wv_out, one_ref, two_ref,
+    ctx_v, gain_v, lat_v, sems,
 ):
+    odd = place_of() & 1
     copy = pltpu.make_async_copy
     pairs = ((ctx_ref, ctx_v), (gain_ref, gain_v), (wk_ref, wk_out), (wv_ref, wv_out))
     ins = [copy(src, dst, sems.at[i]) for i, (src, dst) in enumerate(pairs)]
+    rows = copy(lat_ref, lat_v, sems.at[4])
+    outs = [
+        copy(lat_v.at[pl.ds((1 - odd) * 128, 128)], one_ref, sems.at[5]),
+        copy(lat_v.at[pl.ds(odd * 128, 128)], two_ref, sems.at[6]),
+    ]
+    rows.start()
     for c in ins:
+        c.start()
+    rows.wait()
+    for c in outs:
         c.start()
     ins[0].wait()
     ins[1].wait()
@@ -108,8 +111,8 @@
     rs = lax.rsqrt(jnp.mean(x * x, axis=-1, keepdims=True) + EPSILON)
     ng_ref[0:64, :] = x * rs * gain
     ng_ref[64:72, :] = jnp.broadcast_to(gain, (8, 2048))
-    ins[2].wait()
-    ins[3].wait()
+    for c in ins[2:] + outs:
+        c.wait()
 
 
 def context_kernel(recv_ref, ng_ref, wk_ref, wv_ref, send_ref, vec_ref, kv_v, vec_v, sems):
@@ -166,8 +169,8 @@
 def local_kernel(
     sink_ref, vec_ref, lat_ref, one_ref, two_ref, wq_ref, wk_ref, wv_ref,
     rowc_ref, rows_ref, colc_ref, cols_ref,
-    q_ref, o_ref, l_ref, m_ref,
-    vec_v, lat_v, wq_v, wkv_v, hid_v, o_v, l_v, m_v, sems,
+    q_ref, o_ref, lse_ref,
+    vec_v, lat_v, wq_v, wkv_v, hid_v, sems,
 ):
     place = place_of()
     odd = place & 1
@@ -205,7 +208,7 @@
     for r in (0, 3):
         rows = slice(r * 128, r * 128 + 128)
         hid_v[rows, :] = normed(lat_v[rows, :], mult, shift)
-    for c in weights:
+    for c in weights[:2]:
         c.wait()
     kv = dot(hid_v[...], wkv_v[...]).astype(BF16)
     keys = rotated(kv[:, 0:256], cos, sin, swap).astype(BF16)
@@ -220,6 +223,8 @@
         (from_low + jnp.where(place > 0, 0.0, NEG_BIG), from_high),
         (from_low, from_high + jnp.where(place < last, 0.0, NEG_BIG)),
     )
+    for c in weights[2:]:
+        c.wait()
     slabs = []
     for a in range(2):
         q = dot(hid_v[128:384, :], wq_v[a]).astype(BF16)
@@ -235,6 +240,8 @@
             q_ref[:, at : at + 128] = one
             q_ref[:, at + 128 : at + 256] = two
             slabs += paired(turned[0][:, piece], turned[1][:, piece], low_own)
+    eighth = (iota((128, 128), 1) & 63) >> 3
+    lse = [jnp.zeros((128, 128), F32) for _ in range(2)]
     for a in range(2):
         va = jnp.concatenate([kv[:, 256 + a * 128 : 384 + a * 128], ones], axis=1)
         for b in range(2):
@@ -260,29 +267,20 @@
                 x, y = o[g * 256 : g * 256 + 128], o[g * 256 + 128 : g * 256 + 256]
                 (mx, sx), (my, sy) = ms[2 * g], ms[2 * g + 1]
                 m = jnp.where(low, mx, my)
-                o_v[rows, to] = jnp.where(low, x[:, 0:128], y[:, 0:128])
-                l_v[rows, to] = jnp.where(low, x[:, 128:256], y[:, 128:256]) + jnp.exp2(
-                    jnp.where(low, sx, sy) - m
-                )
-                m_v[rows, to] = m
-    outs = [
-        copy(src, dst, sems.at[8 + i])
-        for i, (src, dst) in enumerate(((o_v, o_ref), (l_v, l_ref), (m_v, m_ref)))
-    ]
-    for c in outs:
-        c.start()
-    for c in outs:
-        c.wait()
+                l = jnp.where(low, x[:, 128:256], y[:, 128:256])
+                l = l + jnp.exp2(jnp.where(low, sx, sy) - m)
+                o_ref[rows, to] = jnp.where(low, x[:, 0:128], y[:, 0:128]) / l
+                lse[b] = jnp.where(eighth == a * 4 + g, m + jnp.log2(l), lse[b])
+    for b in range(2):
+        lse_ref[b * 128 : b * 128 + 128, :] = lse[b]
 
 
 def final_kernel(
-    q_ref, kv_ref, o_ref, l_ref, m_ref, wo_ref, lat_ref, vec_ref, gain_ref, out_ref,
-    o_v, l_v, m_v, wo_v, lat_v, vec_v, gain_v, oc_v, lc_v, mc_v, out_v, sems,
+    q_ref, kv_ref, o_ref, lse_ref, wo_ref, lat_ref, vec_ref, gain_ref, out_ref,
+    wo_v, lat_v, vec_v, gain_v, oc_v, lc_v, mc_v, out_v, sems,
 ):
     copy = pltpu.make_async_copy
-    pairs = [
-        (o_ref, o_v), (l_ref, l_v), (m_ref, m_v), (lat_ref, lat_v), (vec_ref, vec_v), (gain_ref, gain_v),
-    ]
+    pairs = [(lat_ref, lat_v), (vec_ref, vec_v), (gain_ref, gain_v)]
     for a in range(2):
         for g in range(4):
             for i in range(2):
@@ -320,12 +318,14 @@
     for b in range(2):
         rows = slice(b * 128, b * 128 + 128)
         mixed = []
-        for to in slabs:
-            ml, mc = m_v[rows, to], mc_v[rows, to]
+        for i, to in enumerate(slabs):
+            here = [lse_ref[rows, c : c + 1] for c in (i * 8, i * 8 + 64)]
+            here = [jnp.broadcast_to(x, (128, 128)) for x in here]
+            ml, mc = jnp.where(low[0:128], here[0], here[1]), mc_v[rows, to]
             top = jnp.maximum(ml, mc)
             wl, wc = jnp.exp2(ml - top), jnp.exp2(mc - top)
-            num = wl * o_v[rows, to] + wc * oc_v[rows, to]
-            den = wl * l_v[rows, to] + wc * lc_v[rows, to]
+            num = wl * o_ref[rows, to] + wc * oc_v[rows, to]
+            den = wl + wc * lc_v[rows, to]
             mixed.append((num / den).astype(BF16))
         projected = dot(jnp.concatenate(mixed, axis=1), wo_v[...])
         rs = lax.rsqrt(jnp.mean(projected * projected, axis=-1, keepdims=True) + EPSILON)
@@ -379,31 +379,31 @@
     square = (16, 128)
     small = w_key.shape
 
-    parts, one, two = call(
+    (parts,) = call(
         entry_kernel,
         "entry",
-        "hhhh",
-        [("h", (count, 8, 384), BF16), ("h", half, BF16), ("h", half, BF16)],
-        [
-            (square, BF16),
-            (square, BF16),
-            (mod_weight.shape, BF16),
-            (latent.shape, BF16),
-            ((count, 8, 384), BF16),
-        ],
-        7,
-        (cond.reshape(square), ctx_cond.reshape(square), mod_weight, latent),
+        "hhh",
+        [("h", (count, 8, 384), BF16)],
+        [(square, BF16), (square, BF16), (mod_weight.shape, BF16), ((count, 8, 384), BF16)],
+        4,
+        (cond.reshape(square), ctx_cond.reshape(square), mod_weight),
         10**6,
         8,
     )
-    ng, wk_near, wv_near = call(
+    ng, wk_near, wv_near, one, two = call(
         prep_kernel,
         "prep",
-        "hhhhh",
-        [("V", (72, width), F32), ("V", small, BF16), ("V", small, BF16)],
-        [(ctx_rows.shape, BF16), (line, F32)],
-        4,
-        (one, ctx_rows, norm_gain.reshape(line), w_key, w_value),
+        "hhhhhh",
+        [
+            ("V", (72, width), F32),
+            ("V", small, BF16),
+            ("V", small, BF16),
+            ("h", half, BF16),
+            ("h", half, BF16),
+        ],
+        [(ctx_rows.shape, BF16), (line, F32), (latent.shape, BF16)],
+        7,
+        (parts, ctx_rows, norm_gain.reshape(line), w_key, w_value, latent),
         2 * 10**9,
         4,
     )
@@ -435,22 +435,19 @@
     angle = grid_row.astype(F32)[:, None] * jnp.asarray(freq, F32)[None, :]
     tables = (jnp.cos(angle) * by_row, jnp.sin(angle) * by_row, colc, cols)
 
-    query, o, l, m = call(
+    query, o, lse = call(
         local_kernel,
         "local",
         "shhhhhhhvvvv",
-        [("V", wide, BF16), ("h", wide, F32), ("h", wide, F32), ("h", wide, F32)],
+        [("V", wide, BF16), ("V", wide, F32), ("V", (rows, 128), F32)],
         [
             (rest, F32),
             ((2 * rows, width), BF16),
             ((2, width, 512), BF16),
             ((width, 512), BF16),
             ((2 * rows, width), BF16),
-            (wide, F32),
-            (wide, F32),
-            (wide, F32),
         ],
-        11,
+        8,
         (sink, vecs, latent, one, two, w_query, w_key, w_value, *tables),
         10**10,
         26,
@@ -458,12 +455,9 @@
     (updated,) = call(
         final_kernel,
         "final",
-        "VVhhhhhhh",
+        "VVVVhhhh",
         [("h", latent.shape, BF16)],
         [
-            (wide, F32),
-            (wide, F32),
-            (wide, F32),
             (w_out.shape, BF16),
             (latent.shape, BF16),
             (rest, F32),
@@ -473,8 +467,8 @@
             (wide, F32),
             (latent.shape, BF16),
         ],
-        24,
-        (query, kv_ctx, o, l, m, w_out, latent, vecs, out_gain.reshape(line)),
+        21,
+        (query, kv_ctx, o, lse, w_out, latent, vecs, out_gain.reshape(line)),
         10**10,
         28,
     )

time: 61 us -> 63.3 us (1.038); the launches traced: 60.6 us -> 62.1 us
  waiting for transfers between devices: 9.51 us -> 16.6 us
  Pallas kernels: 29.7 us -> 26.5 us
  starting transfers between devices: 20.9 us -> 18.5 us
    all_to_all x1, waiting for transfers between devices: 4.29 us -> 9.62 us  [shards(): lax.all_to_all(send, 'sp', 0, 0, tiled=True).reshape(sp_size * 64, 512)]
    pallas_call x5, Pallas kernels: 29.7 us -> 26.5 us  [call(): pl.pallas_call(kernel, out_shape=[FIXED.get(k, jax.ShapeDtypeStruct)(s, d...]
    ppermute x1, starting transfers between devices: 3.57 us -> 1.65 us  [shards(): one = lax.ppermute(one, both, swap_one)]
    all_to_all x1, waiting for transfers between devices: 5.21 us -> 6.98 us  [shards(): recv = lax.all_to_all(parts, both, 0, 0, tiled=True)]
  transfers between devices with their start and end apart: 4 -> 4, of which waited for: 2 -> 2; matrix products, arithmetic and copies ran while one was open for 0% -> 0% of each run, Pallas kernels for 26% -> 22%
where the time goes in v6:
time: 63.3 us; the launch traced here: 62.1 us
  Pallas kernels  26.5 us (42%)
  starting transfers between devices  18.5 us (29%)
  waiting for transfers between devices  16.6 us (26%)
    pallas_call x5, Pallas kernels, call(): pl.pallas_call(kernel, out_shape=[FIXED.get(k, jax.ShapeDtypeStruct)(s, d...  26.5 us
    all_to_all x1, starting transfers between devices, shards(): recv = lax.all_to_all(parts, both, 0, 0, tiled=True)  11.5 us
    all_to_all x1, waiting for transfers between devices, shards(): lax.all_to_all(send, 'sp', 0, 0, tiled=True).reshape(sp_size * 64, 512)  9.62 us
    all_to_all x1, waiting for transfers between devices, shards(): recv = lax.all_to_all(parts, both, 0, 0, tiled=True)  6.98 us
    all_to_all x1, starting transfers between devices, shards(): lax.all_to_all(send, 'sp', 0, 0, tiled=True).reshape(sp_size * 64, 512)  3.85 us
    ppermute x1, starting transfers between devices, shards(): one = lax.ppermute(one, both, swap_one)  1.65 us
    ppermute x1, starting transfers between devices, shards(): two = lax.ppermute(two, both, swap_two)  1.46 us
  transfers between devices with their start and end apart: 4, of which 2 were waited for; matrix products, arithmetic and copies ran while one was open for 0% of the time, Pallas kernels for 22%

profile of v6, /device:TPU:0, one launch (start us, length us, event | category | flops | bytes accessed | tf_op | source)
XLA Modules:
  0.0 62.1 jit_solution(17941458419998762277)
XLA Ops:
  0.0 2.0 %entry.1.after_ref = bf16[64,8,384]{2,1,0:T(8,128)(2,1)} custom-call(bf16[16,128]{1,0:T(8,128)(2,1)} %bitcast.6, bf16[16,128]{1,0:T(8,128)(2,1)} %bitcast.7, bf16[3,128,512]{2,1,0:T(8,128)(2,1)} %mod_ref.1), custom_call_target="tpu_custom_call" | custom-call | flops 1000000 | tf_op jit(solution)/shard_map/entry/pallas_call | solution.py:349
  2.0 11.5 %all-to-all-start = ((bf16[64,8,384]{2,1,0:T(8,128)(2,1)}), bf16[64,8,384]{2,1,0:T(8,128)(2,1)S(1)}, u32[]{:S(2)}, u32[]{:S(2)}) async-start(bf16[64,8,384]{2,1,0:T(8,128)(2,1)} %entry.1.after_ref), calls=%async_computation | async-start | bytes 786432 | tf_op jit(solution)/shard_map/all_to_all | solution.py:410
  13.5 2.3 %prep.1 = (f32[72,2048]{1,0:T(8,128)S(1)}, bf16[2048,256]{1,0:T(8,128)(2,1)S(1)}, bf16[2048,256]{1,0:T(8,128)(2,1)S(1)}, bf16[128,2048]{1,0:T(8,128)(2,1)}, bf16[128,2048]{1,0:T(8,128)(2,1)}) custom-call(bf16[64,8,384]{2,1,0:T(8,128)(2,1)} %entry.1.after_ref, bf16[64,2048]{1,0:T(8,128)(2,1)} %ctx_ref.1, f32[1,2048]{1,0:T(1,128)} %bitcast.8, ...), custom_call_target="tpu_custom_call" | custom-call | flops 2000000000 | tf_op jit(solution)/shard_map/prep/pallas_call | solution.py:349
  15.8 0.0 copy-start.3
  15.8 0.0 copy-start.4
  15.8 0.0 copy-start
  15.8 0.0 copy-start.1
  15.8 0.0 copy-start.2
  15.9 1.6 %collective-permute-start = (bf16[128,2048]{1,0:T(8,128)(2,1)}, bf16[128,2048]{1,0:T(8,128)(2,1)}, u32[]{:S(2)}, u32[]{:S(2)}) collective-permute-start(bf16[128,2048]{1,0:T(8,128)(2,1)} %get-tuple-element.19), channel_id=1, source_target_pairs={{0,2},{2,0},{4,6},{6,4},{8,10},{10,8},{12,14},{14,12},{16,18},{18,... | collective-permute-start | bytes 1572872 | tf_op jit(solution)/shard_map/ppermute | solution.py:413
  17.5 1.5 %collective-permute-start.1 = (bf16[128,2048]{1,0:T(8,128)(2,1)}, bf16[128,2048]{1,0:T(8,128)(2,1)}, u32[]{:S(2)}, u32[]{:S(2)}) collective-permute-start(bf16[128,2048]{1,0:T(8,128)(2,1)} %get-tuple-element.20), channel_id=1, source_target_pairs={{2,4},{4,2},{6,8},{8,6},{10,12},{12,10},{14,16},{16,14},{18,20},{2... | collective-permute-start | bytes 1572872 | tf_op jit(solution)/shard_map/ppermute | solution.py:414
  19.0 7.0 %all-to-all-done.recv_ref = bf16[64,8,384]{2,1,0:T(8,128)(2,1)S(1)} async-done(((bf16[64,8,384]{2,1,0:T(8,128)(2,1)}), bf16[64,8,384]{2,1,0:T(8,128)(2,1)S(1)}, u32[]{:S(2)}, u32[]{:S(2)}) %all-to-all-start) | async-done | bytes 393248 | tf_op jit(solution)/shard_map/all_to_all | solution.py:410
  26.0 1.6 %context.1 = (bf16[16,64,512]{2,1,0:T(8,128)(2,1)}, f32[8,2048]{1,0:T(8,128)}) custom-call(bf16[64,8,384]{2,1,0:T(8,128)(2,1)S(1)} %all-to-all-done.recv_ref, f32[72,2048]{1,0:T(8,128)S(1)} %get-tuple-element.15.ng_ref, bf16[2048,256]{1,0:T(8,128)(2,1)S(1)} %get-tuple-element.16.wk_ref, bf16[2048,256]{1,0:T(8,128)(2,1)S(1)} %get-tuple-element.17.wv_ref), custom_call_target="tpu_custom_call" | custom-call | flops 1000000 | tf_op jit(solution)/shard_map/context/pallas_call | solution.py:349
  27.6 3.8 %all-to-all-start.1 = ((bf16[16,64,512]{2,1,0:T(8,128)(2,1)}), bf16[16,64,512]{2,1,0:T(8,128)(2,1)S(1)}, u32[]{:S(2)}, u32[]{:S(2)}) async-start(bf16[16,64,512]{2,1,0:T(8,128)(2,1)} %get-tuple-element.22), calls=%async_computation.1 | async-start | bytes 2097152 | tf_op jit(solution)/shard_map/all_to_all | solution.py:426
  31.4 0.0 copy-done.3
  31.4 0.0 copy-done.4
  31.4 0.1 fusion.1
  31.6 0.0 collective-permute-done.one_ref
  31.6 0.0 collective-permute-done.1.two_ref
  31.6 0.0 copy-done
  31.6 0.0 copy-done.1
  31.6 0.0 copy-done.2
  31.6 9.5 %local.1 = (bf16[256,1024]{1,0:T(8,128)(2,1)S(1)}, f32[256,1024]{1,0:T(8,128)S(1)}, f32[256,128]{1,0:T(8,128)S(1)}) custom-call(f32[16]{0:T(128)S(1)} %copy-done, f32[8,2048]{1,0:T(8,128)} %get-tuple-element.18.vec_ref, bf16[256,2048]{1,0:T(8,128)(2,1)} %lat_ref.5, bf16[128,2048]{1,0:T(8,128)(2,1)} %collective-permute-done.one_ref, ...), custom_call_target="tpu_custom_call" | custom-call | flops 10000000000 | tf_op jit(solution)/shard_map/local/pallas_call | solution.py:349
  41.1 9.6 %all-to-all-done.1 = bf16[16,64,512]{2,1,0:T(8,128)(2,1)S(1)} async-done(((bf16[16,64,512]{2,1,0:T(8,128)(2,1)}), bf16[16,64,512]{2,1,0:T(8,128)(2,1)S(1)}, u32[]{:S(2)}, u32[]{:S(2)}) %all-to-all-start.1) | async-done | bytes 1048608 | tf_op jit(solution)/shard_map/all_to_all | solution.py:426
  50.8 11.1 %final.1 = bf16[256,2048]{1,0:T(8,128)(2,1)} custom-call(bf16[256,1024]{1,0:T(8,128)(2,1)S(1)} %get-tuple-element.21.q_ref, bf16[1024,512]{1,0:T(8,128)(2,1)S(1)} %bitcast.5, f32[256,1024]{1,0:T(8,128)S(1)} %get-tuple-element.23.o_ref, f32[256,128]{1,0:T(8,128)S(1)} %get-tuple-element.24.lse_ref, bf16[1024,2048]{1,0:T(8,128)(2,1)} %wo_ref.1, ...), custom_call_target="tpu_custom_call" | custom-call | flops 10000000000 | tf_op jit(solution)/shard_map/final/pallas_call | solution.py:349
  (1 shorter events, 0.0 us)
Async XLA Ops:
  2.0 24.0 %all-to-all-start = ((bf16[64,8,384]{2,1,0:T(8,128)(2,1)}), bf16[64,8,384]{2,1,0:T(8,128)(2,1)S(1)}, u32[]{:S(2)}, u32[]{:S(2)}) async-start(bf16[64,8,384]{2,1,0:T(8,128)(2,1)} %entry.1.after_ref), calls=%async_computation | async-start | bytes 786432 | tf_op jit(solution)/shard_map/all_to_all | solution.py:410
  15.8 15.6 %copy-start.3 = (f32[256]{0:T(256)S(1)}, f32[256]{0:T(256)}, u32[]{:S(2)}) copy-start(f32[256]{0:T(256)} %constant.26.clone) | copy-start | bytes 3076
  15.8 15.6 %copy-start.4 = (f32[256]{0:T(256)S(1)}, f32[256]{0:T(256)}, u32[]{:S(2)}) copy-start(f32[256]{0:T(256)} %constant.27.clone) | copy-start | bytes 3076
  15.8 15.8 %copy-start = (f32[16]{0:T(128)S(1)}, f32[16]{0:T(128)}, u32[]{:S(2)}) copy-start(f32[16]{0:T(128)} %sink_ref.1) | copy-start | bytes 196
  15.8 15.8 %copy-start.1 = (f32[64,256]{1,0:T(8,128)S(1)}, f32[64,256]{1,0:T(8,128)}, u32[]{:S(2)}) copy-start(f32[64,256]{1,0:T(8,128)} %constant.24.clone.colc_ref) | copy-start | bytes 196612
  15.8 15.8 %copy-start.2 = (f32[64,256]{1,0:T(8,128)S(1)}, f32[64,256]{1,0:T(8,128)}, u32[]{:S(2)}) copy-start(f32[64,256]{1,0:T(8,128)} %constant.25.clone.cols_ref) | copy-start | bytes 196612
  15.9 15.7 %collective-permute-start = (bf16[128,2048]{1,0:T(8,128)(2,1)}, bf16[128,2048]{1,0:T(8,128)(2,1)}, u32[]{:S(2)}, u32[]{:S(2)}) collective-permute-start(bf16[128,2048]{1,0:T(8,128)(2,1)} %get-tuple-element.19), channel_id=1, source_target_pairs={{0,2},{2,0},{4,6},{6,4},{8,10},{10,8},{12,14},{14,12},{16,18},{18,... | collective-permute-start | bytes 1572872 | tf_op jit(solution)/shard_map/ppermute | solution.py:413
  17.5 14.1 %collective-permute-start.1 = (bf16[128,2048]{1,0:T(8,128)(2,1)}, bf16[128,2048]{1,0:T(8,128)(2,1)}, u32[]{:S(2)}, u32[]{:S(2)}) collective-permute-start(bf16[128,2048]{1,0:T(8,128)(2,1)} %get-tuple-element.20), channel_id=1, source_target_pairs={{2,4},{4,2},{6,8},{8,6},{10,12},{12,10},{14,16},{16,14},{18,20},{2... | collective-permute-start | bytes 1572872 | tf_op jit(solution)/shard_map/ppermute | solution.py:414
  27.6 23.2 %all-to-all-start.1 = ((bf16[16,64,512]{2,1,0:T(8,128)(2,1)}), bf16[16,64,512]{2,1,0:T(8,128)(2,1)S(1)}, u32[]{:S(2)}, u32[]{:S(2)}) async-start(bf16[16,64,512]{2,1,0:T(8,128)(2,1)} %get-tuple-element.22), calls=%async_computation.1 | async-start | bytes 2097152 | tf_op jit(solution)/shard_map/all_to_all | solution.py:426

commit v7 on v5

--- a/solution.py
+++ b/solution.py
@@ -82,11 +82,13 @@
     block = jnp.concatenate(rows, axis=0).astype(BF16)
     for i in range(block_v.shape[0]):
         block_v[i] = block
-    outs = [copy(block_v, parts_ref, sems.at[4])]
+    outs = [
+        copy(block_v, parts_ref, sems.at[4]),
+        copy(lat_v.at[pl.ds((1 - odd) * 128, 128)], one_ref, sems.at[5]),
+        copy(lat_v.at[pl.ds(odd * 128, 128)], two_ref, sems.at[6]),
+    ]
     outs[0].start()
     ins[3].wait()
-    outs.append(copy(lat_v.at[pl.ds((1 - odd) * 128, 128)], one_ref, sems.at[5]))
-    outs.append(copy(lat_v.at[pl.ds(odd * 128, 128)], two_ref, sems.at[6]))
     outs[1].start()
     outs[2].start()
     for c in outs:
@@ -108,8 +110,8 @@
     rs = lax.rsqrt(jnp.mean(x * x, axis=-1, keepdims=True) + EPSILON)
     ng_ref[0:64, :] = x * rs * gain
     ng_ref[64:72, :] = jnp.broadcast_to(gain, (8, 2048))
-    ins[2].wait()
-    ins[3].wait()
+    for c in ins[2:]:
+        c.wait()
 
 
 def context_kernel(recv_ref, ng_ref, wk_ref, wv_ref, send_ref, vec_ref, kv_v, vec_v, sems):
@@ -166,8 +168,8 @@
 def local_kernel(
     sink_ref, vec_ref, lat_ref, one_ref, two_ref, wq_ref, wk_ref, wv_ref,
     rowc_ref, rows_ref, colc_ref, cols_ref,
-    q_ref, o_ref, l_ref, m_ref,
-    vec_v, lat_v, wq_v, wkv_v, hid_v, o_v, l_v, m_v, sems,
+    q_ref, o_ref, lse_ref,
+    vec_v, lat_v, wq_v, wkv_v, hid_v, sems,
 ):
     place = place_of()
     odd = place & 1
@@ -205,7 +207,7 @@
     for r in (0, 3):
         rows = slice(r * 128, r * 128 + 128)
         hid_v[rows, :] = normed(lat_v[rows, :], mult, shift)
-    for c in weights:
+    for c in weights[:2]:
         c.wait()
     kv = dot(hid_v[...], wkv_v[...]).astype(BF16)
     keys = rotated(kv[:, 0:256], cos, sin, swap).astype(BF16)
@@ -220,6 +222,8 @@
         (from_low + jnp.where(place > 0, 0.0, NEG_BIG), from_high),
         (from_low, from_high + jnp.where(place < last, 0.0, NEG_BIG)),
     )
+    for c in weights[2:]:
+        c.wait()
     slabs = []
     for a in range(2):
         q = dot(hid_v[128:384, :], wq_v[a]).astype(BF16)
@@ -235,6 +239,8 @@
             q_ref[:, at : at + 128] = one
             q_ref[:, at + 128 : at + 256] = two
             slabs += paired(turned[0][:, piece], turned[1][:, piece], low_own)
+    eighth = (iota((128, 128), 1) & 63) >> 3
+    lse = [jnp.zeros((128, 128), F32) for _ in range(2)]
     for a in range(2):
         va = jnp.concatenate([kv[:, 256 + a * 128 : 384 + a * 128], ones], axis=1)
         for b in range(2):
@@ -260,29 +266,20 @@
                 x, y = o[g * 256 : g * 256 + 128], o[g * 256 + 128 : g * 256 + 256]
                 (mx, sx), (my, sy) = ms[2 * g], ms[2 * g + 1]
                 m = jnp.where(low, mx, my)
-                o_v[rows, to] = jnp.where(low, x[:, 0:128], y[:, 0:128])
-                l_v[rows, to] = jnp.where(low, x[:, 128:256], y[:, 128:256]) + jnp.exp2(
-                    jnp.where(low, sx, sy) - m
-                )
-                m_v[rows, to] = m
-    outs = [
-        copy(src, dst, sems.at[8 + i])
-        for i, (src, dst) in enumerate(((o_v, o_ref), (l_v, l_ref), (m_v, m_ref)))
-    ]
-    for c in outs:
-        c.start()
-    for c in outs:
-        c.wait()
+                l = jnp.where(low, x[:, 128:256], y[:, 128:256])
+                l = l + jnp.exp2(jnp.where(low, sx, sy) - m)
+                o_ref[rows, to] = jnp.where(low, x[:, 0:128], y[:, 0:128]) / l
+                lse[b] = jnp.where(eighth == a * 4 + g, m + jnp.log2(l), lse[b])
+    for b in range(2):
+        lse_ref[b * 128 : b * 128 + 128, :] = lse[b]
 
 
 def final_kernel(
-    q_ref, kv_ref, o_ref, l_ref, m_ref, wo_ref, lat_ref, vec_ref, gain_ref, out_ref,
-    o_v, l_v, m_v, wo_v, lat_v, vec_v, gain_v, oc_v, lc_v, mc_v, out_v, sems,
+    q_ref, kv_ref, o_ref, lse_ref, wo_ref, lat_ref, vec_ref, gain_ref, out_ref,
+    wo_v, lat_v, vec_v, gain_v, mix_v, out_v, kt_v, va_v, even_v, odd_v, sems,
 ):
     copy = pltpu.make_async_copy
-    pairs = [
-        (o_ref, o_v), (l_ref, l_v), (m_ref, m_v), (lat_ref, lat_v), (vec_ref, vec_v), (gain_ref, gain_v),
-    ]
+    pairs = [(lat_ref, lat_v), (vec_ref, vec_v), (gain_ref, gain_v)]
     for a in range(2):
         for g in range(4):
             for i in range(2):
@@ -293,41 +290,51 @@
     for c in ins:
         c.start()
     low = iota((256, 128), 1) < HEAD_DIM
-    ones = jnp.ones((1024, 128), BF16)
-    kt = dot_nt(identity(), kv_ref[:, 0:256]).astype(BF16)
-    slabs = [slice(i * 128, i * 128 + 128) for i in range(8)]
-
-    def scores(i):
-        stacked = jnp.concatenate(split_pair(q_ref[:, slabs[i]], low), axis=0)
-        return dot(stacked, kt[(i // 4) * 128 : (i // 4) * 128 + 128, :])
-
-    s = scores(0)
-    for i in range(8):
-        coming = scores(i + 1) if i < 7 else None
-        a = i // 4
-        va = jnp.concatenate([kv_ref[:, 256 + a * 128 : 384 + a * 128], ones], axis=1)
+    eye = identity()
+    for a in range(2):
+        kt_v[a] = dot_nt(eye[a * 128 : a * 128 + 128], kv_ref[:, 0:256]).astype(BF16)
+        va_v[a, :, 0:128] = kv_ref[:, 256 + a * 128 : 384 + a * 128]
+        va_v[a, :, 128:256] = jnp.ones((1024, 128), BF16)
+
+    def scores(i, s_ref):
+        q = q_ref[:, pl.ds(pl.multiple_of(i * 128, 128), 128)]
+        stacked = jnp.concatenate(split_pair(q, low), axis=0)
+        s_ref[...] = dot(stacked, kt_v[i // 4])
+
+    def attend(i, s_ref):
+        s = s_ref[...]
         m = jnp.max(s, axis=-1, keepdims=True) * FACTOR
-        o = dot(jnp.exp2(s * FACTOR - m).astype(BF16), va)
+        o = dot(jnp.exp2(s * FACTOR - m).astype(BF16), va_v[i // 4])
         m = jnp.broadcast_to(m, (512, 128))
-        mc_v[:, slabs[i]] = jnp.where(low, m[0:256], m[256:512])
-        oc_v[:, slabs[i]] = jnp.where(low, o[0:256, 0:128], o[256:512, 0:128])
-        lc_v[:, slabs[i]] = jnp.where(low, o[0:256, 128:256], o[256:512, 128:256])
-        s = coming
+        mc = jnp.where(low, m[0:256], m[256:512])
+        oc = jnp.where(low, o[0:256, 0:128], o[256:512, 0:128])
+        lc = jnp.where(low, o[0:256, 128:256], o[256:512, 128:256])
+        at = pl.ds(pl.multiple_of(i * 128, 128), 128)
+        lse = pltpu.roll(lse_ref[...], (128 - 8 * i) & 127, 1)
+        here = [jnp.broadcast_to(lse[:, c : c + 1], (256, 128)) for c in (0, 64)]
+        ml = jnp.where(low, here[0], here[1])
+        top = jnp.maximum(ml, mc)
+        wl, wc = jnp.exp2(ml - top), jnp.exp2(mc - top)
+        mix_v[:, at] = ((wl * o_ref[:, at] + wc * oc) / (wl + wc * lc)).astype(BF16)
+
+    scores(0, even_v)
+
+    def two(j, carry):
+        i = 2 * j
+        scores(i + 1, odd_v)
+        attend(i, even_v)
+        scores(jnp.minimum(i + 2, 7), even_v)
+        attend(i + 1, odd_v)
+        return carry
+
+    lax.fori_loop(0, 4, two, 0)
     for c in ins:
         c.wait()
     scale = vec_v[2:3, :] * gain_v[...]
     outs = []
     for b in range(2):
         rows = slice(b * 128, b * 128 + 128)
-        mixed = []
-        for to in slabs:
-            ml, mc = m_v[rows, to], mc_v[rows, to]
-            top = jnp.maximum(ml, mc)
-            wl, wc = jnp.exp2(ml - top), jnp.exp2(mc - top)
-            num = wl * o_v[rows, to] + wc * oc_v[rows, to]
-            den = wl * l_v[rows, to] + wc * lc_v[rows, to]
-            mixed.append((num / den).astype(BF16))
-        projected = dot(jnp.concatenate(mixed, axis=1), wo_v[...])
+        projected = dot(mix_v[rows, :], wo_v[...])
         rs = lax.rsqrt(jnp.mean(projected * projected, axis=-1, keepdims=True) + EPSILON)
         out_v[rows, :] = (lat_v[rows, :].astype(F32) + projected * rs * scale).astype(BF16)
         there = pl.ds(b * 128, 128)
@@ -435,22 +442,19 @@
     angle = grid_row.astype(F32)[:, None] * jnp.asarray(freq, F32)[None, :]
     tables = (jnp.cos(angle) * by_row, jnp.sin(angle) * by_row, colc, cols)
 
-    query, o, l, m = call(
+    query, o, lse = call(
         local_kernel,
         "local",
         "shhhhhhhvvvv",
-        [("V", wide, BF16), ("h", wide, F32), ("h", wide, F32), ("h", wide, F32)],
+        [("V", wide, BF16), ("V", wide, F32), ("V", (rows, 128), F32)],
         [
             (rest, F32),
             ((2 * rows, width), BF16),
             ((2, width, 512), BF16),
             ((width, 512), BF16),
             ((2 * rows, width), BF16),
-            (wide, F32),
-            (wide, F32),
-            (wide, F32),
         ],
-        11,
+        8,
         (sink, vecs, latent, one, two, w_query, w_key, w_value, *tables),
         10**10,
         26,
@@ -458,23 +462,22 @@
     (updated,) = call(
         final_kernel,
         "final",
-        "VVhhhhhhh",
+        "VVVVhhhh",
         [("h", latent.shape, BF16)],
         [
-            (wide, F32),
-            (wide, F32),
-            (wide, F32),
             (w_out.shape, BF16),
             (latent.shape, BF16),
             (rest, F32),
             (line, F32),
-            (wide, F32),
-            (wide, F32),
-            (wide, F32),
+            (wide, BF16),
             (latent.shape, BF16),
+            ((2, 128, 1024), BF16),
+            ((2, 1024, 256), BF16),
+            ((512, 1024), F32),
+            ((512, 1024), F32),
         ],
-        24,
-        (query, kv_ctx, o, l, m, w_out, latent, vecs, out_gain.reshape(line)),
+        21,
+        (query, kv_ctx, o, lse, w_out, latent, vecs, out_gain.reshape(line)),
         10**10,
         28,
     )

time: 61 us -> 59.5 us (0.975)
  waiting for transfers between devices: 9.51 us -> 14.8 us
  Pallas kernels: 29.7 us -> 25.3 us
  starting transfers between devices: 20.9 us -> 18.5 us
    pallas_call x5, Pallas kernels: 29.7 us -> 25.3 us  [call(): pl.pallas_call(kernel, out_shape=[FIXED.get(k, jax.ShapeDtypeStruct)(s, d...]
    all_to_all x1, waiting for transfers between devices: 5.21 us -> 8.45 us  [shards(): recv = lax.all_to_all(parts, both, 0, 0, tiled=True)]
    all_to_all x1, waiting for transfers between devices: 4.29 us -> 6.32 us  [shards(): lax.all_to_all(send, 'sp', 0, 0, tiled=True).reshape(sp_size * 64, 512)]
    ppermute x1, starting transfers between devices: 3.57 us -> 1.65 us  [shards(): one = lax.ppermute(one, both, swap_one)]
  transfers between devices with their start and end apart: 4 -> 4, of which waited for: 2 -> 2; matrix products, arithmetic and copies ran while one was open for 0% -> 0% of each run, Pallas kernels for 26% -> 22%
where the time goes in v7:
time: 59.5 us; the launch traced here: 59 us
  Pallas kernels  25.3 us (43%)
  starting transfers between devices  18.5 us (31%)
  waiting for transfers between devices  14.8 us (25%)
    pallas_call x5, Pallas kernels, call(): pl.pallas_call(kernel, out_shape=[FIXED.get(k, jax.ShapeDtypeStruct)(s, d...  25.3 us
    all_to_all x1, starting transfers between devices, shards(): recv = lax.all_to_all(parts, both, 0, 0, tiled=True)  11.5 us
    all_to_all x1, waiting for transfers between devices, shards(): recv = lax.all_to_all(parts, both, 0, 0, tiled=True)  8.45 us
    all_to_all x1, waiting for transfers between devices, shards(): lax.all_to_all(send, 'sp', 0, 0, tiled=True).reshape(sp_size * 64, 512)  6.32 us
    all_to_all x1, starting transfers between devices, shards(): lax.all_to_all(send, 'sp', 0, 0, tiled=True).reshape(sp_size * 64, 512)  3.85 us
    ppermute x1, starting transfers between devices, shards(): one = lax.ppermute(one, both, swap_one)  1.65 us
    ppermute x1, starting transfers between devices, shards(): two = lax.ppermute(two, both, swap_two)  1.47 us
  transfers between devices with their start and end apart: 4, of which 2 were waited for; matrix products, arithmetic and copies ran while one was open for 0% of the time, Pallas kernels for 22%

profile of v7, /device:TPU:0, one launch (start us, length us, event | category | flops | bytes accessed | tf_op | source)
XLA Modules:
  0.0 59.0 jit_solution(6790762933428272600)
XLA Ops:
  0.0 2.4 %entry.1 = (bf16[64,8,384]{2,1,0:T(8,128)(2,1)}, bf16[128,2048]{1,0:T(8,128)(2,1)}, bf16[128,2048]{1,0:T(8,128)(2,1)}) custom-call(bf16[16,128]{1,0:T(8,128)(2,1)} %bitcast.6, bf16[16,128]{1,0:T(8,128)(2,1)} %bitcast.7, bf16[3,128,512]{2,1,0:T(8,128)(2,1)} %mod_ref.1, bf16[256,2048]{1,0:T(8,128)(2,1)} %lat_ref.5), custom_call_target="tpu_custom_call" | custom-call | flops 1000000 | tf_op jit(solution)/shard_map/entry/pallas_call | solution.py:356
  2.4 11.5 %all-to-all-start = ((bf16[64,8,384]{2,1,0:T(8,128)(2,1)}), bf16[64,8,384]{2,1,0:T(8,128)(2,1)S(1)}, u32[]{:S(2)}, u32[]{:S(2)}) async-start(bf16[64,8,384]{2,1,0:T(8,128)(2,1)} %get-tuple-element.16), calls=%async_computation | async-start | bytes 786432 | tf_op jit(solution)/shard_map/all_to_all | solution.py:417
  14.0 1.6 %collective-permute-start = (bf16[128,2048]{1,0:T(8,128)(2,1)}, bf16[128,2048]{1,0:T(8,128)(2,1)}, u32[]{:S(2)}, u32[]{:S(2)}) collective-permute-start(bf16[128,2048]{1,0:T(8,128)(2,1)} %get-tuple-element.17.after_ref), channel_id=1, source_target_pairs={{0,2},{2,0},{4,6},{6,4},{8,10},{10,8},{12,14},{14,12},{16,18},{18,... | collective-permute-start | bytes 1572872 | tf_op jit(solution)/shard_map/ppermute | solution.py:420
  15.6 1.5 %collective-permute-start.1 = (bf16[128,2048]{1,0:T(8,128)(2,1)}, bf16[128,2048]{1,0:T(8,128)(2,1)}, u32[]{:S(2)}, u32[]{:S(2)}) collective-permute-start(bf16[128,2048]{1,0:T(8,128)(2,1)} %get-tuple-element.22), channel_id=1, source_target_pairs={{2,4},{4,2},{6,8},{8,6},{10,12},{12,10},{14,16},{16,14},{18,20},{2... | collective-permute-start | bytes 1572872 | tf_op jit(solution)/shard_map/ppermute | solution.py:421
  17.1 1.7 %prep.1 = (f32[72,2048]{1,0:T(8,128)S(1)}, bf16[2048,256]{1,0:T(8,128)(2,1)S(1)}, bf16[2048,256]{1,0:T(8,128)(2,1)S(1)}) custom-call(bf16[128,2048]{1,0:T(8,128)(2,1)} %get-tuple-element.17.after_ref, bf16[64,2048]{1,0:T(8,128)(2,1)} %ctx_ref.1, f32[1,2048]{1,0:T(1,128)} %bitcast.8, bf16[2048,256]{1,0:T(8,128)(2,1)} %wk_ref.3, bf16[2048,256]{1,0:T(8,128)(2,1)} %wv_ref.3), custom_call_target="tpu_custom_call" | custom-call | flops 2000000000 | tf_op jit(solution)/shard_map/prep/pallas_call | solution.py:356
  18.8 0.0 copy-start.3
  18.8 0.0 copy-start.4
  18.8 0.0 copy-start
  18.8 0.0 copy-start.1
  18.8 0.0 copy-start.2
  18.8 8.4 %all-to-all-done.recv_ref = bf16[64,8,384]{2,1,0:T(8,128)(2,1)S(1)} async-done(((bf16[64,8,384]{2,1,0:T(8,128)(2,1)}), bf16[64,8,384]{2,1,0:T(8,128)(2,1)S(1)}, u32[]{:S(2)}, u32[]{:S(2)}) %all-to-all-start) | async-done | bytes 393248 | tf_op jit(solution)/shard_map/all_to_all | solution.py:417
  27.3 1.6 %context.1 = (bf16[16,64,512]{2,1,0:T(8,128)(2,1)}, f32[8,2048]{1,0:T(8,128)}) custom-call(bf16[64,8,384]{2,1,0:T(8,128)(2,1)S(1)} %all-to-all-done.recv_ref, f32[72,2048]{1,0:T(8,128)S(1)} %get-tuple-element.18.ng_ref, bf16[2048,256]{1,0:T(8,128)(2,1)S(1)} %get-tuple-element.19.wk_ref, bf16[2048,256]{1,0:T(8,128)(2,1)S(1)} %get-tuple-element.20.wv_ref), custom_call_target="tpu_custom_call" | custom-call | flops 1000000 | tf_op jit(solution)/shard_map/context/pallas_call | solution.py:356
  28.9 3.8 %all-to-all-start.1 = ((bf16[16,64,512]{2,1,0:T(8,128)(2,1)}), bf16[16,64,512]{2,1,0:T(8,128)(2,1)S(1)}, u32[]{:S(2)}, u32[]{:S(2)}) async-start(bf16[16,64,512]{2,1,0:T(8,128)(2,1)} %get-tuple-element.24), calls=%async_computation.1 | async-start | bytes 2097152 | tf_op jit(solution)/shard_map/all_to_all | solution.py:433
  32.8 0.0 copy-done.3
  32.8 0.0 copy-done.4
  32.8 0.1 fusion.1
  32.9 0.0 collective-permute-done.one_ref
  32.9 0.0 collective-permute-done.1.two_ref
  32.9 0.0 copy-done
  32.9 0.0 copy-done.1
  32.9 0.0 copy-done.2
  32.9 9.5 %local.1 = (bf16[256,1024]{1,0:T(8,128)(2,1)S(1)}, f32[256,1024]{1,0:T(8,128)S(1)}, f32[256,128]{1,0:T(8,128)S(1)}) custom-call(f32[16]{0:T(128)S(1)} %copy-done, f32[8,2048]{1,0:T(8,128)} %get-tuple-element.21.vec_ref, bf16[256,2048]{1,0:T(8,128)(2,1)} %lat_ref.5, bf16[128,2048]{1,0:T(8,128)(2,1)} %collective-permute-done.one_ref, ...), custom_call_target="tpu_custom_call" | custom-call | flops 10000000000 | tf_op jit(solution)/shard_map/local/pallas_call | solution.py:356
  42.5 6.3 %all-to-all-done.1 = bf16[16,64,512]{2,1,0:T(8,128)(2,1)S(1)} async-done(((bf16[16,64,512]{2,1,0:T(8,128)(2,1)}), bf16[16,64,512]{2,1,0:T(8,128)(2,1)S(1)}, u32[]{:S(2)}, u32[]{:S(2)}) %all-to-all-start.1) | async-done | bytes 1048608 | tf_op jit(solution)/shard_map/all_to_all | solution.py:433
  48.8 10.1 %final.1 = bf16[256,2048]{1,0:T(8,128)(2,1)} custom-call(bf16[256,1024]{1,0:T(8,128)(2,1)S(1)} %get-tuple-element.23.q_ref, bf16[1024,512]{1,0:T(8,128)(2,1)S(1)} %bitcast.5, f32[256,1024]{1,0:T(8,128)S(1)} %get-tuple-element.25.o_ref, f32[256,128]{1,0:T(8,128)S(1)} %get-tuple-element.26.lse_ref, bf16[1024,2048]{1,0:T(8,128)(2,1)} %wo_ref.1, ...), custom_call_target="tpu_custom_call" | custom-call | flops 10000000000 | tf_op jit(solution)/shard_map/final/pallas_call | solution.py:356
  (1 shorter events, 0.0 us)
Async XLA Ops:
  2.4 24.9 %all-to-all-start = ((bf16[64,8,384]{2,1,0:T(8,128)(2,1)}), bf16[64,8,384]{2,1,0:T(8,128)(2,1)S(1)}, u32[]{:S(2)}, u32[]{:S(2)}) async-start(bf16[64,8,384]{2,1,0:T(8,128)(2,1)} %get-tuple-element.16), calls=%async_computation | async-start | bytes 786432 | tf_op jit(solution)/shard_map/all_to_all | solution.py:417
  14.0 18.9 %collective-permute-start = (bf16[128,2048]{1,0:T(8,128)(2,1)}, bf16[128,2048]{1,0:T(8,128)(2,1)}, u32[]{:S(2)}, u32[]{:S(2)}) collective-permute-start(bf16[128,2048]{1,0:T(8,128)(2,1)} %get-tuple-element.17.after_ref), channel_id=1, source_target_pairs={{0,2},{2,0},{4,6},{6,4},{8,10},{10,8},{12,14},{14,12},{16,18},{18,... | collective-permute-start | bytes 1572872 | tf_op jit(solution)/shard_map/ppermute | solution.py:420
  15.6 17.3 %collective-permute-start.1 = (bf16[128,2048]{1,0:T(8,128)(2,1)}, bf16[128,2048]{1,0:T(8,128)(2,1)}, u32[]{:S(2)}, u32[]{:S(2)}) collective-permute-start(bf16[128,2048]{1,0:T(8,128)(2,1)} %get-tuple-element.22), channel_id=1, source_target_pairs={{2,4},{4,2},{6,8},{8,6},{10,12},{12,10},{14,16},{16,14},{18,20},{2... | collective-permute-start | bytes 1572872 | tf_op jit(solution)/shard_map/ppermute | solution.py:421
  18.8 14.0 %copy-start.3 = (f32[256]{0:T(256)S(1)}, f32[256]{0:T(256)}, u32[]{:S(2)}) copy-start(f32[256]{0:T(256)} %constant.26.clone) | copy-start | bytes 3076
  18.8 14.0 %copy-start.4 = (f32[256]{0:T(256)S(1)}, f32[256]{0:T(256)}, u32[]{:S(2)}) copy-start(f32[256]{0:T(256)} %constant.27.clone) | copy-start | bytes 3076
  18.8 14.1 %copy-start = (f32[16]{0:T(128)S(1)}, f32[16]{0:T(128)}, u32[]{:S(2)}) copy-start(f32[16]{0:T(128)} %sink_ref.1) | copy-start | bytes 196
  18.8 14.1 %copy-start.1 = (f32[64,256]{1,0:T(8,128)S(1)}, f32[64,256]{1,0:T(8,128)}, u32[]{:S(2)}) copy-start(f32[64,256]{1,0:T(8,128)} %constant.24.clone.colc_ref) | copy-start | bytes 196612
  18.8 14.1 %copy-start.2 = (f32[64,256]{1,0:T(8,128)S(1)}, f32[64,256]{1,0:T(8,128)}, u32[]{:S(2)}) copy-start(f32[64,256]{1,0:T(8,128)} %constant.25.clone.cols_ref) | copy-start | bytes 196612
  28.9 19.9 %all-to-all-start.1 = ((bf16[16,64,512]{2,1,0:T(8,128)(2,1)}), bf16[16,64,512]{2,1,0:T(8,128)(2,1)S(1)}, u32[]{:S(2)}, u32[]{:S(2)}) async-start(bf16[16,64,512]{2,1,0:T(8,128)(2,1)} %get-tuple-element.24), calls=%async_computation.1 | async-start | bytes 2097152 | tf_op jit(solution)/shard_map/all_to_all | solution.py:433

commit v8 on v7

--- a/solution.py
+++ b/solution.py
@@ -226,12 +226,13 @@
         c.wait()
     slabs = []
     for a in range(2):
-        q = dot(hid_v[128:384, :], wq_v[a]).astype(BF16)
+        q = dot(hid_v[128:384, :], wq_v[a])
         plain, turned = [], []
         for h in range(2):
             part = q[:, h * 256 : h * 256 + 256]
-            plain.append(part.astype(F32))
-            turned.append(rotated(part, cos[128:384], sin[128:384], swap))
+            plain.append(part * FACTOR)
+            part = part.astype(BF16)
+            turned.append(rotated(part, cos[128:384], sin[128:384], swap) * FACTOR)
         for p in range(2):
             piece = slice(p * 128, p * 128 + 128)
             at = a * 512 + p * 256
@@ -256,8 +257,8 @@
                 s0, s1, s2 = si[:, 0:128] + bias[b][0], si[:, 128:256], si[:, 256:384] + bias[b][1]
                 sink = sink_ref[(2 * a + i % 2) * 4 + i // 2] * LOG2E
                 m = jnp.max(jnp.maximum(jnp.maximum(s0, s1), s2), axis=-1, keepdims=True)
-                m = jnp.maximum(m * FACTOR, sink)
-                p = [jnp.exp2(x * FACTOR - m).astype(BF16) for x in (s0, s1, s2)]
+                m = jnp.maximum(m, sink)
+                p = [jnp.exp2(x - m).astype(BF16) for x in (s0, s1, s2)]
                 ps.append(jnp.concatenate(p, axis=1))
                 ms.append((jnp.broadcast_to(m, (128, 128)), sink))
             o = dot(jnp.concatenate(ps, axis=0), va[seen])
@@ -303,8 +304,8 @@
 
     def attend(i, s_ref):
         s = s_ref[...]
-        m = jnp.max(s, axis=-1, keepdims=True) * FACTOR
-        o = dot(jnp.exp2(s * FACTOR - m).astype(BF16), va_v[i // 4])
+        m = jnp.max(s, axis=-1, keepdims=True)
+        o = dot(jnp.exp2(s - m).astype(BF16), va_v[i // 4])
         m = jnp.broadcast_to(m, (512, 128))
         mc = jnp.where(low, m[0:256], m[256:512])
         oc = jnp.where(low, o[0:256, 0:128], o[256:512, 0:128])
@@ -323,13 +324,16 @@
         i = 2 * j
         scores(i + 1, odd_v)
         attend(i, even_v)
-        scores(jnp.minimum(i + 2, 7), even_v)
+        scores(i + 2, even_v)
         attend(i + 1, odd_v)
         return carry
 
-    lax.fori_loop(0, 4, two, 0)
+    lax.fori_loop(0, 3, two, 0)
     for c in ins:
         c.wait()
+    scores(7, odd_v)
+    attend(6, even_v)
+    attend(7, odd_v)
     scale = vec_v[2:3, :] * gain_v[...]
     outs = []
     for b in range(2):

time: 59.5 us -> 58.3 us (0.980)
  Pallas kernels: 25.3 us -> 23.8 us
    pallas_call x5, Pallas kernels: 25.3 us -> 23.8 us  [call(): pl.pallas_call(kernel, out_shape=[FIXED.get(k, jax.ShapeDtypeStruct)(s, d...]
where the time goes in v8:
time: 58.3 us; the launch traced here: 57.8 us
  Pallas kernels  23.8 us (41%)
  starting transfers between devices  18.5 us (32%)
  waiting for transfers between devices  15 us (26%)
    pallas_call x5, Pallas kernels, call(): pl.pallas_call(kernel, out_shape=[FIXED.get(k, jax.ShapeDtypeStruct)(s, d...  23.8 us
    all_to_all x1, starting transfers between devices, shards(): recv = lax.all_to_all(parts, both, 0, 0, tiled=True)  11.5 us
    all_to_all x1, waiting for transfers between devices, shards(): recv = lax.all_to_all(parts, both, 0, 0, tiled=True)  8.45 us
    all_to_all x1, waiting for transfers between devices, shards(): lax.all_to_all(send, 'sp', 0, 0, tiled=True).reshape(sp_size * 64, 512)  6.51 us
    all_to_all x1, starting transfers between devices, shards(): lax.all_to_all(send, 'sp', 0, 0, tiled=True).reshape(sp_size * 64, 512)  3.85 us
    ppermute x1, starting transfers between devices, shards(): one = lax.ppermute(one, both, swap_one)  1.65 us
    ppermute x1, starting transfers between devices, shards(): two = lax.ppermute(two, both, swap_two)  1.47 us
  transfers between devices with their start and end apart: 4, of which 2 were waited for; matrix products, arithmetic and copies ran while one was open for 0% of the time, Pallas kernels for 22%

profile of v8, /device:TPU:0, one launch (start us, length us, event | category | flops | bytes accessed | tf_op | source)
XLA Modules:
  0.0 57.8 jit_solution(10239589660669675520)
XLA Ops:
  0.0 2.4 %entry.1 = (bf16[64,8,384]{2,1,0:T(8,128)(2,1)}, bf16[128,2048]{1,0:T(8,128)(2,1)}, bf16[128,2048]{1,0:T(8,128)(2,1)}) custom-call(bf16[16,128]{1,0:T(8,128)(2,1)} %bitcast.6, bf16[16,128]{1,0:T(8,128)(2,1)} %bitcast.7, bf16[3,128,512]{2,1,0:T(8,128)(2,1)} %mod_ref.1, bf16[256,2048]{1,0:T(8,128)(2,1)} %lat_ref.5), custom_call_target="tpu_custom_call" | custom-call | flops 1000000 | tf_op jit(solution)/shard_map/entry/pallas_call | solution.py:360
  2.4 11.5 %all-to-all-start = ((bf16[64,8,384]{2,1,0:T(8,128)(2,1)}), bf16[64,8,384]{2,1,0:T(8,128)(2,1)S(1)}, u32[]{:S(2)}, u32[]{:S(2)}) async-start(bf16[64,8,384]{2,1,0:T(8,128)(2,1)} %get-tuple-element.16), calls=%async_computation | async-start | bytes 786432 | tf_op jit(solution)/shard_map/all_to_all | solution.py:421
  14.0 1.6 %collective-permute-start = (bf16[128,2048]{1,0:T(8,128)(2,1)}, bf16[128,2048]{1,0:T(8,128)(2,1)}, u32[]{:S(2)}, u32[]{:S(2)}) collective-permute-start(bf16[128,2048]{1,0:T(8,128)(2,1)} %get-tuple-element.17.after_ref), channel_id=1, source_target_pairs={{0,2},{2,0},{4,6},{6,4},{8,10},{10,8},{12,14},{14,12},{16,18},{18,... | collective-permute-start | bytes 1572872 | tf_op jit(solution)/shard_map/ppermute | solution.py:424
  15.6 1.5 %collective-permute-start.1 = (bf16[128,2048]{1,0:T(8,128)(2,1)}, bf16[128,2048]{1,0:T(8,128)(2,1)}, u32[]{:S(2)}, u32[]{:S(2)}) collective-permute-start(bf16[128,2048]{1,0:T(8,128)(2,1)} %get-tuple-element.22), channel_id=1, source_target_pairs={{2,4},{4,2},{6,8},{8,6},{10,12},{12,10},{14,16},{16,14},{18,20},{2... | collective-permute-start | bytes 1572872 | tf_op jit(solution)/shard_map/ppermute | solution.py:425
  17.1 1.7 %prep.1 = (f32[72,2048]{1,0:T(8,128)S(1)}, bf16[2048,256]{1,0:T(8,128)(2,1)S(1)}, bf16[2048,256]{1,0:T(8,128)(2,1)S(1)}) custom-call(bf16[128,2048]{1,0:T(8,128)(2,1)} %get-tuple-element.17.after_ref, bf16[64,2048]{1,0:T(8,128)(2,1)} %ctx_ref.1, f32[1,2048]{1,0:T(1,128)} %bitcast.8, bf16[2048,256]{1,0:T(8,128)(2,1)} %wk_ref.3, bf16[2048,256]{1,0:T(8,128)(2,1)} %wv_ref.3), custom_call_target="tpu_custom_call" | custom-call | flops 2000000000 | tf_op jit(solution)/shard_map/prep/pallas_call | solution.py:360
  18.8 0.0 copy-start.3
  18.8 0.0 copy-start.4
  18.8 0.0 copy-start
  18.8 0.0 copy-start.1
  18.8 0.0 copy-start.2
  18.8 8.4 %all-to-all-done.recv_ref = bf16[64,8,384]{2,1,0:T(8,128)(2,1)S(1)} async-done(((bf16[64,8,384]{2,1,0:T(8,128)(2,1)}), bf16[64,8,384]{2,1,0:T(8,128)(2,1)S(1)}, u32[]{:S(2)}, u32[]{:S(2)}) %all-to-all-start) | async-done | bytes 393248 | tf_op jit(solution)/shard_map/all_to_all | solution.py:421
  27.3 1.6 %context.1 = (bf16[16,64,512]{2,1,0:T(8,128)(2,1)}, f32[8,2048]{1,0:T(8,128)}) custom-call(bf16[64,8,384]{2,1,0:T(8,128)(2,1)S(1)} %all-to-all-done.recv_ref, f32[72,2048]{1,0:T(8,128)S(1)} %get-tuple-element.18.ng_ref, bf16[2048,256]{1,0:T(8,128)(2,1)S(1)} %get-tuple-element.19.wk_ref, bf16[2048,256]{1,0:T(8,128)(2,1)S(1)} %get-tuple-element.20.wv_ref), custom_call_target="tpu_custom_call" | custom-call | flops 1000000 | tf_op jit(solution)/shard_map/context/pallas_call | solution.py:360
  28.9 3.8 %all-to-all-start.1 = ((bf16[16,64,512]{2,1,0:T(8,128)(2,1)}), bf16[16,64,512]{2,1,0:T(8,128)(2,1)S(1)}, u32[]{:S(2)}, u32[]{:S(2)}) async-start(bf16[16,64,512]{2,1,0:T(8,128)(2,1)} %get-tuple-element.24), calls=%async_computation.1 | async-start | bytes 2097152 | tf_op jit(solution)/shard_map/all_to_all | solution.py:437
  32.8 0.0 copy-done.3
  32.8 0.0 copy-done.4
  32.8 0.1 fusion.1
  32.9 0.0 collective-permute-done.one_ref
  32.9 0.0 collective-permute-done.1.two_ref
  32.9 0.0 copy-done
  32.9 0.0 copy-done.1
  32.9 0.0 copy-done.2
  32.9 9.3 %local.1 = (bf16[256,1024]{1,0:T(8,128)(2,1)S(1)}, f32[256,1024]{1,0:T(8,128)S(1)}, f32[256,128]{1,0:T(8,128)S(1)}) custom-call(f32[16]{0:T(128)S(1)} %copy-done, f32[8,2048]{1,0:T(8,128)} %get-tuple-element.21.vec_ref, bf16[256,2048]{1,0:T(8,128)(2,1)} %lat_ref.5, bf16[128,2048]{1,0:T(8,128)(2,1)} %collective-permute-done.one_ref, ...), custom_call_target="tpu_custom_call" | custom-call | flops 10000000000 | tf_op jit(solution)/shard_map/local/pallas_call | solution.py:360
  42.3 6.5 %all-to-all-done.1 = bf16[16,64,512]{2,1,0:T(8,128)(2,1)S(1)} async-done(((bf16[16,64,512]{2,1,0:T(8,128)(2,1)}), bf16[16,64,512]{2,1,0:T(8,128)(2,1)S(1)}, u32[]{:S(2)}, u32[]{:S(2)}) %all-to-all-start.1) | async-done | bytes 1048608 | tf_op jit(solution)/shard_map/all_to_all | solution.py:437
  48.8 8.8 %final.1 = bf16[256,2048]{1,0:T(8,128)(2,1)} custom-call(bf16[256,1024]{1,0:T(8,128)(2,1)S(1)} %get-tuple-element.23.q_ref, bf16[1024,512]{1,0:T(8,128)(2,1)S(1)} %bitcast.5, f32[256,1024]{1,0:T(8,128)S(1)} %get-tuple-element.25.o_ref, f32[256,128]{1,0:T(8,128)S(1)} %get-tuple-element.26.lse_ref, bf16[1024,2048]{1,0:T(8,128)(2,1)} %wo_ref.1, ...), custom_call_target="tpu_custom_call" | custom-call | flops 10000000000 | tf_op jit(solution)/shard_map/final/pallas_call | solution.py:360
  (1 shorter events, 0.0 us)
Async XLA Ops:
  2.4 24.9 %all-to-all-start = ((bf16[64,8,384]{2,1,0:T(8,128)(2,1)}), bf16[64,8,384]{2,1,0:T(8,128)(2,1)S(1)}, u32[]{:S(2)}, u32[]{:S(2)}) async-start(bf16[64,8,384]{2,1,0:T(8,128)(2,1)} %get-tuple-element.16), calls=%async_computation | async-start | bytes 786432 | tf_op jit(solution)/shard_map/all_to_all | solution.py:421
  14.0 18.9 %collective-permute-start = (bf16[128,2048]{1,0:T(8,128)(2,1)}, bf16[128,2048]{1,0:T(8,128)(2,1)}, u32[]{:S(2)}, u32[]{:S(2)}) collective-permute-start(bf16[128,2048]{1,0:T(8,128)(2,1)} %get-tuple-element.17.after_ref), channel_id=1, source_target_pairs={{0,2},{2,0},{4,6},{6,4},{8,10},{10,8},{12,14},{14,12},{16,18},{18,... | collective-permute-start | bytes 1572872 | tf_op jit(solution)/shard_map/ppermute | solution.py:424
  15.6 17.3 %collective-permute-start.1 = (bf16[128,2048]{1,0:T(8,128)(2,1)}, bf16[128,2048]{1,0:T(8,128)(2,1)}, u32[]{:S(2)}, u32[]{:S(2)}) collective-permute-start(bf16[128,2048]{1,0:T(8,128)(2,1)} %get-tuple-element.22), channel_id=1, source_target_pairs={{2,4},{4,2},{6,8},{8,6},{10,12},{12,10},{14,16},{16,14},{18,20},{2... | collective-permute-start | bytes 1572872 | tf_op jit(solution)/shard_map/ppermute | solution.py:425
  18.8 14.0 %copy-start.3 = (f32[256]{0:T(256)S(1)}, f32[256]{0:T(256)}, u32[]{:S(2)}) copy-start(f32[256]{0:T(256)} %constant.26.clone) | copy-start | bytes 3076
  18.8 14.0 %copy-start.4 = (f32[256]{0:T(256)S(1)}, f32[256]{0:T(256)}, u32[]{:S(2)}) copy-start(f32[256]{0:T(256)} %constant.27.clone) | copy-start | bytes 3076
  18.8 14.1 %copy-start = (f32[16]{0:T(128)S(1)}, f32[16]{0:T(128)}, u32[]{:S(2)}) copy-start(f32[16]{0:T(128)} %sink_ref.1) | copy-start | bytes 196
  18.8 14.1 %copy-start.1 = (f32[64,256]{1,0:T(8,128)S(1)}, f32[64,256]{1,0:T(8,128)}, u32[]{:S(2)}) copy-start(f32[64,256]{1,0:T(8,128)} %constant.24.clone.colc_ref) | copy-start | bytes 196612
  18.8 14.1 %copy-start.2 = (f32[64,256]{1,0:T(8,128)S(1)}, f32[64,256]{1,0:T(8,128)}, u32[]{:S(2)}) copy-start(f32[64,256]{1,0:T(8,128)} %constant.25.clone.cols_ref) | copy-start | bytes 196612
  28.9 19.9 %all-to-all-start.1 = ((bf16[16,64,512]{2,1,0:T(8,128)(2,1)}), bf16[16,64,512]{2,1,0:T(8,128)(2,1)S(1)}, u32[]{:S(2)}, u32[]{:S(2)}) async-start(bf16[16,64,512]{2,1,0:T(8,128)(2,1)} %get-tuple-element.24), calls=%async_computation.1 | async-start | bytes 2097152 | tf_op jit(solution)/shard_map/all_to_all | solution.py:437

commit v9 on v8

--- a/solution.py
+++ b/solution.py
@@ -292,8 +292,9 @@
         c.start()
     low = iota((256, 128), 1) < HEAD_DIM
     eye = identity()
+    keys = dot_nt(eye, kv_ref[:, 0:256]).astype(BF16)
     for a in range(2):
-        kt_v[a] = dot_nt(eye[a * 128 : a * 128 + 128], kv_ref[:, 0:256]).astype(BF16)
+        kt_v[a] = keys[a * 128 : a * 128 + 128]
         va_v[a, :, 0:128] = kv_ref[:, 256 + a * 128 : 384 + a * 128]
         va_v[a, :, 128:256] = jnp.ones((1024, 128), BF16)
 
@@ -332,13 +333,14 @@
     for c in ins:
         c.wait()
     scores(7, odd_v)
+    part = dot(mix_v[:, 0:768], wo_v[0:768])
     attend(6, even_v)
     attend(7, odd_v)
     scale = vec_v[2:3, :] * gain_v[...]
     outs = []
     for b in range(2):
         rows = slice(b * 128, b * 128 + 128)
-        projected = dot(mix_v[rows, :], wo_v[...])
+        projected = part[rows] + dot(mix_v[rows, 768:1024], wo_v[768:1024])
         rs = lax.rsqrt(jnp.mean(projected * projected, axis=-1, keepdims=True) + EPSILON)
         out_v[rows, :] = (lat_v[rows, :].astype(F32) + projected * rs * scale).astype(BF16)
         there = pl.ds(b * 128, 128)

time: 58.3 us -> 58.1 us (level)
  no operation moved by 1% of the time
where the time goes in v9:
time: 58.1 us; the launch traced here: 57.6 us
  Pallas kernels  23.7 us (41%)
  starting transfers between devices  18.5 us (32%)
  waiting for transfers between devices  15 us (26%)
    pallas_call x5, Pallas kernels, call(): pl.pallas_call(kernel, out_shape=[FIXED.get(k, jax.ShapeDtypeStruct)(s, d...  23.7 us
    all_to_all x1, starting transfers between devices, shards(): recv = lax.all_to_all(parts, both, 0, 0, tiled=True)  11.5 us
    all_to_all x1, waiting for transfers between devices, shards(): recv = lax.all_to_all(parts, both, 0, 0, tiled=True)  8.45 us
    all_to_all x1, waiting for transfers between devices, shards(): lax.all_to_all(send, 'sp', 0, 0, tiled=True).reshape(sp_size * 64, 512)  6.51 us
    all_to_all x1, starting transfers between devices, shards(): lax.all_to_all(send, 'sp', 0, 0, tiled=True).reshape(sp_size * 64, 512)  3.85 us
    ppermute x1, starting transfers between devices, shards(): one = lax.ppermute(one, both, swap_one)  1.65 us
    ppermute x1, starting transfers between devices, shards(): two = lax.ppermute(two, both, swap_two)  1.47 us
  transfers between devices with their start and end apart: 4, of which 2 were waited for; matrix products, arithmetic and copies ran while one was open for 0% of the time, Pallas kernels for 22%

profile of v9, /device:TPU:0, one launch (start us, length us, event | category | flops | bytes accessed | tf_op | source)
XLA Modules:
  0.0 57.6 jit_solution(3458087520282020895)
XLA Ops:
  0.0 2.4 %entry.1 = (bf16[64,8,384]{2,1,0:T(8,128)(2,1)}, bf16[128,2048]{1,0:T(8,128)(2,1)}, bf16[128,2048]{1,0:T(8,128)(2,1)}) custom-call(bf16[16,128]{1,0:T(8,128)(2,1)} %bitcast.6, bf16[16,128]{1,0:T(8,128)(2,1)} %bitcast.7, bf16[3,128,512]{2,1,0:T(8,128)(2,1)} %mod_ref.1, bf16[256,2048]{1,0:T(8,128)(2,1)} %lat_ref.5), custom_call_target="tpu_custom_call" | custom-call | flops 1000000 | tf_op jit(solution)/shard_map/entry/pallas_call | solution.py:362
  2.4 11.5 %all-to-all-start = ((bf16[64,8,384]{2,1,0:T(8,128)(2,1)}), bf16[64,8,384]{2,1,0:T(8,128)(2,1)S(1)}, u32[]{:S(2)}, u32[]{:S(2)}) async-start(bf16[64,8,384]{2,1,0:T(8,128)(2,1)} %get-tuple-element.16), calls=%async_computation | async-start | bytes 786432 | tf_op jit(solution)/shard_map/all_to_all | solution.py:423
  14.0 1.6 %collective-permute-start = (bf16[128,2048]{1,0:T(8,128)(2,1)}, bf16[128,2048]{1,0:T(8,128)(2,1)}, u32[]{:S(2)}, u32[]{:S(2)}) collective-permute-start(bf16[128,2048]{1,0:T(8,128)(2,1)} %get-tuple-element.17.after_ref), channel_id=1, source_target_pairs={{0,2},{2,0},{4,6},{6,4},{8,10},{10,8},{12,14},{14,12},{16,18},{18,... | collective-permute-start | bytes 1572872 | tf_op jit(solution)/shard_map/ppermute | solution.py:426
  15.6 1.5 %collective-permute-start.1 = (bf16[128,2048]{1,0:T(8,128)(2,1)}, bf16[128,2048]{1,0:T(8,128)(2,1)}, u32[]{:S(2)}, u32[]{:S(2)}) collective-permute-start(bf16[128,2048]{1,0:T(8,128)(2,1)} %get-tuple-element.22), channel_id=1, source_target_pairs={{2,4},{4,2},{6,8},{8,6},{10,12},{12,10},{14,16},{16,14},{18,20},{2... | collective-permute-start | bytes 1572872 | tf_op jit(solution)/shard_map/ppermute | solution.py:427
  17.1 1.7 %prep.1 = (f32[72,2048]{1,0:T(8,128)S(1)}, bf16[2048,256]{1,0:T(8,128)(2,1)S(1)}, bf16[2048,256]{1,0:T(8,128)(2,1)S(1)}) custom-call(bf16[128,2048]{1,0:T(8,128)(2,1)} %get-tuple-element.17.after_ref, bf16[64,2048]{1,0:T(8,128)(2,1)} %ctx_ref.1, f32[1,2048]{1,0:T(1,128)} %bitcast.8, bf16[2048,256]{1,0:T(8,128)(2,1)} %wk_ref.3, bf16[2048,256]{1,0:T(8,128)(2,1)} %wv_ref.3), custom_call_target="tpu_custom_call" | custom-call | flops 2000000000 | tf_op jit(solution)/shard_map/prep/pallas_call | solution.py:362
  18.8 0.0 copy-start.3
  18.8 0.0 copy-start.4
  18.8 0.0 copy-start
  18.8 0.0 copy-start.1
  18.8 0.0 copy-start.2
  18.8 8.4 %all-to-all-done.recv_ref = bf16[64,8,384]{2,1,0:T(8,128)(2,1)S(1)} async-done(((bf16[64,8,384]{2,1,0:T(8,128)(2,1)}), bf16[64,8,384]{2,1,0:T(8,128)(2,1)S(1)}, u32[]{:S(2)}, u32[]{:S(2)}) %all-to-all-start) | async-done | bytes 393248 | tf_op jit(solution)/shard_map/all_to_all | solution.py:423
  27.3 1.6 %context.1 = (bf16[16,64,512]{2,1,0:T(8,128)(2,1)}, f32[8,2048]{1,0:T(8,128)}) custom-call(bf16[64,8,384]{2,1,0:T(8,128)(2,1)S(1)} %all-to-all-done.recv_ref, f32[72,2048]{1,0:T(8,128)S(1)} %get-tuple-element.18.ng_ref, bf16[2048,256]{1,0:T(8,128)(2,1)S(1)} %get-tuple-element.19.wk_ref, bf16[2048,256]{1,0:T(8,128)(2,1)S(1)} %get-tuple-element.20.wv_ref), custom_call_target="tpu_custom_call" | custom-call | flops 1000000 | tf_op jit(solution)/shard_map/context/pallas_call | solution.py:362
  28.9 3.8 %all-to-all-start.1 = ((bf16[16,64,512]{2,1,0:T(8,128)(2,1)}), bf16[16,64,512]{2,1,0:T(8,128)(2,1)S(1)}, u32[]{:S(2)}, u32[]{:S(2)}) async-start(bf16[16,64,512]{2,1,0:T(8,128)(2,1)} %get-tuple-element.24), calls=%async_computation.1 | async-start | bytes 2097152 | tf_op jit(solution)/shard_map/all_to_all | solution.py:439
  32.8 0.0 copy-done.3
  32.8 0.0 copy-done.4
  32.8 0.1 fusion.1
  32.9 0.0 collective-permute-done.one_ref
  32.9 0.0 collective-permute-done.1.two_ref
  32.9 0.0 copy-done
  32.9 0.0 copy-done.1
  32.9 0.0 copy-done.2
  32.9 9.3 %local.1 = (bf16[256,1024]{1,0:T(8,128)(2,1)S(1)}, f32[256,1024]{1,0:T(8,128)S(1)}, f32[256,128]{1,0:T(8,128)S(1)}) custom-call(f32[16]{0:T(128)S(1)} %copy-done, f32[8,2048]{1,0:T(8,128)} %get-tuple-element.21.vec_ref, bf16[256,2048]{1,0:T(8,128)(2,1)} %lat_ref.5, bf16[128,2048]{1,0:T(8,128)(2,1)} %collective-permute-done.one_ref, ...), custom_call_target="tpu_custom_call" | custom-call | flops 10000000000 | tf_op jit(solution)/shard_map/local/pallas_call | solution.py:362
  42.3 6.5 %all-to-all-done.1 = bf16[16,64,512]{2,1,0:T(8,128)(2,1)S(1)} async-done(((bf16[16,64,512]{2,1,0:T(8,128)(2,1)}), bf16[16,64,512]{2,1,0:T(8,128)(2,1)S(1)}, u32[]{:S(2)}, u32[]{:S(2)}) %all-to-all-start.1) | async-done | bytes 1048608 | tf_op jit(solution)/shard_map/all_to_all | solution.py:439
  48.8 8.6 %final.1 = bf16[256,2048]{1,0:T(8,128)(2,1)} custom-call(bf16[256,1024]{1,0:T(8,128)(2,1)S(1)} %get-tuple-element.23.q_ref, bf16[1024,512]{1,0:T(8,128)(2,1)S(1)} %bitcast.5, f32[256,1024]{1,0:T(8,128)S(1)} %get-tuple-element.25.o_ref, f32[256,128]{1,0:T(8,128)S(1)} %get-tuple-element.26.lse_ref, bf16[1024,2048]{1,0:T(8,128)(2,1)} %wo_ref.1, ...), custom_call_target="tpu_custom_call" | custom-call | flops 10000000000 | tf_op jit(solution)/shard_map/final/pallas_call | solution.py:362
  (1 shorter events, 0.0 us)
Async XLA Ops:
  2.4 24.9 %all-to-all-start = ((bf16[64,8,384]{2,1,0:T(8,128)(2,1)}), bf16[64,8,384]{2,1,0:T(8,128)(2,1)S(1)}, u32[]{:S(2)}, u32[]{:S(2)}) async-start(bf16[64,8,384]{2,1,0:T(8,128)(2,1)} %get-tuple-element.16), calls=%async_computation | async-start | bytes 786432 | tf_op jit(solution)/shard_map/all_to_all | solution.py:423
  14.0 18.9 %collective-permute-start = (bf16[128,2048]{1,0:T(8,128)(2,1)}, bf16[128,2048]{1,0:T(8,128)(2,1)}, u32[]{:S(2)}, u32[]{:S(2)}) collective-permute-start(bf16[128,2048]{1,0:T(8,128)(2,1)} %get-tuple-element.17.after_ref), channel_id=1, source_target_pairs={{0,2},{2,0},{4,6},{6,4},{8,10},{10,8},{12,14},{14,12},{16,18},{18,... | collective-permute-start | bytes 1572872 | tf_op jit(solution)/shard_map/ppermute | solution.py:426
  15.6 17.3 %collective-permute-start.1 = (bf16[128,2048]{1,0:T(8,128)(2,1)}, bf16[128,2048]{1,0:T(8,128)(2,1)}, u32[]{:S(2)}, u32[]{:S(2)}) collective-permute-start(bf16[128,2048]{1,0:T(8,128)(2,1)} %get-tuple-element.22), channel_id=1, source_target_pairs={{2,4},{4,2},{6,8},{8,6},{10,12},{12,10},{14,16},{16,14},{18,20},{2... | collective-permute-start | bytes 1572872 | tf_op jit(solution)/shard_map/ppermute | solution.py:427
  18.8 14.0 %copy-start.3 = (f32[256]{0:T(256)S(1)}, f32[256]{0:T(256)}, u32[]{:S(2)}) copy-start(f32[256]{0:T(256)} %constant.26.clone) | copy-start | bytes 3076
  18.8 14.0 %copy-start.4 = (f32[256]{0:T(256)S(1)}, f32[256]{0:T(256)}, u32[]{:S(2)}) copy-start(f32[256]{0:T(256)} %constant.27.clone) | copy-start | bytes 3076
  18.8 14.1 %copy-start = (f32[16]{0:T(128)S(1)}, f32[16]{0:T(128)}, u32[]{:S(2)}) copy-start(f32[16]{0:T(128)} %sink_ref.1) | copy-start | bytes 196
  18.8 14.1 %copy-start.1 = (f32[64,256]{1,0:T(8,128)S(1)}, f32[64,256]{1,0:T(8,128)}, u32[]{:S(2)}) copy-start(f32[64,256]{1,0:T(8,128)} %constant.24.clone.colc_ref) | copy-start | bytes 196612
  18.8 14.1 %copy-start.2 = (f32[64,256]{1,0:T(8,128)S(1)}, f32[64,256]{1,0:T(8,128)}, u32[]{:S(2)}) copy-start(f32[64,256]{1,0:T(8,128)} %constant.25.clone.cols_ref) | copy-start | bytes 196612
  28.9 19.9 %all-to-all-start.1 = ((bf16[16,64,512]{2,1,0:T(8,128)(2,1)}), bf16[16,64,512]{2,1,0:T(8,128)(2,1)S(1)}, u32[]{:S(2)}, u32[]{:S(2)}) async-start(bf16[16,64,512]{2,1,0:T(8,128)(2,1)} %get-tuple-element.24), calls=%async_computation.1 | async-start | bytes 2097152 | tf_op jit(solution)/shard_map/all_to_all | solution.py:439

commit v10 on v7

--- a/solution.py
+++ b/solution.py
@@ -73,12 +73,11 @@
     ins[0].wait()
     parts = [dot(v, mod_v[i]) for i in range(3)]
     five = (parts[0][0:1], parts[0][1:2], parts[1][0:1], parts[1][1:2], parts[2][0:1])
-    zero = jnp.zeros((1, 128), F32)
     rows = []
     for j in range(4):
-        cut = [x[:, j * 128 : (j + 1) * 128] for x in five]
-        rows.append(jnp.concatenate(cut[:3], axis=1))
-        rows.append(jnp.concatenate(cut[3:] + [zero], axis=1))
+        exact = jnp.concatenate([x[:, j * 128 : (j + 1) * 128] for x in five], axis=1)
+        high = exact.astype(BF16).astype(F32)
+        rows += [high, exact - high]
     block = jnp.concatenate(rows, axis=0).astype(BF16)
     for i in range(block_v.shape[0]):
         block_v[i] = block
@@ -126,8 +125,8 @@
         cuts = []
         for t in range(4):
             for j in range(4):
-                r, c = 2 * j + v // 3, (v % 3) * 128
-                cuts.append(sums[t][r : r + 1, c : c + 128])
+                both = sums[t][2 * j : 2 * j + 2, v * 128 : v * 128 + 128]
+                cuts.append(both[0:1] + both[1:2])
         return jnp.concatenate(cuts, axis=1)
 
     hidden = (ng_ref[0:64, :] * (1.0 + vector(3)) + vector(1)).astype(BF16)
@@ -291,8 +290,9 @@
         c.start()
     low = iota((256, 128), 1) < HEAD_DIM
     eye = identity()
+    keys = dot_nt(eye, kv_ref[:, 0:256]).astype(BF16)
     for a in range(2):
-        kt_v[a] = dot_nt(eye[a * 128 : a * 128 + 128], kv_ref[:, 0:256]).astype(BF16)
+        kt_v[a] = keys[a * 128 : a * 128 + 128]
         va_v[a, :, 0:128] = kv_ref[:, 256 + a * 128 : 384 + a * 128]
         va_v[a, :, 128:256] = jnp.ones((1024, 128), BF16)
 
@@ -323,18 +323,22 @@
         i = 2 * j
         scores(i + 1, odd_v)
         attend(i, even_v)
-        scores(jnp.minimum(i + 2, 7), even_v)
+        scores(i + 2, even_v)
         attend(i + 1, odd_v)
         return carry
 
-    lax.fori_loop(0, 4, two, 0)
+    lax.fori_loop(0, 3, two, 0)
     for c in ins:
         c.wait()
+    scores(7, odd_v)
+    part = dot(mix_v[:, 0:768], wo_v[0:768])
+    attend(6, even_v)
+    attend(7, odd_v)
     scale = vec_v[2:3, :] * gain_v[...]
     outs = []
     for b in range(2):
         rows = slice(b * 128, b * 128 + 128)
-        projected = dot(mix_v[rows, :], wo_v[...])
+        projected = part[rows] + dot(mix_v[rows, 768:1024], wo_v[768:1024])
         rs = lax.rsqrt(jnp.mean(projected * projected, axis=-1, keepdims=True) + EPSILON)
         out_v[rows, :] = (lat_v[rows, :].astype(F32) + projected * rs * scale).astype(BF16)
         there = pl.ds(b * 128, 128)
@@ -390,13 +394,13 @@
         entry_kernel,
         "entry",
         "hhhh",
-        [("h", (count, 8, 384), BF16), ("h", half, BF16), ("h", half, BF16)],
+        [("h", (count, 8, 640), BF16), ("h", half, BF16), ("h", half, BF16)],
         [
             (square, BF16),
             (square, BF16),
             (mod_weight.shape, BF16),
             (latent.shape, BF16),
-            ((count, 8, 384), BF16),
+            ((count, 8, 640), BF16),
         ],
         7,
         (cond.reshape(square), ctx_cond.reshape(square), mod_weight, latent),

time: 59.5 us -> 66.1 us (1.11)
  the two profiles are of different devices: /device:TPU:0 before, /device:TPU:6 now
where the time goes in v10:
time: 66.1 us; the launch traced here: 65.7 us
  Pallas kernels  24.7 us (37%)
  starting transfers between devices  23 us (35%)
  waiting for transfers between devices  17.6 us (27%)
    pallas_call x5, Pallas kernels, call(): pl.pallas_call(kernel, out_shape=[FIXED.get(k, jax.ShapeDtypeStruct)(s, d...  24.7 us
    all_to_all x1, waiting for transfers between devices, shards(): recv = lax.all_to_all(parts, both, 0, 0, tiled=True)  14 us
    all_to_all x1, starting transfers between devices, shards(): recv = lax.all_to_all(parts, both, 0, 0, tiled=True)  11.5 us
    all_to_all x1, starting transfers between devices, shards(): lax.all_to_all(send, 'sp', 0, 0, tiled=True).reshape(sp_size * 64, 512)  6.6 us
    ppermute x1, starting transfers between devices, shards(): two = lax.ppermute(two, both, swap_two)  3.97 us
    all_to_all x1, waiting for transfers between devices, shards(): lax.all_to_all(send, 'sp', 0, 0, tiled=True).reshape(sp_size * 64, 512)  3.62 us
  transfers between devices with their start and end apart: 4, of which 2 were waited for; matrix products, arithmetic and copies ran while one was open for 0% of the time, Pallas kernels for 20%

profile of v10, /device:TPU:6, one launch (start us, length us, event | category | flops | bytes accessed | tf_op | source)
XLA Modules:
  0.0 65.7 jit_solution(16391286073377544469)
XLA Ops:
  0.0 2.4 %entry.1 = (bf16[64,8,640]{2,1,0:T(8,128)(2,1)}, bf16[128,2048]{1,0:T(8,128)(2,1)}, bf16[128,2048]{1,0:T(8,128)(2,1)}) custom-call(bf16[16,128]{1,0:T(8,128)(2,1)} %bitcast.6, bf16[16,128]{1,0:T(8,128)(2,1)} %bitcast.7, bf16[3,128,512]{2,1,0:T(8,128)(2,1)} %mod_ref.1, bf16[256,2048]{1,0:T(8,128)(2,1)} %lat_ref.5), custom_call_target="tpu_custom_call" | custom-call | flops 1000000 | tf_op jit(solution)/shard_map/entry/pallas_call | solution.py:360
  2.4 11.5 %all-to-all-start = ((bf16[64,8,640]{2,1,0:T(8,128)(2,1)}), bf16[64,8,640]{2,1,0:T(8,128)(2,1)S(1)}, u32[]{:S(2)}, u32[]{:S(2)}) async-start(bf16[64,8,640]{2,1,0:T(8,128)(2,1)} %get-tuple-element.16), calls=%async_computation | async-start | bytes 1310720 | tf_op jit(solution)/shard_map/all_to_all | solution.py:421
  13.9 0.9 %collective-permute-start = (bf16[128,2048]{1,0:T(8,128)(2,1)}, bf16[128,2048]{1,0:T(8,128)(2,1)}, u32[]{:S(2)}, u32[]{:S(2)}) collective-permute-start(bf16[128,2048]{1,0:T(8,128)(2,1)} %get-tuple-element.17.after_ref), channel_id=1, source_target_pairs={{0,2},{2,0},{4,6},{6,4},{8,10},{10,8},{12,14},{14,12},{16,18},{18,... | collective-permute-start | bytes 1572872 | tf_op jit(solution)/shard_map/ppermute | solution.py:424
  14.8 4.0 %collective-permute-start.1 = (bf16[128,2048]{1,0:T(8,128)(2,1)}, bf16[128,2048]{1,0:T(8,128)(2,1)}, u32[]{:S(2)}, u32[]{:S(2)}) collective-permute-start(bf16[128,2048]{1,0:T(8,128)(2,1)} %get-tuple-element.22), channel_id=1, source_target_pairs={{2,4},{4,2},{6,8},{8,6},{10,12},{12,10},{14,16},{16,14},{18,20},{2... | collective-permute-start | bytes 1572872 | tf_op jit(solution)/shard_map/ppermute | solution.py:425
  18.8 1.7 %prep.1 = (f32[72,2048]{1,0:T(8,128)S(1)}, bf16[2048,256]{1,0:T(8,128)(2,1)S(1)}, bf16[2048,256]{1,0:T(8,128)(2,1)S(1)}) custom-call(bf16[128,2048]{1,0:T(8,128)(2,1)} %get-tuple-element.17.after_ref, bf16[64,2048]{1,0:T(8,128)(2,1)} %ctx_ref.1, f32[1,2048]{1,0:T(1,128)} %bitcast.8, bf16[2048,256]{1,0:T(8,128)(2,1)} %wk_ref.3, bf16[2048,256]{1,0:T(8,128)(2,1)} %wv_ref.3), custom_call_target="tpu_custom_call" | custom-call | flops 2000000000 | tf_op jit(solution)/shard_map/prep/pallas_call | solution.py:360
  20.5 0.0 copy-start.3
  20.5 0.0 copy-start.4
  20.5 0.0 copy-start
  20.6 0.0 copy-start.1
  20.6 0.0 copy-start.2
  20.6 14.0 %all-to-all-done.recv_ref = bf16[64,8,640]{2,1,0:T(8,128)(2,1)S(1)} async-done(((bf16[64,8,640]{2,1,0:T(8,128)(2,1)}), bf16[64,8,640]{2,1,0:T(8,128)(2,1)S(1)}, u32[]{:S(2)}, u32[]{:S(2)}) %all-to-all-start) | async-done | bytes 655392 | tf_op jit(solution)/shard_map/all_to_all | solution.py:421
  34.6 1.6 %context.1 = (bf16[16,64,512]{2,1,0:T(8,128)(2,1)}, f32[8,2048]{1,0:T(8,128)}) custom-call(bf16[64,8,640]{2,1,0:T(8,128)(2,1)S(1)} %all-to-all-done.recv_ref, f32[72,2048]{1,0:T(8,128)S(1)} %get-tuple-element.18.ng_ref, bf16[2048,256]{1,0:T(8,128)(2,1)S(1)} %get-tuple-element.19.wk_ref, bf16[2048,256]{1,0:T(8,128)(2,1)S(1)} %get-tuple-element.20.wv_ref), custom_call_target="tpu_custom_call" | custom-call | flops 1000000 | tf_op jit(solution)/shard_map/context/pallas_call | solution.py:360
  36.2 6.6 %all-to-all-start.1 = ((bf16[16,64,512]{2,1,0:T(8,128)(2,1)}), bf16[16,64,512]{2,1,0:T(8,128)(2,1)S(1)}, u32[]{:S(2)}, u32[]{:S(2)}) async-start(bf16[16,64,512]{2,1,0:T(8,128)(2,1)} %get-tuple-element.24), calls=%async_computation.1 | async-start | bytes 2097152 | tf_op jit(solution)/shard_map/all_to_all | solution.py:437
  42.8 0.0 copy-done.3
  42.8 0.0 copy-done.4
  42.8 0.1 fusion.1
  42.9 0.0 collective-permute-done.one_ref
  42.9 0.0 collective-permute-done.1.two_ref
  42.9 0.0 copy-done
  43.0 0.0 copy-done.1
  43.0 0.0 copy-done.2
  43.0 9.5 %local.1 = (bf16[256,1024]{1,0:T(8,128)(2,1)S(1)}, f32[256,1024]{1,0:T(8,128)S(1)}, f32[256,128]{1,0:T(8,128)S(1)}) custom-call(f32[16]{0:T(128)S(1)} %copy-done, f32[8,2048]{1,0:T(8,128)} %get-tuple-element.21.vec_ref, bf16[256,2048]{1,0:T(8,128)(2,1)} %lat_ref.5, bf16[128,2048]{1,0:T(8,128)(2,1)} %collective-permute-done.one_ref, ...), custom_call_target="tpu_custom_call" | custom-call | flops 10000000000 | tf_op jit(solution)/shard_map/local/pallas_call | solution.py:360
  52.5 3.6 %all-to-all-done.1 = bf16[16,64,512]{2,1,0:T(8,128)(2,1)S(1)} async-done(((bf16[16,64,512]{2,1,0:T(8,128)(2,1)}), bf16[16,64,512]{2,1,0:T(8,128)(2,1)S(1)}, u32[]{:S(2)}, u32[]{:S(2)}) %all-to-all-start.1) | async-done | bytes 1048608 | tf_op jit(solution)/shard_map/all_to_all | solution.py:437
  56.1 9.5 %final.1 = bf16[256,2048]{1,0:T(8,128)(2,1)} custom-call(bf16[256,1024]{1,0:T(8,128)(2,1)S(1)} %get-tuple-element.23.q_ref, bf16[1024,512]{1,0:T(8,128)(2,1)S(1)} %bitcast.5, f32[256,1024]{1,0:T(8,128)S(1)} %get-tuple-element.25.o_ref, f32[256,128]{1,0:T(8,128)S(1)} %get-tuple-element.26.lse_ref, bf16[1024,2048]{1,0:T(8,128)(2,1)} %wo_ref.1, ...), custom_call_target="tpu_custom_call" | custom-call | flops 10000000000 | tf_op jit(solution)/shard_map/final/pallas_call | solution.py:360
  (1 shorter events, 0.0 us)
Async XLA Ops:
  2.4 32.1 %all-to-all-start = ((bf16[64,8,640]{2,1,0:T(8,128)(2,1)}), bf16[64,8,640]{2,1,0:T(8,128)(2,1)S(1)}, u32[]{:S(2)}, u32[]{:S(2)}) async-start(bf16[64,8,640]{2,1,0:T(8,128)(2,1)} %get-tuple-element.16), calls=%async_computation | async-start | bytes 1310720 | tf_op jit(solution)/shard_map/all_to_all | solution.py:421
  13.9 29.0 %collective-permute-start = (bf16[128,2048]{1,0:T(8,128)(2,1)}, bf16[128,2048]{1,0:T(8,128)(2,1)}, u32[]{:S(2)}, u32[]{:S(2)}) collective-permute-start(bf16[128,2048]{1,0:T(8,128)(2,1)} %get-tuple-element.17.after_ref), channel_id=1, source_target_pairs={{0,2},{2,0},{4,6},{6,4},{8,10},{10,8},{12,14},{14,12},{16,18},{18,... | collective-permute-start | bytes 1572872 | tf_op jit(solution)/shard_map/ppermute | solution.py:424
  14.8 28.1 %collective-permute-start.1 = (bf16[128,2048]{1,0:T(8,128)(2,1)}, bf16[128,2048]{1,0:T(8,128)(2,1)}, u32[]{:S(2)}, u32[]{:S(2)}) collective-permute-start(bf16[128,2048]{1,0:T(8,128)(2,1)} %get-tuple-element.22), channel_id=1, source_target_pairs={{2,4},{4,2},{6,8},{8,6},{10,12},{12,10},{14,16},{16,14},{18,20},{2... | collective-permute-start | bytes 1572872 | tf_op jit(solution)/shard_map/ppermute | solution.py:425
  20.5 22.3 %copy-start.3 = (f32[256]{0:T(256)S(1)}, f32[256]{0:T(256)}, u32[]{:S(2)}) copy-start(f32[256]{0:T(256)} %constant.26.clone) | copy-start | bytes 3076
  20.5 22.3 %copy-start.4 = (f32[256]{0:T(256)S(1)}, f32[256]{0:T(256)}, u32[]{:S(2)}) copy-start(f32[256]{0:T(256)} %constant.27.clone) | copy-start | bytes 3076
  20.5 22.4 %copy-start = (f32[16]{0:T(128)S(1)}, f32[16]{0:T(128)}, u32[]{:S(2)}) copy-start(f32[16]{0:T(128)} %sink_ref.1) | copy-start | bytes 196
  20.6 22.4 %copy-start.1 = (f32[64,256]{1,0:T(8,128)S(1)}, f32[64,256]{1,0:T(8,128)}, u32[]{:S(2)}) copy-start(f32[64,256]{1,0:T(8,128)} %constant.24.clone.colc_ref) | copy-start | bytes 196612
  20.6 22.4 %copy-start.2 = (f32[64,256]{1,0:T(8,128)S(1)}, f32[64,256]{1,0:T(8,128)}, u32[]{:S(2)}) copy-start(f32[64,256]{1,0:T(8,128)} %constant.25.clone.cols_ref) | copy-start | bytes 196612
  36.2 19.9 %all-to-all-start.1 = ((bf16[16,64,512]{2,1,0:T(8,128)(2,1)}), bf16[16,64,512]{2,1,0:T(8,128)(2,1)S(1)}, u32[]{:S(2)}, u32[]{:S(2)}) async-start(bf16[16,64,512]{2,1,0:T(8,128)(2,1)} %get-tuple-element.24), calls=%async_computation.1 | async-start | bytes 2097152 | tf_op jit(solution)/shard_map/all_to_all | solution.py:437

commit v11 on v10

--- a/solution.py
+++ b/solution.py
@@ -356,7 +356,7 @@
     return [pl.BlockSpec(memory_space=KINDS[k]) for k in kinds]
 
 
-def call(kernel, name, ins, outs, scratch, copies, args, flops, limit):
+def call(kernel, ins, outs, scratch, copies, args, flops, limit):
     return pl.pallas_call(
         kernel,
         out_shape=[FIXED.get(k, jax.ShapeDtypeStruct)(s, d) for k, s, d in outs],
@@ -366,7 +366,6 @@
         + [pltpu.SemaphoreType.DMA((copies,))],
         compiler_params=pltpu.CompilerParams(vmem_limit_bytes=limit * 1024 * 1024),
         cost_estimate=pl.CostEstimate(flops=flops, bytes_accessed=0, transcendentals=0),
-        name=name,
     )(
         *[
             pltpu.with_memory_space_constraint(x, FIXED[k]) if k in FIXED else x
@@ -392,7 +391,6 @@
 
     parts, one, two = call(
         entry_kernel,
-        "entry",
         "hhhh",
         [("h", (count, 8, 640), BF16), ("h", half, BF16), ("h", half, BF16)],
         [
@@ -409,7 +407,6 @@
     )
     ng, wk_near, wv_near = call(
         prep_kernel,
-        "prep",
         "hhhhh",
         [("V", (72, width), F32), ("V", small, BF16), ("V", small, BF16)],
         [(ctx_rows.shape, BF16), (line, F32)],
@@ -425,7 +422,6 @@
     two = lax.ppermute(two, both, swap_two)
     send, vecs = call(
         context_kernel,
-        "context",
         "vVVV",
         [("h", (sp_size, 64, 512), BF16), ("h", rest, F32)],
         [((64, 512), BF16), (rest, F32)],
@@ -448,7 +444,6 @@
 
     query, o, lse = call(
         local_kernel,
-        "local",
         "shhhhhhhvvvv",
         [("V", wide, BF16), ("V", wide, F32), ("V", (rows, 128), F32)],
         [
@@ -465,7 +460,6 @@
     )
     (updated,) = call(
         final_kernel,
-        "final",
         "VVVVhhhh",
         [("h", latent.shape, BF16)],
         [
@@ -503,6 +497,7 @@
         P(),
         P(),
     )
+
     return jax.shard_map(
         shards, mesh=mesh, in_specs=placed, out_specs=P(("dp", "sp", "tp"), None), check_vma=False
     )

time: 66.1 us -> 66.1 us (level)
  no operation moved by 1% of the time
where the time goes in v11:
time: 66.1 us; the launch traced here: 65.7 us
  Pallas kernels  24.7 us (37%)
  starting transfers between devices  23 us (35%)
  waiting for transfers between devices  17.6 us (27%)
    pallas_call x5, Pallas kernels, call(): pl.pallas_call(kernel, out_shape=[FIXED.get(k, jax.ShapeDtypeStruct)(s, d...  24.7 us
    all_to_all x1, waiting for transfers between devices, shards(): recv = lax.all_to_all(parts, both, 0, 0, tiled=True)  14 us
    all_to_all x1, starting transfers between devices, shards(): recv = lax.all_to_all(parts, both, 0, 0, tiled=True)  11.5 us
    all_to_all x1, starting transfers between devices, shards(): lax.all_to_all(send, 'sp', 0, 0, tiled=True).reshape(sp_size * 64, 512)  6.6 us
    ppermute x1, starting transfers between devices, shards(): two = lax.ppermute(two, both, swap_two)  3.97 us
    all_to_all x1, waiting for transfers between devices, shards(): lax.all_to_all(send, 'sp', 0, 0, tiled=True).reshape(sp_size * 64, 512)  3.62 us
  transfers between devices with their start and end apart: 4, of which 2 were waited for; matrix products, arithmetic and copies ran while one was open for 0% of the time, Pallas kernels for 20%

profile of v11, /device:TPU:6, one launch (start us, length us, event | category | flops | bytes accessed | tf_op | source)
XLA Modules:
  0.0 65.7 jit_solution(16391286073377544469)
XLA Ops:
  0.0 2.4 %shard_map.154 = (bf16[64,8,640]{2,1,0:T(8,128)(2,1)}, bf16[128,2048]{1,0:T(8,128)(2,1)}, bf16[128,2048]{1,0:T(8,128)(2,1)}) custom-call(bf16[16,128]{1,0:T(8,128)(2,1)} %bitcast.6, bf16[16,128]{1,0:T(8,128)(2,1)} %bitcast.7, bf16[3,128,512]{2,1,0:T(8,128)(2,1)} %mod_ref.1, bf16[256,2048]{1,0:T(8,128)(2,1)} %lat_ref.5), custom_call_target="tpu_custom_call" | custom-call | flops 1000000 | tf_op jit(solution)/shard_map/pallas_call | solution.py:360
  2.4 11.5 %all-to-all-start = ((bf16[64,8,640]{2,1,0:T(8,128)(2,1)}), bf16[64,8,640]{2,1,0:T(8,128)(2,1)S(1)}, u32[]{:S(2)}, u32[]{:S(2)}) async-start(bf16[64,8,640]{2,1,0:T(8,128)(2,1)} %get-tuple-element.16), calls=%async_computation | async-start | bytes 1310720 | tf_op jit(solution)/shard_map/all_to_all | solution.py:418
  13.9 0.9 %collective-permute-start = (bf16[128,2048]{1,0:T(8,128)(2,1)}, bf16[128,2048]{1,0:T(8,128)(2,1)}, u32[]{:S(2)}, u32[]{:S(2)}) collective-permute-start(bf16[128,2048]{1,0:T(8,128)(2,1)} %get-tuple-element.17.after_ref), channel_id=1, source_target_pairs={{0,2},{2,0},{4,6},{6,4},{8,10},{10,8},{12,14},{14,12},{16,18},{18,... | collective-permute-start | bytes 1572872 | tf_op jit(solution)/shard_map/ppermute | solution.py:421
  14.8 4.0 %collective-permute-start.1 = (bf16[128,2048]{1,0:T(8,128)(2,1)}, bf16[128,2048]{1,0:T(8,128)(2,1)}, u32[]{:S(2)}, u32[]{:S(2)}) collective-permute-start(bf16[128,2048]{1,0:T(8,128)(2,1)} %get-tuple-element.22), channel_id=1, source_target_pairs={{2,4},{4,2},{6,8},{8,6},{10,12},{12,10},{14,16},{16,14},{18,20},{2... | collective-permute-start | bytes 1572872 | tf_op jit(solution)/shard_map/ppermute | solution.py:422
  18.8 1.7 %shard_map.155 = (f32[72,2048]{1,0:T(8,128)S(1)}, bf16[2048,256]{1,0:T(8,128)(2,1)S(1)}, bf16[2048,256]{1,0:T(8,128)(2,1)S(1)}) custom-call(bf16[128,2048]{1,0:T(8,128)(2,1)} %get-tuple-element.17.after_ref, bf16[64,2048]{1,0:T(8,128)(2,1)} %ctx_ref.1, f32[1,2048]{1,0:T(1,128)} %bitcast.8, bf16[2048,256]{1,0:T(8,128)(2,1)} %wk_ref.3, bf16[2048,256]{1,0:T(8,128)(2,1)} %wv_ref.3), custom_call_target="tpu_custom_call" | custom-call | flops 2000000000 | tf_op jit(solution)/shard_map/pallas_call | solution.py:360
  20.5 0.0 copy-start.3
  20.5 0.0 copy-start.4
  20.5 0.0 copy-start
  20.6 0.0 copy-start.1
  20.6 0.0 copy-start.2
  20.6 14.0 %all-to-all-done.recv_ref = bf16[64,8,640]{2,1,0:T(8,128)(2,1)S(1)} async-done(((bf16[64,8,640]{2,1,0:T(8,128)(2,1)}), bf16[64,8,640]{2,1,0:T(8,128)(2,1)S(1)}, u32[]{:S(2)}, u32[]{:S(2)}) %all-to-all-start) | async-done | bytes 655392 | tf_op jit(solution)/shard_map/all_to_all | solution.py:418
  34.6 1.6 %shard_map.156 = (bf16[16,64,512]{2,1,0:T(8,128)(2,1)}, f32[8,2048]{1,0:T(8,128)}) custom-call(bf16[64,8,640]{2,1,0:T(8,128)(2,1)S(1)} %all-to-all-done.recv_ref, f32[72,2048]{1,0:T(8,128)S(1)} %get-tuple-element.18.ng_ref, bf16[2048,256]{1,0:T(8,128)(2,1)S(1)} %get-tuple-element.19.wk_ref, bf16[2048,256]{1,0:T(8,128)(2,1)S(1)} %get-tuple-element.20.wv_ref), custom_call_target="tpu_custom_call" | custom-call | flops 1000000 | tf_op jit(solution)/shard_map/pallas_call | solution.py:360
  36.2 6.6 %all-to-all-start.1 = ((bf16[16,64,512]{2,1,0:T(8,128)(2,1)}), bf16[16,64,512]{2,1,0:T(8,128)(2,1)S(1)}, u32[]{:S(2)}, u32[]{:S(2)}) async-start(bf16[16,64,512]{2,1,0:T(8,128)(2,1)} %get-tuple-element.24), calls=%async_computation.1 | async-start | bytes 2097152 | tf_op jit(solution)/shard_map/all_to_all | solution.py:433
  42.8 0.0 copy-done.3
  42.8 0.0 copy-done.4
  42.8 0.1 fusion.1
  42.9 0.0 collective-permute-done.one_ref
  42.9 0.0 collective-permute-done.1.two_ref
  42.9 0.0 copy-done
  43.0 0.0 copy-done.1
  43.0 0.0 copy-done.2
  43.0 9.5 %shard_map.157 = (bf16[256,1024]{1,0:T(8,128)(2,1)S(1)}, f32[256,1024]{1,0:T(8,128)S(1)}, f32[256,128]{1,0:T(8,128)S(1)}) custom-call(f32[16]{0:T(128)S(1)} %copy-done, f32[8,2048]{1,0:T(8,128)} %get-tuple-element.21.vec_ref, bf16[256,2048]{1,0:T(8,128)(2,1)} %lat_ref.5, bf16[128,2048]{1,0:T(8,128)(2,1)} %collective-permute-done.one_ref, ...), custom_call_target="tpu_custom_call" | custom-call | flops 10000000000 | tf_op jit(solution)/shard_map/pallas_call | solution.py:360
  52.5 3.6 %all-to-all-done.1 = bf16[16,64,512]{2,1,0:T(8,128)(2,1)S(1)} async-done(((bf16[16,64,512]{2,1,0:T(8,128)(2,1)}), bf16[16,64,512]{2,1,0:T(8,128)(2,1)S(1)}, u32[]{:S(2)}, u32[]{:S(2)}) %all-to-all-start.1) | async-done | bytes 1048608 | tf_op jit(solution)/shard_map/all_to_all | solution.py:433
  56.1 9.5 %shard_map.158 = bf16[256,2048]{1,0:T(8,128)(2,1)} custom-call(bf16[256,1024]{1,0:T(8,128)(2,1)S(1)} %get-tuple-element.23.q_ref, bf16[1024,512]{1,0:T(8,128)(2,1)S(1)} %bitcast.5, f32[256,1024]{1,0:T(8,128)S(1)} %get-tuple-element.25.o_ref, f32[256,128]{1,0:T(8,128)S(1)} %get-tuple-element.26.lse_ref, bf16[1024,2048]{1,0:T(8,128)(2,1)} %wo_ref.1, ...), custom_call_target="tpu_custom_call" | custom-call | flops 10000000000 | tf_op jit(solution)/shard_map/pallas_call | solution.py:360
  (1 shorter events, 0.0 us)
Async XLA Ops:
  2.4 32.1 %all-to-all-start = ((bf16[64,8,640]{2,1,0:T(8,128)(2,1)}), bf16[64,8,640]{2,1,0:T(8,128)(2,1)S(1)}, u32[]{:S(2)}, u32[]{:S(2)}) async-start(bf16[64,8,640]{2,1,0:T(8,128)(2,1)} %get-tuple-element.16), calls=%async_computation | async-start | bytes 1310720 | tf_op jit(solution)/shard_map/all_to_all | solution.py:418
  13.9 29.0 %collective-permute-start = (bf16[128,2048]{1,0:T(8,128)(2,1)}, bf16[128,2048]{1,0:T(8,128)(2,1)}, u32[]{:S(2)}, u32[]{:S(2)}) collective-permute-start(bf16[128,2048]{1,0:T(8,128)(2,1)} %get-tuple-element.17.after_ref), channel_id=1, source_target_pairs={{0,2},{2,0},{4,6},{6,4},{8,10},{10,8},{12,14},{14,12},{16,18},{18,... | collective-permute-start | bytes 1572872 | tf_op jit(solution)/shard_map/ppermute | solution.py:421
  14.8 28.1 %collective-permute-start.1 = (bf16[128,2048]{1,0:T(8,128)(2,1)}, bf16[128,2048]{1,0:T(8,128)(2,1)}, u32[]{:S(2)}, u32[]{:S(2)}) collective-permute-start(bf16[128,2048]{1,0:T(8,128)(2,1)} %get-tuple-element.22), channel_id=1, source_target_pairs={{2,4},{4,2},{6,8},{8,6},{10,12},{12,10},{14,16},{16,14},{18,20},{2... | collective-permute-start | bytes 1572872 | tf_op jit(solution)/shard_map/ppermute | solution.py:422
  20.5 22.3 %copy-start.3 = (f32[256]{0:T(256)S(1)}, f32[256]{0:T(256)}, u32[]{:S(2)}) copy-start(f32[256]{0:T(256)} %constant.26.clone) | copy-start | bytes 3076
  20.5 22.3 %copy-start.4 = (f32[256]{0:T(256)S(1)}, f32[256]{0:T(256)}, u32[]{:S(2)}) copy-start(f32[256]{0:T(256)} %constant.27.clone) | copy-start | bytes 3076
  20.5 22.4 %copy-start = (f32[16]{0:T(128)S(1)}, f32[16]{0:T(128)}, u32[]{:S(2)}) copy-start(f32[16]{0:T(128)} %sink_ref.1) | copy-start | bytes 196
  20.6 22.4 %copy-start.1 = (f32[64,256]{1,0:T(8,128)S(1)}, f32[64,256]{1,0:T(8,128)}, u32[]{:S(2)}) copy-start(f32[64,256]{1,0:T(8,128)} %constant.24.clone.colc_ref) | copy-start | bytes 196612
  20.6 22.4 %copy-start.2 = (f32[64,256]{1,0:T(8,128)S(1)}, f32[64,256]{1,0:T(8,128)}, u32[]{:S(2)}) copy-start(f32[64,256]{1,0:T(8,128)} %constant.25.clone.cols_ref) | copy-start | bytes 196612
  36.2 19.9 %all-to-all-start.1 = ((bf16[16,64,512]{2,1,0:T(8,128)(2,1)}), bf16[16,64,512]{2,1,0:T(8,128)(2,1)S(1)}, u32[]{:S(2)}, u32[]{:S(2)}) async-start(bf16[16,64,512]{2,1,0:T(8,128)(2,1)} %get-tuple-element.24), calls=%async_computation.1 | async-start | bytes 2097152 | tf_op jit(solution)/shard_map/all_to_all | solution.py:433
